TPU v7x, 32 devices: a whole 2x2x4 slice. The times are simulated.
32 devices in a mesh: ep: 4 (over y, x), tp: 8 (over z, core).
Axes of the slice: x: 2, y: 2, z: 4, core: 2. Of those that a mesh axis runs over, the one named last changes fastest.
Arguments:
- tokens: bfloat16 [96, 4096], P('ep'), may hold values from -6 to 6
- norm_gain: float32 [4096], replicated, may hold values from 0.1 to 1.9
- w_query: bfloat16 [4096, 2048], P('ep', 'tp'), may hold values from -0.09375 to 0.09375
- w_forget: bfloat16 [4096, 2048], P('ep', 'tp'), may hold values from -0.09375 to 0.09375
- w_input: bfloat16 [4096, 2048], P('ep', 'tp'), may hold values from -0.09375 to 0.09375
- w_outgate: bfloat16 [4096, 2048], P('ep', 'tp'), may hold values from -0.09375 to 0.09375
- forget_floor: float32 [2048], P('tp'), may hold values from 0.3 to 0.95
- head_gain: float32 [2048], P('tp'), may hold values from 0.1 to 1.9
- recurrent_state: float32 [96, 16, 128, 128], P('ep', 'tp'), may hold values from -2.4 to 2.4
- w_output: bfloat16 [2048, 4096], P('tp', 'ep'), may hold values from -0.125 to 0.125
- ffn_gain: float32 [4096], replicated, may hold values from 0.1 to 1.9
- w_router: bfloat16 [4096, 8], replicated, may hold values from -0.09375 to 0.09375
- routes: int32 [96, 2], P('ep'), may hold values from 0 to 7, all different within a row; in each aligned block of 24 rows (0 to 23, 24 to 47, ...) at most 12 rows name the same one
- expert_gate: bfloat16 [8, 4096, 2816], P('ep', None, 'tp'), may hold values from -0.09375 to 0.09375
- expert_up: bfloat16 [8, 4096, 2816], P('ep', None, 'tp'), may hold values from -0.09375 to 0.09375
- expert_down: bfloat16 [8, 2816, 4096], P('ep', 'tp'), may hold values from -0.109375 to 0.109375
- shared_gate_w: bfloat16 [4096, 2816], P('ep', 'tp'), may hold values from -0.09375 to 0.09375
- shared_up_w: bfloat16 [4096, 2816], P('ep', 'tp'), may hold values from -0.09375 to 0.09375
- shared_down_w: bfloat16 [2816, 4096], P('tp', 'ep'), may hold values from -0.109375 to 0.109375
- branch_gate: bfloat16 [4096], replicated, may hold values from -0.09375 to 0.09375
Outputs:
- layer_out: bfloat16 [96, 4096], P('ep', 'tp')
- new_state: float32 [96, 16, 128, 128], P('ep', 'tp')
Inputs may be any that keep to these rules, and one draw needn't show every extreme that they name: `routes`: each row names 2 different experts. Among the rows of one index of ep, no expert is named more than 12 times, a bound that some block reaches.
All inputs are finite; a program needn't handle non-finite values.
Results may differ from a plain program's by a relative error of at most 0.025.
Values may be sent and summed in bfloat16 or wider, within the bound.
No kernel may reach another device: no remote copies, remote signals or barrier semaphores. Data moves between devices by JAX's collectives and lax.ppermute only.
A program may use at most 64 MiB of HBM per device.

v0:
```python
import functools

import jax
import jax.numpy as jnp
from jax import lax
from jax.experimental import pallas as pl
from jax.experimental.pallas import tpu as pltpu
from jax.sharding import PartitionSpec as P


NORM_EPSILON = 1e-06
ROUTED_SCALE = 2.5
LANES = 128
F32 = jnp.float32
BF16 = jnp.bfloat16
VMEM = pl.BlockSpec(memory_space=pltpu.VMEM)
HBM = pl.BlockSpec(memory_space=pltpu.HBM)


def dot(a, b):
    return jnp.dot(a, b, preferred_element_type=F32)


def dot_t(a, b):
    return lax.dot_general(a, b, (((1,), (1,)), ((), ())), preferred_element_type=F32)


def silu(x):
    return x * jax.nn.sigmoid(x)


def swap(value, axis, size, step):
    return lax.ppermute(value, axis, [(s, s ^ step) for s in range(size)])


def inverse_rms(floats):
    return lax.rsqrt(jnp.mean(floats * floats, axis=-1, keepdims=True) + NORM_EPSILON)


def lane_slice(index, size):
    return pl.ds(pl.multiple_of(index * size, LANES), size)


def call(body, outs, ins, args, scratch=(), flops=0, limit=24):
    return pl.pallas_call(
        body,
        out_shape=[jax.ShapeDtypeStruct(s, d) for s, d in outs],
        in_specs=ins,
        out_specs=[VMEM] * len(outs),
        scratch_shapes=list(scratch),
        cost_estimate=pl.CostEstimate(flops=flops, bytes_accessed=0, transcendentals=0),
        compiler_params=pltpu.CompilerParams(vmem_limit_bytes=limit << 20),
    )(*args)


def prepare_kernel(tokens, *refs):
    outs, sems = refs[:-1], refs[-1]
    e = lax.axis_index("ep")
    block = outs[0].shape[1]
    copies = [
        pltpu.make_async_copy(tokens.at[:, lane_slice(e ^ k, block)], out, sems.at[k])
        for k, out in enumerate(outs)
    ]
    for copy in copies:
        copy.start()
    for copy in copies:
        copy.wait()


def route_mask(routes_t):
    batch = routes_t.shape[1]
    names = lax.broadcasted_iota(jnp.int32, (LANES, batch), 0)
    hit = names == routes_t[0:1, :]
    for j in range(1, routes_t.shape[0]):
        hit = hit | (names == routes_t[j : j + 1, :])
    eye = lax.broadcasted_iota(jnp.int32, (batch, batch), 0) == lax.broadcasted_iota(
        jnp.int32, (batch, batch), 1
    )
    return dot_t(jnp.where(eye, 1.0, 0.0).astype(BF16), jnp.where(hit, 1.0, 0.0).astype(BF16))


def fetch_kernel(arrays, *refs):
    sources, copied, token, sems = refs[:arrays], refs[-arrays - 2 : -2], refs[-2], refs[-1]
    copies = []
    for source, target in zip(sources, copied, strict=True):
        rows = target.shape[0]
        whole = 1 if target.ndim == 2 else rows
        parts = 4 if rows % (32 if target.ndim == 2 else 4) == 0 else whole
        step = rows // parts
        for p in range(parts):
            span = pl.ds(p * step, step)
            copies.append(
                pltpu.make_async_copy(source.at[span], target.at[span], sems.at[len(copies)])
            )
    for copy in copies:
        copy.start()
    for copy in copies:
        copy.wait()
    token[...] = jnp.zeros_like(token)


def fetch(arrays, after):
    arrays = [pltpu.with_memory_space_constraint(a, pltpu.HBM) for a in arrays]
    *copied, token = call(
        functools.partial(fetch_kernel, len(arrays)),
        [(a.shape, a.dtype) for a in arrays] + [((8, LANES), F32)],
        [HBM] * len(arrays) + [VMEM],
        (*arrays, after),
        [pltpu.SemaphoreType.DMA((24 * len(arrays),))],
        flops=1 << 26,
        limit=1,
    )
    return copied, token


def inverse_kernel(tokens, router_t, branch, out, router):
    out[...] = jnp.broadcast_to(inverse_rms(tokens[...].astype(F32)), out.shape)
    extra = jnp.broadcast_to(branch[...].astype(F32), (8, branch.shape[1]))
    router[...] = jnp.concatenate([router_t[...].astype(F32), extra], axis=0).astype(BF16)


def project_kernel(n_ep, *refs):
    payloads, gain, weights = refs[:n_ep], refs[n_ep], refs[n_ep + 1 : n_ep + 5]
    own, sent = refs[n_ep + 6], refs[n_ep + 7 :]
    batch = own.shape[0]
    block, channels = weights[0].shape
    row = gain[:, lane_slice(lax.axis_index("ep"), block)]
    scaled = jnp.concatenate([p[...].astype(F32) for p in payloads], axis=0) * row
    scaled = scaled.astype(BF16)
    for i, weight in enumerate(weights):
        part = dot(scaled, weight[...])
        lanes = slice(i * channels, (i + 1) * channels)
        own[:, lanes] = part[:batch]
        for k in range(1, n_ep):
            sent[k - 1][:, lanes] = part[k * batch : (k + 1) * batch].astype(BF16)


def columns_of(value):
    rows, lanes = value.shape
    return jnp.concatenate([value, jnp.zeros((LANES - rows, lanes), F32)], axis=0).T


def read_kernel(n_ep, *refs):
    own, got = refs[0], refs[1:n_ep]
    inverse, floor, head_gain, state, routes_t = refs[n_ep : n_ep + 5]
    mixed, gates, scratch = refs[n_ep + 6 :]
    batch, heads, size = state.shape[:3]
    channels = heads * size
    total = own[...]
    for g in got:
        total = total + g[...].astype(F32)
    total = total * inverse[:, 0:1]
    query, forget_pre, value, out_gate = (
        total[:, i * channels : (i + 1) * channels] for i in range(4)
    )
    low = floor[...]
    forget = low + (1.0 - low) * jax.nn.sigmoid(forget_pre)
    key = (1.0 - low) * jax.nn.sigmoid(-forget_pre)
    gates[:, :channels] = forget
    gates[:, channels : 2 * channels] = key
    gates[:, 2 * channels :] = value
    active = silu(query)
    weight = columns_of(active * forget)
    for b in range(batch):
        for h in range(heads):
            column = weight[h * size : (h + 1) * size, b : b + 1]
            scratch[b : b + 1, h * size : (h + 1) * size] = jnp.sum(
                column * state[b, h], axis=0, keepdims=True
            )
    mixed[:, channels:] = route_mask(routes_t[...]).astype(BF16)
    scale = head_gain[...] * silu(out_gate)
    for h in range(heads):
        lanes = slice(h * size, (h + 1) * size)
        read = scratch[:, lanes] + value[:, lanes] * jnp.sum(
            active[:, lanes] * key[:, lanes], axis=-1, keepdims=True
        )
        mixed[:, lanes] = (read * inverse_rms(read) * scale[:, lanes]).astype(BF16)


def update_kernel(group, gates, state, out, token, buffer, sems):
    batch, heads, size = state.shape[:3]
    channels = heads * size
    forget = columns_of(gates[:, :channels])
    key = columns_of(gates[:, channels : 2 * channels])
    copies = []
    for b in range(batch):
        for h in range(heads):
            rows = slice(h * size, (h + 1) * size)
            value = gates[b : b + 1, 2 * channels + h * size : 2 * channels + (h + 1) * size]
            buffer[b, h] = forget[rows, b : b + 1] * state[b, h] + key[rows, b : b + 1] * value
        if (b + 1) % group == 0:
            span = pl.ds(b + 1 - group, group)
            copies.append(
                pltpu.make_async_copy(buffer.at[span], out.at[span], sems.at[len(copies)])
            )
            copies[-1].start()
    for copy in copies:
        copy.wait()
    token[...] = jnp.zeros_like(token)


def output_kernel(n_ep, *refs):
    mixed, weight, give, keep = refs[:n_ep], refs[n_ep], refs[-2], refs[-1]
    c = lax.rem(lax.axis_index("tp"), 2)
    half = keep.shape[1]
    rows = jnp.concatenate([m[...].astype(F32) for m in mixed], axis=0).astype(BF16)
    rows = rows[:, : weight.shape[0]]
    give[...] = dot(rows, weight[:, lane_slice(1 - c, half)]).astype(BF16)
    keep[...] = dot(rows, weight[:, lane_slice(c, half)])


def add_kernel(keep, got, out):
    out[...] = (keep[...] + got[...].astype(F32)).astype(BF16)


def hidden_kernel(n_ep, *refs):
    payloads, keep, core, others = refs[:n_ep], refs[n_ep], refs[n_ep + 1], refs[n_ep + 2 : -2]
    out = refs[-1]
    c = lax.rem(lax.axis_index("tp"), 2)
    half = keep.shape[1]
    total = jnp.concatenate([p[:, lane_slice(c, half)].astype(F32) for p in payloads], axis=0)
    mixed = keep[...] + core[...].astype(F32)
    for other in others:
        mixed = mixed + other[...].astype(F32)
    out[...] = (total + mixed).astype(BF16)


def shared_kernel(mine, other, gain, gate_t, up_t, own, sent):
    c = lax.rem(lax.axis_index("tp"), 2)
    e = lax.axis_index("ep")
    half = mine.shape[1]
    inner, padded = gate_t.shape[0], own.shape[1] // 2
    own[...] = jnp.zeros_like(own)
    total = [None, None]
    for piece, h in ((mine, c), (other, 1 - c)):
        row = gain[:, lane_slice(2 * e + h, half)]
        scaled = (piece[...].astype(F32) * row).astype(BF16)
        for i, weight in enumerate((gate_t, up_t)):
            part = dot_t(scaled, weight[:, lane_slice(h, half)])
            total[i] = part if total[i] is None else total[i] + part
    for i in range(2):
        own[:, i * padded : i * padded + inner] = total[i]
    sent[...] = own[...].astype(BF16)


def expert_kernel(n_ep, *refs):
    pieces, others, payloads = refs[:n_ep], refs[n_ep : 2 * n_ep], refs[2 * n_ep : 3 * n_ep]
    gain, router, gate_w, up_w, down = refs[3 * n_ep : 3 * n_ep + 5]
    inner, scales, own_hidden, down_out, x_ref, n_ref, sems = refs[3 * n_ep + 5 :]
    local = inner.shape[0]
    fetches = [
        pltpu.make_async_copy(down.at[i], down_out.at[i], sems.at[i]) for i in range(local)
    ]
    for copy in fetches:
        copy.start()
    e = lax.axis_index("ep")
    t = lax.axis_index("tp")
    c = lax.rem(t, 2)
    rows, half = pieces[0].shape
    batch = rows // n_ep
    squares = jnp.zeros((rows, half), F32)
    for k in range(n_ep):
        for source, h in ((pieces[k], c), (others[k], 1 - c)):
            floats = source[...].astype(F32)
            floats = jnp.concatenate(
                [floats[(j ^ k) * batch : ((j ^ k) + 1) * batch] for j in range(n_ep)], axis=0
            )
            squares = squares + floats * floats
            x_ref[:, lane_slice(2 * (e ^ k) + h, half)] = floats
    width = x_ref.shape[1]
    inv = lax.rsqrt(jnp.sum(squares, axis=-1, keepdims=True) / width + NORM_EPSILON)
    own_hidden[...] = x_ref[:batch, lane_slice(t, own_hidden.shape[1])]
    n_ref[...] = (x_ref[...] * inv * gain[...]).astype(BF16)
    scores = jax.nn.sigmoid(dot_t(n_ref[...], router[...]))
    experts = router.shape[0] - 8
    lane = lax.broadcasted_iota(jnp.int32, scores.shape, 1)
    start = payloads[0].shape[1] - LANES
    mask = jnp.concatenate([p[:, start:].astype(F32) for p in payloads], axis=0)
    chosen = jnp.where(mask[:, : router.shape[0]] > 0.5, scores, 0.0)
    weights = chosen / jnp.sum(chosen, axis=1, keepdims=True) * ROUTED_SCALE
    branch = jnp.sum(jnp.where(lane == experts, scores, 0.0), axis=1, keepdims=True)
    spread = lax.broadcasted_iota(jnp.int32, scales.shape, 1)
    scales[...] = jnp.where(spread == 0, inv, branch)
    for i in range(local):
        combine = jnp.sum(jnp.where(lane == e * local + i, weights, 0.0), axis=1, keepdims=True)
        gate = dot_t(n_ref[...], gate_w[i])
        up = dot_t(n_ref[...], up_w[i])
        inner[i] = (silu(gate) * up * combine).astype(BF16)
    for copy in fetches:
        copy.wait()


def shared_activation(n_ep, shape, own, *refs):
    got, scales = refs[:-1], refs[-1]
    rows, width = shape
    batch = rows // n_ep
    total = own[...]
    for k in range(1, n_ep):
        floats = got[k - 1][...].astype(F32)
        total = total + jnp.concatenate(
            [floats[(j ^ k) * batch : ((j ^ k) + 1) * batch] for j in range(n_ep)], axis=0
        )
    total = total * scales[:, 0:1]
    padded = total.shape[1] // 2
    shared = silu(total[:, :padded]) * total[:, padded:] * scales[:, 1:2]
    return shared[:, :width].astype(BF16)


def down_kernel(n_ep, n_z, mine, inner, *refs):
    if mine:
        shared, weight, shared_down, out = refs
    else:
        *refs, weight, shared_down, out, shared = refs
        shared[...] = shared_activation(n_ep, shared.shape, *refs)
    e = lax.axis_index("ep")
    c = lax.rem(lax.axis_index("tp"), 2)
    h = c if mine else 1 - c
    size = weight.shape[2] // (2 * n_z)
    local = inner.shape[0]
    ratio = shared_down.shape[1] // size
    for z in range(n_z):
        lanes = lane_slice(2 * z + h, size)
        part = dot(inner[0], weight[0, :, lanes])
        for i in range(1, local):
            part = part + dot(inner[i], weight[i, :, lanes])
        out[:, z * size : (z + 1) * size] = part.astype(out.dtype)
    for z in range(n_z):
        q = 2 * z + h

        @pl.when(lax.div(q, ratio) == e)
        def _():
            lanes = slice(z * size, (z + 1) * size)
            extra = dot(shared[...], shared_down[:, lane_slice(lax.rem(q, ratio), size)])
            out[:, lanes] = (out[:, lanes].astype(F32) + extra).astype(out.dtype)


def merge_kernel(n_ep, keep, got, own, *sent):
    batch = own.shape[0]
    total = keep[...] + got[...].astype(F32)
    own[...] = total[:batch]
    for k in range(1, n_ep):
        sent[k - 1][...] = total[k * batch : (k + 1) * batch].astype(BF16)


def gather_kernel(n_ep, n_z, *refs):
    own, got = refs[0], refs[1:n_ep]
    hidden, base, sent, scratch = refs[n_ep], refs[n_ep + 1], refs[n_ep + 2 : -1], refs[-1]
    z = lax.div(lax.axis_index("tp"), 2)
    size = base.shape[1]
    total = own[...]
    for g in got:
        total = total + g[...].astype(F32)
    scratch[...] = total
    base[...] = hidden[...] + scratch[:, lane_slice(z, size)]
    for m in range(1, n_z):
        sent[m - 1][...] = scratch[:, lane_slice(z ^ m, size)].astype(BF16)


def finish_kernel(*refs):
    total = refs[0][...]
    for r in refs[1:-1]:
        total = total + r[...].astype(F32)
    refs[-1][...] = total.astype(BF16)


def make_body(n_ep, n_tp):
    n_z = n_tp // 2

    def ep_swap(value, k):
        return swap(value, "ep", n_ep, k)

    def z_swap(value, m):
        return swap(value, "tp", n_tp, 2 * m)

    def core_swap(value):
        return swap(value, "tp", n_tp, 1)

    def body(
        tokens, norm_gain, w_query, w_forget, w_input, w_outgate, forget_floor, head_gain,
        recurrent_state, w_output, ffn_gain, w_router, routes, expert_gate, expert_up,
        expert_down, shared_gate_w, shared_up_w, shared_down_w, branch_gate,
    ):
        batch, width = tokens.shape
        rows = n_ep * batch
        block = width // n_ep
        half = block // 2
        heads, size = recurrent_state.shape[1:3]
        channels = heads * size
        local, _, inner_width = expert_gate.shape
        shared_width = shared_gate_w.shape[1]
        slice_width = width // n_tp
        side = n_z * slice_width
        others = range(1, n_ep)

        payloads = call(
            prepare_kernel,
            [((batch, block), BF16)] * n_ep,
            [HBM],
            (pltpu.with_memory_space_constraint(tokens, pltpu.HBM),),
            [pltpu.SemaphoreType.DMA((n_ep,))],
        )
        own_payload = payloads[0]
        payloads = [own_payload] + [ep_swap(payloads[k], k) for k in others]

        (*weights, gain), token = fetch(
            (w_query, w_forget, w_input, w_outgate, norm_gain[None]), own_payload
        )
        own, *sent = call(
            functools.partial(project_kernel, n_ep),
            [((batch, 4 * channels), F32)] + [((batch, 4 * channels), BF16)] * (n_ep - 1),
            [VMEM] * (n_ep + 6),
            (*payloads, gain, *weights, token),
            flops=8 * rows * block * channels,
        )
        got = [ep_swap(sent[k - 1], k) for k in others]
        (state, full, router_t), token = fetch((recurrent_state, tokens, w_router.T), own)
        inverse, router = call(
            inverse_kernel,
            [((batch, LANES), F32), ((w_router.shape[1] + 8, width), BF16)],
            [VMEM] * 3,
            (full, router_t, branch_gate[None]),
        )


        mixed, gates = call(
            functools.partial(read_kernel, n_ep),
            [((batch, channels + LANES), BF16), ((batch, 3 * channels), F32)],
            [VMEM] * (n_ep + 6),
            (own, *got, inverse, forget_floor[None], head_gain[None], state, routes.T, token),
            [pltpu.VMEM((batch, channels), F32)],
            flops=1 << 24,
        )
        mixed_all = [mixed] + [ep_swap(mixed, k) for k in others]

        group = 4
        new_state, token = pl.pallas_call(
            functools.partial(update_kernel, group),
            out_shape=[
                jax.ShapeDtypeStruct(recurrent_state.shape, F32),
                jax.ShapeDtypeStruct((8, LANES), F32),
            ],
            in_specs=[VMEM] * 2,
            out_specs=[HBM, VMEM],
            scratch_shapes=[
                pltpu.VMEM(recurrent_state.shape, F32),
                pltpu.SemaphoreType.DMA((batch // group,)),
            ],
            cost_estimate=pl.CostEstimate(flops=1 << 26, bytes_accessed=0, transcendentals=0),
            compiler_params=pltpu.CompilerParams(vmem_limit_bytes=16 << 20),
        )(gates, state)

        give, keep = call(
            functools.partial(output_kernel, n_ep),
            [((rows, half), BF16), ((rows, half), F32)],
            [VMEM] * (n_ep + 2),
            (*mixed_all, w_output, token),
            flops=2 * rows * channels * block,
        )
        core = core_swap(give)
        (summed,) = call(add_kernel, [((rows, half), BF16)], [VMEM] * 2, (keep, core))
        along = [z_swap(summed, m) for m in range(1, n_z)]
        (gate_w, up_w), token = fetch(
            (jnp.swapaxes(expert_gate, 1, 2), jnp.swapaxes(expert_up, 1, 2)), summed
        )
        (part,) = call(
            functools.partial(hidden_kernel, n_ep),
            [((rows, half), BF16)],
            [VMEM] * (n_ep + n_z + 2),
            (*payloads, keep, core, *along, token),
        )

        pieces = [part] + [ep_swap(part, k) for k in others]
        sibling = core_swap(part)
        padded = -(-shared_width // LANES) * LANES
        shared_own, shared_sent = call(
            shared_kernel,
            [((rows, 2 * padded), F32), ((rows, 2 * padded), BF16)],
            [VMEM] * 5,
            (
                part, sibling, ffn_gain[None],
                jnp.swapaxes(shared_gate_w, 0, 1), jnp.swapaxes(shared_up_w, 0, 1),
            ),
            flops=4 * rows * block * shared_width,
        )
        siblings = [sibling] + [core_swap(pieces[k]) for k in others]
        shared_got = [ep_swap(shared_sent, k) for k in others]

        inner, scales, own_hidden, down_w = call(
            functools.partial(expert_kernel, n_ep),
            [
                ((local, rows, inner_width), BF16),
                ((rows, LANES), F32),
                ((batch, slice_width), F32),
                (expert_down.shape, BF16),
            ],
            [VMEM] * (3 * n_ep + 4) + [HBM],
            (
                *pieces, *siblings, *mixed_all, ffn_gain[None], router, gate_w, up_w,
                pltpu.with_memory_space_constraint(expert_down, pltpu.HBM),
            ),
            [
                pltpu.VMEM((rows, width), F32),
                pltpu.VMEM((rows, width), BF16),
                pltpu.SemaphoreType.DMA((local,)),
            ],
            flops=4 * rows * width * inner_width * local,
        )

        give, shared = call(
            functools.partial(down_kernel, n_ep, n_z, False),
            [((rows, side), BF16), ((rows, shared_width), BF16)],
            [VMEM] * (n_ep + 4),
            (inner, shared_own, *shared_got, scales, down_w, shared_down_w),
            flops=rows * width * inner_width * local,
        )
        core = core_swap(give)
        (keep,) = call(
            functools.partial(down_kernel, n_ep, n_z, True),
            [((rows, side), F32)],
            [VMEM] * 4,
            (inner, shared, down_w, shared_down_w),
            flops=rows * width * inner_width * local,
        )
        own, *sent = call(
            functools.partial(merge_kernel, n_ep),
            [((batch, side), F32)] + [((batch, side), BF16)] * (n_ep - 1),
            [VMEM] * 2,
            (keep, core),
        )
        got = [ep_swap(sent[k - 1], k) for k in others]
        base, *sent = call(
            functools.partial(gather_kernel, n_ep, n_z),
            [((batch, slice_width), F32)] + [((batch, slice_width), BF16)] * (n_z - 1),
            [VMEM] * (n_ep + 1),
            (own, *got, own_hidden),
            [pltpu.VMEM((batch, side), F32)],
        )
        got = [z_swap(sent[m - 1], m) for m in range(1, n_z)]
        (layer_out,) = call(
            finish_kernel, [((batch, slice_width), BF16)], [VMEM] * n_z, (base, *got)
        )
        return layer_out, new_state

    return body


def solution(mesh):
    body = make_body(mesh.shape["ep"], mesh.shape["tp"])

    return jax.shard_map(
        body,
        mesh=mesh,
        in_specs=(
            P("ep", None),
            P(),
            P("ep", "tp"),
            P("ep", "tp"),
            P("ep", "tp"),
            P("ep", "tp"),
            P("tp"),
            P("tp"),
            P("ep", "tp", None, None),
            P("tp", "ep"),
            P(),
            P(),
            P("ep", None),
            P("ep", None, "tp"),
            P("ep", None, "tp"),
            P("ep", "tp", None),
            P("ep", "tp"),
            P("ep", "tp"),
            P("tp", "ep"),
            P(),
        ),
        out_specs=(P("ep", "tp"), P("ep", "tp", None, None)),
        check_vma=False,
    )
```

profile of v0, /device:TPU:0, one launch (start us, length us, event | category | flops | bytes accessed | tf_op | source)
XLA Modules:
  0.0 78.3 jit_solution(7520313047197367315)
XLA Ops:
  0.7 0.9 %shard_map.203 = (bf16[24,1024]{1,0:T(8,128)(2,1)S(1)}, bf16[24,1024]{1,0:T(8,128)(2,1)S(1)}, bf16[24,1024]{1,0:T(8,128)(2,1)S(1)}, bf16[24,1024]{1,0:T(8,128)(2,1)S(1)}) custom-call(bf16[24,4096]{1,0:T(8,128)(2,1)} %refs_1_.3), custom_call_target="tpu_custom_call" | custom-call | tf_op jit(solution)/shard_map/pallas_call | solution.py:45
  1.6 3.0 %collective-permute-start = (bf16[24,1024]{1,0:T(8,128)(2,1)S(1)}, bf16[24,1024]{1,0:T(8,128)(2,1)S(1)}, u32[]{:S(2)}, u32[]{:S(2)}) collective-permute-start(bf16[24,1024]{1,0:T(8,128)(2,1)S(1)} %get-tuple-element.48), channel_id=1, source_target_pairs={{0,8},{8,0},{16,24},{24,16},{1,9},{9,1},{17,25},{25,17},{2,10},{10... | collective-permute-start | bytes 147464 | tf_op jit(solution)/shard_map/ppermute | solution.py:33
  4.6 1.5 %collective-permute-start.1 = (bf16[24,1024]{1,0:T(8,128)(2,1)S(1)}, bf16[24,1024]{1,0:T(8,128)(2,1)S(1)}, u32[]{:S(2)}, u32[]{:S(2)}) collective-permute-start(bf16[24,1024]{1,0:T(8,128)(2,1)S(1)} %get-tuple-element.49), channel_id=1, source_target_pairs={{0,16},{8,24},{16,0},{24,8},{1,17},{9,25},{17,1},{25,9},{2,18},{10... | collective-permute-start | bytes 147464 | tf_op jit(solution)/shard_map/ppermute | solution.py:33
  6.2 2.7 %shard_map.204 = (bf16[1024,256]{1,0:T(8,128)(2,1)S(1)}, bf16[1024,256]{1,0:T(8,128)(2,1)S(1)}, bf16[1024,256]{1,0:T(8,128)(2,1)S(1)}, bf16[1024,256]{1,0:T(8,12...) custom-call(bf16[1024,256]{1,0:T(8,128)(2,1)} %refs_0_.2, bf16[1024,256]{1,0:T(8,128)(2,1)} %refs_1_.2, ...), custom_call_target="tpu_custom_call" | custom-call | flops 67108864 | tf_op jit(solution)/shard_map/pallas_call | solution.py:45
  8.9 2.3 %collective-permute-done.2.refs_3_ = bf16[24,1024]{1,0:T(8,128)(2,1)S(1)} collective-permute-done((bf16[24,1024]{1,0:T(8,128)(2,1)S(1)}, bf16[24,1024]{1,0:T(8,128)(2,1)S(1)}, u32[]{:S(2)}, u32[]{:S(2)}) %collective-permute-start.2) | collective-permute-done | bytes 49184 | tf_op jit(solution)/shard_map/ppermute | solution.py:33
  11.1 0.5 shard_map.205
  11.6 0.6 collective-permute-start.3
  12.2 0.7 collective-permute-start.4
  12.9 2.3 %collective-permute-start.5 = (bf16[24,1024]{1,0:T(8,128)(2,1)S(1)}, bf16[24,1024]{1,0:T(8,128)(2,1)S(1)}, u32[]{:S(2)}, u32[]{:S(2)}) collective-permute-start(bf16[24,1024]{1,0:T(8,128)(2,1)S(1)} %get-tuple-element.60), channel_id=1, source_target_pairs={{0,24},{8,16},{16,8},{24,0},{1,25},{9,17},{17,9},{25,1},{2,26},{10... | collective-permute-start | bytes 147464 | tf_op jit(solution)/shard_map/ppermute | solution.py:33
  15.2 0.7 broadcast_in_dim.17.branch
  15.9 2.5 %shard_map.206 = (f32[24,2,128,128]{3,2,1,0:T(8,128)S(1)}, bf16[24,4096]{1,0:T(8,128)(2,1)S(1)}, bf16[8,4096]{1,0:T(8,128)(2,1)S(1)}, f32[8,128]{1,0:T(8,128)S(1)}) custom-call(f32[24,2,128,128]{3,2,1,0:T(8,128)} %refs_0_.3, bf16[24,4096]{1,0:T(8,128)(2,1)} %refs_1_.3, bf16[8,4096]{1,0:T(8,128)(2,1)} %bitcast.19, ...), custom_call_target="tpu_custom_call" | custom-call | flops 67108864 | tf_op jit(solution)/shard_map/pallas_call | solution.py:45
  18.6 1.2 %shard_map.208 = (bf16[24,384]{1,0:T(8,128)(2,1)S(1)}, f32[24,768]{1,0:T(8,128)S(1)}) custom-call(f32[24,1024]{1,0:T(8,128)S(1)} %get-tuple-element.57.refs_3_.refs_0_, bf16[24,1024]{1,0:T(8,128)(2,1)S(1)} %collective-permute-done.3.refs_1_, bf16[24,1024]{1,0:T(8,128)(2,1)S(1)} %collective-permute-done.4.refs_2_, ...), custom_call_target="tpu_custom_call" | custom-call | flops 16777216 | tf_op jit(solution)/shard_map/pallas_call | solution.py:45
  19.8 1.6 %collective-permute-start.8 = (bf16[24,384]{1,0:T(8,128)(2,1)S(1)}, bf16[24,384]{1,0:T(8,128)(2,1)S(1)}, u32[]{:S(2)}, u32[]{:S(2)}) collective-permute-start(bf16[24,384]{1,0:T(8,128)(2,1)S(1)} %get-tuple-element.66.refs_0_.refs_8_), channel_id=1, source_target_pairs={{0,24},{8,16},{16,8},{24,0},{1,25},{9,17},{17,9},{25,1},{2,26},{10... | collective-permute-start | bytes 55304 | tf_op jit(solution)/shard_map/ppermute | solution.py:33
  21.5 0.5 collective-permute-start.7
  22.0 1.4 %collective-permute-start.6 = (bf16[24,384]{1,0:T(8,128)(2,1)S(1)}, bf16[24,384]{1,0:T(8,128)(2,1)S(1)}, u32[]{:S(2)}, u32[]{:S(2)}) collective-permute-start(bf16[24,384]{1,0:T(8,128)(2,1)S(1)} %get-tuple-element.66.refs_0_.refs_8_), channel_id=1, source_target_pairs={{0,8},{8,0},{16,24},{24,16},{1,9},{9,1},{17,25},{25,17},{2,10},{10... | collective-permute-start | bytes 55304 | tf_op jit(solution)/shard_map/ppermute | solution.py:33
  23.4 2.7 %shard_map.209 = (f32[24,2,128,128]{3,2,1,0:T(8,128)}, f32[8,128]{1,0:T(8,128)S(1)}) custom-call(f32[24,768]{1,0:T(8,128)S(1)} %get-tuple-element.67.gates, f32[24,2,128,128]{3,2,1,0:T(8,128)S(1)} %get-tuple-element.64.refs_7_.state), custom_call_target="tpu_custom_call" | custom-call | flops 67108864 | tf_op jit(solution)/shard_map/pallas_call | solution.py:436
  26.4 1.3 %collective-permute-done.9.got.refs_5_ = bf16[96,512]{1,0:T(8,128)(2,1)S(1)} collective-permute-done((bf16[96,512]{1,0:T(8,128)(2,1)S(1)}, bf16[96,512]{1,0:T(8,128)(2,1)S(1)}, u32[]{:S(2)}, u32[]{:S(2)}) %collective-permute-start.9) | collective-permute-done | bytes 98336 | tf_op jit(solution)/shard_map/ppermute | solution.py:33
  27.8 3.7 %collective-permute-start.12 = (bf16[96,512]{1,0:T(8,128)(2,1)S(1)}, bf16[96,512]{1,0:T(8,128)(2,1)S(1)}, u32[]{:S(2)}, u32[]{:S(2)}) collective-permute-start(bf16[96,512]{1,0:T(8,128)(2,1)S(1)} %shard_map.211.refs_2_), channel_id=1, source_target_pairs={{0,6},{1,7},{2,4},{3,5},{4,2},{5,3},{6,0},{7,1},{8,14},{9,15},{10,... | collective-permute-start | bytes 294920 | tf_op jit(solution)/shard_map/ppermute | solution.py:33
  31.4 0.8 collective-permute-start.10
  32.2 4.9 %shard_map.212 = (bf16[2,352,4096]{2,1,0:T(8,128)(2,1)S(1)}, bf16[2,352,4096]{2,1,0:T(8,128)(2,1)S(1)}, f32[8,128]{1,0:T(8,128)S(1)}) custom-call(bf16[2,352,4096]{2,1,0:T(8,128)(2,1)} %bitcast.17, bf16[2,352,4096]{2,1,0:T(8,128)(2,1)} %bitcast.18, bf16[96,512]{1,0:T(8,128)(2,1)S(1)} %shard_map.211.refs_2_), custom_call_target="tpu_custom_call" | custom-call | flops 67108864 | tf_op jit(solution)/shard_map/pallas_call | solution.py:45
  37.1 2.9 %collective-permute-done.11.refs_7_ = bf16[96,512]{1,0:T(8,128)(2,1)S(1)} collective-permute-done((bf16[96,512]{1,0:T(8,128)(2,1)S(1)}, bf16[96,512]{1,0:T(8,128)(2,1)S(1)}, u32[]{:S(2)}, u32[]{:S(2)}) %collective-permute-start.11) | collective-permute-done | bytes 98336 | tf_op jit(solution)/shard_map/ppermute | solution.py:33
  40.1 1.6 %collective-permute-start.15 = (bf16[96,512]{1,0:T(8,128)(2,1)S(1)}, bf16[96,512]{1,0:T(8,128)(2,1)S(1)}, u32[]{:S(2)}, u32[]{:S(2)}) collective-permute-start(bf16[96,512]{1,0:T(8,128)(2,1)S(1)} %shard_map.213.refs_0_.mine), channel_id=1, source_target_pairs={{0,24},{8,16},{16,8},{24,0},{1,25},{9,17},{17,9},{25,1},{2,26},{10... | collective-permute-start | bytes 294920 | tf_op jit(solution)/shard_map/ppermute | solution.py:33
  41.7 0.9 %collective-permute-start.14 = (bf16[96,512]{1,0:T(8,128)(2,1)S(1)}, bf16[96,512]{1,0:T(8,128)(2,1)S(1)}, u32[]{:S(2)}, u32[]{:S(2)}) collective-permute-start(bf16[96,512]{1,0:T(8,128)(2,1)S(1)} %shard_map.213.refs_0_.mine), channel_id=1, source_target_pairs={{0,16},{8,24},{16,0},{24,8},{1,17},{9,25},{17,1},{25,9},{2,18},{10... | collective-permute-start | bytes 294920 | tf_op jit(solution)/shard_map/ppermute | solution.py:33
  42.6 1.0 %collective-permute-start.13 = (bf16[96,512]{1,0:T(8,128)(2,1)S(1)}, bf16[96,512]{1,0:T(8,128)(2,1)S(1)}, u32[]{:S(2)}, u32[]{:S(2)}) collective-permute-start(bf16[96,512]{1,0:T(8,128)(2,1)S(1)} %shard_map.213.refs_0_.mine), channel_id=1, source_target_pairs={{0,8},{8,0},{16,24},{24,16},{1,9},{9,1},{17,25},{25,17},{2,10},{10... | collective-permute-start | bytes 294920 | tf_op jit(solution)/shard_map/ppermute | solution.py:33
  43.6 3.1 %collective-permute-done.15.refs_3_ = bf16[96,512]{1,0:T(8,128)(2,1)S(1)} collective-permute-done((bf16[96,512]{1,0:T(8,128)(2,1)S(1)}, bf16[96,512]{1,0:T(8,128)(2,1)S(1)}, u32[]{:S(2)}, u32[]{:S(2)}) %collective-permute-start.15) | collective-permute-done | bytes 98336 | tf_op jit(solution)/shard_map/ppermute | solution.py:33
  46.7 0.4 collective-permute-done.14.refs_2_
  47.3 0.4 collective-permute-start.17
  47.7 0.6 shard_map.215
  48.3 1.6 %collective-permute-start.22 = (bf16[96,768]{1,0:T(8,128)(2,1)S(1)}, bf16[96,768]{1,0:T(8,128)(2,1)S(1)}, u32[]{:S(2)}, u32[]{:S(2)}) collective-permute-start(bf16[96,768]{1,0:T(8,128)(2,1)S(1)} %get-tuple-element.77), channel_id=1, source_target_pairs={{0,24},{8,16},{16,8},{24,0},{1,25},{9,17},{17,9},{25,1},{2,26},{10... | collective-permute-start | bytes 442376 | tf_op jit(solution)/shard_map/ppermute | solution.py:33
  49.9 0.9 %collective-permute-start.21 = (bf16[96,768]{1,0:T(8,128)(2,1)S(1)}, bf16[96,768]{1,0:T(8,128)(2,1)S(1)}, u32[]{:S(2)}, u32[]{:S(2)}) collective-permute-start(bf16[96,768]{1,0:T(8,128)(2,1)S(1)} %get-tuple-element.77), channel_id=1, source_target_pairs={{0,16},{8,24},{16,0},{24,8},{1,17},{9,25},{17,1},{25,9},{2,18},{10... | collective-permute-start | bytes 442376 | tf_op jit(solution)/shard_map/ppermute | solution.py:33
  50.8 1.0 %collective-permute-start.20 = (bf16[96,768]{1,0:T(8,128)(2,1)S(1)}, bf16[96,768]{1,0:T(8,128)(2,1)S(1)}, u32[]{:S(2)}, u32[]{:S(2)}) collective-permute-start(bf16[96,768]{1,0:T(8,128)(2,1)S(1)} %get-tuple-element.77), channel_id=1, source_target_pairs={{0,8},{8,0},{16,24},{24,16},{1,9},{9,1},{17,25},{25,17},{2,10},{10... | collective-permute-start | bytes 442376 | tf_op jit(solution)/shard_map/ppermute | solution.py:33
  51.8 3.8 %shard_map.214 = (bf16[2,96,352]{2,1,0:T(8,128)(2,1)S(1)}, f32[96,128]{1,0:T(8,128)S(1)}, f32[24,512]{1,0:T(8,128)S(1)}, bf16[2,352,4096]{2,1,0:T(8,128)(2,1)S(1)}) custom-call(bf16[96,512]{1,0:T(8,128)(2,1)S(1)} %shard_map.213.refs_0_.mine, bf16[96,512]{1,0:T(8,128)(2,1)S(1)} %collective-permute-done.13.refs_1_, ...), custom_call_target="tpu_custom_call" | custom-call | flops 1107296256 | tf_op jit(solution)/shard_map/pallas_call | solution.py:45
  55.6 0.4 collective-permute-done.22.refs_3_
  56.0 2.2 %collective-permute-done.21.refs_2_ = bf16[96,768]{1,0:T(8,128)(2,1)S(1)} collective-permute-done((bf16[96,768]{1,0:T(8,128)(2,1)S(1)}, bf16[96,768]{1,0:T(8,128)(2,1)S(1)}, u32[]{:S(2)}, u32[]{:S(2)}) %collective-permute-start.21) | collective-permute-done | bytes 147488 | tf_op jit(solution)/shard_map/ppermute | solution.py:33
  58.2 0.9 %shard_map.216 = (bf16[96,2048]{1,0:T(8,128)(2,1)S(1)}, bf16[96,352]{1,0:T(8,128)(2,1)S(1)}) custom-call(bf16[2,96,352]{2,1,0:T(8,128)(2,1)S(1)} %get-tuple-element.75.inner, f32[96,768]{1,0:T(8,128)S(1)} %get-tuple-element.76.refs_0_, bf16[96,768]{1,0:T(8,128)(2,1)S(1)} %collective-permute-done.20.refs_1_, ...), custom_call_target="tpu_custom_call" | custom-call | flops 276824064 | tf_op jit(solution)/shard_map/pallas_call | solution.py:45
  59.3 1.0 %shard_map.217.keep = f32[96,2048]{1,0:T(8,128)S(1)} custom-call(bf16[2,96,352]{2,1,0:T(8,128)(2,1)S(1)} %get-tuple-element.75.inner, bf16[96,352]{1,0:T(8,128)(2,1)S(1)} %get-tuple-element.80.refs_0_, bf16[2,352,4096]{2,1,0:T(8,128)(2,1)S(1)} %get-tuple-element.79.refs_5_.refs_1_, bf16[352,1024]{1,0:T(8,128)(2,1)S(1)} %copy-done), custom_call_target="tpu_custom_call" | custom-call | flops 276824064 | tf_op jit(solution)/shard_map/pallas_call | solution.py:45
  60.2 0.7 collective-permute-done.23.got
  61.0 1.1 %collective-permute-start.24 = (bf16[24,2048]{1,0:T(8,128)(2,1)S(1)}, bf16[24,2048]{1,0:T(8,128)(2,1)S(1)}, u32[]{:S(2)}, u32[]{:S(2)}) collective-permute-start(bf16[24,2048]{1,0:T(8,128)(2,1)S(1)} %get-tuple-element.83), channel_id=1, source_target_pairs={{0,8},{8,0},{16,24},{24,16},{1,9},{9,1},{17,25},{25,17},{2,10},{10... | collective-permute-start | bytes 294920 | tf_op jit(solution)/shard_map/ppermute | solution.py:33
  62.1 1.1 %collective-permute-start.25 = (bf16[24,2048]{1,0:T(8,128)(2,1)S(1)}, bf16[24,2048]{1,0:T(8,128)(2,1)S(1)}, u32[]{:S(2)}, u32[]{:S(2)}) collective-permute-start(bf16[24,2048]{1,0:T(8,128)(2,1)S(1)} %get-tuple-element.84), channel_id=1, source_target_pairs={{0,16},{8,24},{16,0},{24,8},{1,17},{9,25},{17,1},{25,9},{2,18},{10... | collective-permute-start | bytes 294920 | tf_op jit(solution)/shard_map/ppermute | solution.py:33
  63.2 1.4 %collective-permute-start.26 = (bf16[24,2048]{1,0:T(8,128)(2,1)S(1)}, bf16[24,2048]{1,0:T(8,128)(2,1)S(1)}, u32[]{:S(2)}, u32[]{:S(2)}) collective-permute-start(bf16[24,2048]{1,0:T(8,128)(2,1)S(1)} %get-tuple-element.85), channel_id=1, source_target_pairs={{0,24},{8,16},{16,8},{24,0},{1,25},{9,17},{17,9},{25,1},{2,26},{10... | collective-permute-start | bytes 294920 | tf_op jit(solution)/shard_map/ppermute | solution.py:33
  64.6 1.5 %collective-permute-done.24.refs_1_ = bf16[24,2048]{1,0:T(8,128)(2,1)S(1)} collective-permute-done((bf16[24,2048]{1,0:T(8,128)(2,1)S(1)}, bf16[24,2048]{1,0:T(8,128)(2,1)S(1)}, u32[]{:S(2)}, u32[]{:S(2)}) %collective-permute-start.24) | collective-permute-done | bytes 98336 | tf_op jit(solution)/shard_map/ppermute | solution.py:33
  66.1 2.7 %collective-permute-done.25.refs_2_ = bf16[24,2048]{1,0:T(8,128)(2,1)S(1)} collective-permute-done((bf16[24,2048]{1,0:T(8,128)(2,1)S(1)}, bf16[24,2048]{1,0:T(8,128)(2,1)S(1)}, u32[]{:S(2)}, u32[]{:S(2)}) %collective-permute-start.25) | collective-permute-done | bytes 98336 | tf_op jit(solution)/shard_map/ppermute | solution.py:33
  68.9 0.6 collective-permute-start.27
  69.5 2.5 %collective-permute-start.28 = (bf16[24,512]{1,0:T(8,128)(2,1)S(1)}, bf16[24,512]{1,0:T(8,128)(2,1)S(1)}, u32[]{:S(2)}, u32[]{:S(2)}) collective-permute-start(bf16[24,512]{1,0:T(8,128)(2,1)S(1)} %get-tuple-element.89), channel_id=1, source_target_pairs={{0,4},{1,5},{2,6},{3,7},{4,0},{5,1},{6,2},{7,3},{8,12},{9,13},{10,... | collective-permute-start | bytes 73736 | tf_op jit(solution)/shard_map/ppermute | solution.py:33
  72.0 1.3 %collective-permute-start.29 = (bf16[24,512]{1,0:T(8,128)(2,1)S(1)}, bf16[24,512]{1,0:T(8,128)(2,1)S(1)}, u32[]{:S(2)}, u32[]{:S(2)}) collective-permute-start(bf16[24,512]{1,0:T(8,128)(2,1)S(1)} %get-tuple-element.90), channel_id=1, source_target_pairs={{0,6},{1,7},{2,4},{3,5},{4,2},{5,3},{6,0},{7,1},{8,14},{9,15},{10,... | collective-permute-start | bytes 73736 | tf_op jit(solution)/shard_map/ppermute | solution.py:33
  73.4 0.8 %collective-permute-done.28.refs_2_ = bf16[24,512]{1,0:T(8,128)(2,1)S(1)} collective-permute-done((bf16[24,512]{1,0:T(8,128)(2,1)S(1)}, bf16[24,512]{1,0:T(8,128)(2,1)S(1)}, u32[]{:S(2)}, u32[]{:S(2)}) %collective-permute-start.28) | collective-permute-done | bytes 24608 | tf_op jit(solution)/shard_map/ppermute | solution.py:33
  74.2 3.4 %collective-permute-done.29.refs_3_ = bf16[24,512]{1,0:T(8,128)(2,1)S(1)} collective-permute-done((bf16[24,512]{1,0:T(8,128)(2,1)S(1)}, bf16[24,512]{1,0:T(8,128)(2,1)S(1)}, u32[]{:S(2)}, u32[]{:S(2)}) %collective-permute-start.29) | collective-permute-done | bytes 24608 | tf_op jit(solution)/shard_map/ppermute | solution.py:33
  77.7 0.6 shard_map.220
  (47 shorter events, 1.0 us)
Async XLA Ops:
  0.6 17.9 %copy-start.7 = (s32[24,2]{0,1:T(2,128)S(1)}, s32[24,2]{0,1:T(2,128)}, u32[]{:S(2)}) copy-start(s32[24,2]{0,1:T(2,128)} %param.32) | copy-start | bytes 580
  0.6 17.9 %copy-start.6 = (f32[256]{0:T(256)S(1)}, f32[256]{0:T(256)}, u32[]{:S(2)}) copy-start(f32[256]{0:T(256)} %param.27) | copy-start | bytes 3076
  0.7 17.9 %copy-start.5 = (f32[256]{0:T(256)S(1)}, f32[256]{0:T(256)}, u32[]{:S(2)}) copy-start(f32[256]{0:T(256)} %param.26) | copy-start | bytes 3076
  1.6 7.2 %collective-permute-start = (bf16[24,1024]{1,0:T(8,128)(2,1)S(1)}, bf16[24,1024]{1,0:T(8,128)(2,1)S(1)}, u32[]{:S(2)}, u32[]{:S(2)}) collective-permute-start(bf16[24,1024]{1,0:T(8,128)(2,1)S(1)} %get-tuple-element.48), channel_id=1, source_target_pairs={{0,8},{8,0},{16,24},{24,16},{1,9},{9,1},{17,25},{25,17},{2,10},{10... | collective-permute-start | bytes 147464 | tf_op jit(solution)/shard_map/ppermute | solution.py:33
  4.6 4.2 %collective-permute-start.1 = (bf16[24,1024]{1,0:T(8,128)(2,1)S(1)}, bf16[24,1024]{1,0:T(8,128)(2,1)S(1)}, u32[]{:S(2)}, u32[]{:S(2)}) collective-permute-start(bf16[24,1024]{1,0:T(8,128)(2,1)S(1)} %get-tuple-element.49), channel_id=1, source_target_pairs={{0,16},{8,24},{16,0},{24,8},{1,17},{9,25},{17,1},{25,9},{2,18},{10... | collective-permute-start | bytes 147464 | tf_op jit(solution)/shard_map/ppermute | solution.py:33
  6.1 5.0 %collective-permute-start.2 = (bf16[24,1024]{1,0:T(8,128)(2,1)S(1)}, bf16[24,1024]{1,0:T(8,128)(2,1)S(1)}, u32[]{:S(2)}, u32[]{:S(2)}) collective-permute-start(bf16[24,1024]{1,0:T(8,128)(2,1)S(1)} %get-tuple-element.50), channel_id=1, source_target_pairs={{0,24},{8,16},{16,8},{24,0},{1,25},{9,17},{17,9},{25,1},{2,26},{10... | collective-permute-start | bytes 147464 | tf_op jit(solution)/shard_map/ppermute | solution.py:33
  11.6 14.5 %copy-start.3 = (bf16[256,1024]{1,0:T(8,128)(2,1)S(1)}, bf16[256,1024]{1,0:T(8,128)(2,1)}, u32[]{:S(2)}) copy-start(bf16[256,1024]{1,0:T(8,128)(2,1)} %refs_4_.1) | copy-start | bytes 1572868
  11.6 6.9 %collective-permute-start.3 = (bf16[24,1024]{1,0:T(8,128)(2,1)S(1)}, bf16[24,1024]{1,0:T(8,128)(2,1)S(1)}, u32[]{:S(2)}, u32[]{:S(2)}) collective-permute-start(bf16[24,1024]{1,0:T(8,128)(2,1)S(1)} %get-tuple-element.58), channel_id=1, source_target_pairs={{0,8},{8,0},{16,24},{24,16},{1,9},{9,1},{17,25},{25,17},{2,10},{10... | collective-permute-start | bytes 147464 | tf_op jit(solution)/shard_map/ppermute | solution.py:33
  12.2 6.3 %collective-permute-start.4 = (bf16[24,1024]{1,0:T(8,128)(2,1)S(1)}, bf16[24,1024]{1,0:T(8,128)(2,1)S(1)}, u32[]{:S(2)}, u32[]{:S(2)}) collective-permute-start(bf16[24,1024]{1,0:T(8,128)(2,1)S(1)} %get-tuple-element.59), channel_id=1, source_target_pairs={{0,16},{8,24},{16,0},{24,8},{1,17},{9,25},{17,1},{25,9},{2,18},{10... | collective-permute-start | bytes 147464 | tf_op jit(solution)/shard_map/ppermute | solution.py:33
  12.9 5.7 %collective-permute-start.5 = (bf16[24,1024]{1,0:T(8,128)(2,1)S(1)}, bf16[24,1024]{1,0:T(8,128)(2,1)S(1)}, u32[]{:S(2)}, u32[]{:S(2)}) collective-permute-start(bf16[24,1024]{1,0:T(8,128)(2,1)S(1)} %get-tuple-element.60), channel_id=1, source_target_pairs={{0,24},{8,16},{16,8},{24,0},{1,25},{9,17},{17,9},{25,1},{2,26},{10... | collective-permute-start | bytes 147464 | tf_op jit(solution)/shard_map/ppermute | solution.py:33
  19.8 6.3 %collective-permute-start.8 = (bf16[24,384]{1,0:T(8,128)(2,1)S(1)}, bf16[24,384]{1,0:T(8,128)(2,1)S(1)}, u32[]{:S(2)}, u32[]{:S(2)}) collective-permute-start(bf16[24,384]{1,0:T(8,128)(2,1)S(1)} %get-tuple-element.66.refs_0_.refs_8_), channel_id=1, source_target_pairs={{0,24},{8,16},{16,8},{24,0},{1,25},{9,17},{17,9},{25,1},{2,26},{10... | collective-permute-start | bytes 55304 | tf_op jit(solution)/shard_map/ppermute | solution.py:33
  21.5 4.6 %collective-permute-start.7 = (bf16[24,384]{1,0:T(8,128)(2,1)S(1)}, bf16[24,384]{1,0:T(8,128)(2,1)S(1)}, u32[]{:S(2)}, u32[]{:S(2)}) collective-permute-start(bf16[24,384]{1,0:T(8,128)(2,1)S(1)} %get-tuple-element.66.refs_0_.refs_8_), channel_id=1, source_target_pairs={{0,16},{8,24},{16,0},{24,8},{1,17},{9,25},{17,1},{25,9},{2,18},{10... | collective-permute-start | bytes 55304 | tf_op jit(solution)/shard_map/ppermute | solution.py:33
  22.0 4.1 %collective-permute-start.6 = (bf16[24,384]{1,0:T(8,128)(2,1)S(1)}, bf16[24,384]{1,0:T(8,128)(2,1)S(1)}, u32[]{:S(2)}, u32[]{:S(2)}) collective-permute-start(bf16[24,384]{1,0:T(8,128)(2,1)S(1)} %get-tuple-element.66.refs_0_.refs_8_), channel_id=1, source_target_pairs={{0,8},{8,0},{16,24},{24,16},{1,9},{9,1},{17,25},{25,17},{2,10},{10... | collective-permute-start | bytes 55304 | tf_op jit(solution)/shard_map/ppermute | solution.py:33
  26.4 1.4 %collective-permute-start.9 = (bf16[96,512]{1,0:T(8,128)(2,1)S(1)}, bf16[96,512]{1,0:T(8,128)(2,1)S(1)}, u32[]{:S(2)}, u32[]{:S(2)}) collective-permute-start(bf16[96,512]{1,0:T(8,128)(2,1)S(1)} %get-tuple-element.70), channel_id=1, source_target_pairs={{0,1},{1,0},{2,3},{3,2},{4,5},{5,4},{6,7},{7,6},{8,9},{9,8},{10,11... | collective-permute-start | bytes 294920 | tf_op jit(solution)/shard_map/ppermute | solution.py:33
  27.8 9.4 %collective-permute-start.12 = (bf16[96,512]{1,0:T(8,128)(2,1)S(1)}, bf16[96,512]{1,0:T(8,128)(2,1)S(1)}, u32[]{:S(2)}, u32[]{:S(2)}) collective-permute-start(bf16[96,512]{1,0:T(8,128)(2,1)S(1)} %shard_map.211.refs_2_), channel_id=1, source_target_pairs={{0,6},{1,7},{2,4},{3,5},{4,2},{5,3},{6,0},{7,1},{8,14},{9,15},{10,... | collective-permute-start | bytes 294920 | tf_op jit(solution)/shard_map/ppermute | solution.py:33
  31.4 8.6 %collective-permute-start.11 = (bf16[96,512]{1,0:T(8,128)(2,1)S(1)}, bf16[96,512]{1,0:T(8,128)(2,1)S(1)}, u32[]{:S(2)}, u32[]{:S(2)}) collective-permute-start(bf16[96,512]{1,0:T(8,128)(2,1)S(1)} %shard_map.211.refs_2_), channel_id=1, source_target_pairs={{0,4},{1,5},{2,6},{3,7},{4,0},{5,1},{6,2},{7,3},{8,12},{9,13},{10,... | collective-permute-start | bytes 294920 | tf_op jit(solution)/shard_map/ppermute | solution.py:33
  31.4 8.6 %collective-permute-start.10 = (bf16[96,512]{1,0:T(8,128)(2,1)S(1)}, bf16[96,512]{1,0:T(8,128)(2,1)S(1)}, u32[]{:S(2)}, u32[]{:S(2)}) collective-permute-start(bf16[96,512]{1,0:T(8,128)(2,1)S(1)} %shard_map.211.refs_2_), channel_id=1, source_target_pairs={{0,2},{1,3},{2,0},{3,1},{4,6},{5,7},{6,4},{7,5},{8,10},{9,11},{10,... | collective-permute-start | bytes 294920 | tf_op jit(solution)/shard_map/ppermute | solution.py:33
  32.2 15.5 %copy-start.1 = (bf16[1024,352]{0,1:T(8,128)(2,1)S(1)}, bf16[1024,352]{0,1:T(8,128)(2,1)}, u32[]{:S(2)}) copy-start(bf16[1024,352]{0,1:T(8,128)(2,1)} %param.36) | copy-start | bytes 2162692
  32.2 15.5 %copy-start.2 = (bf16[1024,352]{0,1:T(8,128)(2,1)S(1)}, bf16[1024,352]{0,1:T(8,128)(2,1)}, u32[]{:S(2)}) copy-start(bf16[1024,352]{0,1:T(8,128)(2,1)} %param.37) | copy-start | bytes 2162692
  32.2 15.5 %copy-start.4 = (f32[4096]{0:T(1024)S(1)}, f32[4096]{0:T(1024)}, u32[]{:S(2)}) copy-start(f32[4096]{0:T(1024)} %param.30) | copy-start | bytes 49156
  40.1 6.7 %collective-permute-start.15 = (bf16[96,512]{1,0:T(8,128)(2,1)S(1)}, bf16[96,512]{1,0:T(8,128)(2,1)S(1)}, u32[]{:S(2)}, u32[]{:S(2)}) collective-permute-start(bf16[96,512]{1,0:T(8,128)(2,1)S(1)} %shard_map.213.refs_0_.mine), channel_id=1, source_target_pairs={{0,24},{8,16},{16,8},{24,0},{1,25},{9,17},{17,9},{25,1},{2,26},{10... | collective-permute-start | bytes 294920 | tf_op jit(solution)/shard_map/ppermute | solution.py:33
  41.7 5.4 %collective-permute-start.14 = (bf16[96,512]{1,0:T(8,128)(2,1)S(1)}, bf16[96,512]{1,0:T(8,128)(2,1)S(1)}, u32[]{:S(2)}, u32[]{:S(2)}) collective-permute-start(bf16[96,512]{1,0:T(8,128)(2,1)S(1)} %shard_map.213.refs_0_.mine), channel_id=1, source_target_pairs={{0,16},{8,24},{16,0},{24,8},{1,17},{9,25},{17,1},{25,9},{2,18},{10... | collective-permute-start | bytes 294920 | tf_op jit(solution)/shard_map/ppermute | solution.py:33
  42.6 4.6 %collective-permute-start.13 = (bf16[96,512]{1,0:T(8,128)(2,1)S(1)}, bf16[96,512]{1,0:T(8,128)(2,1)S(1)}, u32[]{:S(2)}, u32[]{:S(2)}) collective-permute-start(bf16[96,512]{1,0:T(8,128)(2,1)S(1)} %shard_map.213.refs_0_.mine), channel_id=1, source_target_pairs={{0,8},{8,0},{16,24},{24,16},{1,9},{9,1},{17,25},{25,17},{2,10},{10... | collective-permute-start | bytes 294920 | tf_op jit(solution)/shard_map/ppermute | solution.py:33
  43.6 4.0 %collective-permute-start.16 = (bf16[96,512]{1,0:T(8,128)(2,1)S(1)}, bf16[96,512]{1,0:T(8,128)(2,1)S(1)}, u32[]{:S(2)}, u32[]{:S(2)}) collective-permute-start(bf16[96,512]{1,0:T(8,128)(2,1)S(1)} %shard_map.213.refs_0_.mine), channel_id=1, source_target_pairs={{0,1},{1,0},{2,3},{3,2},{4,5},{5,4},{6,7},{7,6},{8,9},{9,8},{10,11... | collective-permute-start | bytes 294920 | tf_op jit(solution)/shard_map/ppermute | solution.py:33
  46.7 4.1 %collective-permute-start.19 = (bf16[96,512]{1,0:T(8,128)(2,1)S(1)}, bf16[96,512]{1,0:T(8,128)(2,1)S(1)}, u32[]{:S(2)}, u32[]{:S(2)}) collective-permute-start(bf16[96,512]{1,0:T(8,128)(2,1)S(1)} %collective-permute-done.15.refs_3_), channel_id=1, source_target_pairs={{0,1},{1,0},{2,3},{3,2},{4,5},{5,4},{6,7},{7,6},{8,9},{9,8},{10,11... | collective-permute-start | bytes 294920 | tf_op jit(solution)/shard_map/ppermute | solution.py:33
  47.2 4.7 %collective-permute-start.18 = (bf16[96,512]{1,0:T(8,128)(2,1)S(1)}, bf16[96,512]{1,0:T(8,128)(2,1)S(1)}, u32[]{:S(2)}, u32[]{:S(2)}) collective-permute-start(bf16[96,512]{1,0:T(8,128)(2,1)S(1)} %collective-permute-done.14.refs_2_), channel_id=1, source_target_pairs={{0,1},{1,0},{2,3},{3,2},{4,5},{5,4},{6,7},{7,6},{8,9},{9,8},{10,11... | collective-permute-start | bytes 294920 | tf_op jit(solution)/shard_map/ppermute | solution.py:33
  47.3 4.6 %collective-permute-start.17 = (bf16[96,512]{1,0:T(8,128)(2,1)S(1)}, bf16[96,512]{1,0:T(8,128)(2,1)S(1)}, u32[]{:S(2)}, u32[]{:S(2)}) collective-permute-start(bf16[96,512]{1,0:T(8,128)(2,1)S(1)} %collective-permute-done.13.refs_1_), channel_id=1, source_target_pairs={{0,1},{1,0},{2,3},{3,2},{4,5},{5,4},{6,7},{7,6},{8,9},{9,8},{10,11... | collective-permute-start | bytes 294920 | tf_op jit(solution)/shard_map/ppermute | solution.py:33
  48.3 7.7 %collective-permute-start.22 = (bf16[96,768]{1,0:T(8,128)(2,1)S(1)}, bf16[96,768]{1,0:T(8,128)(2,1)S(1)}, u32[]{:S(2)}, u32[]{:S(2)}) collective-permute-start(bf16[96,768]{1,0:T(8,128)(2,1)S(1)} %get-tuple-element.77), channel_id=1, source_target_pairs={{0,24},{8,16},{16,8},{24,0},{1,25},{9,17},{17,9},{25,1},{2,26},{10... | collective-permute-start | bytes 442376 | tf_op jit(solution)/shard_map/ppermute | solution.py:33
  49.9 8.3 %collective-permute-start.21 = (bf16[96,768]{1,0:T(8,128)(2,1)S(1)}, bf16[96,768]{1,0:T(8,128)(2,1)S(1)}, u32[]{:S(2)}, u32[]{:S(2)}) collective-permute-start(bf16[96,768]{1,0:T(8,128)(2,1)S(1)} %get-tuple-element.77), channel_id=1, source_target_pairs={{0,16},{8,24},{16,0},{24,8},{1,17},{9,25},{17,1},{25,9},{2,18},{10... | collective-permute-start | bytes 442376 | tf_op jit(solution)/shard_map/ppermute | solution.py:33
  50.8 7.4 %collective-permute-start.20 = (bf16[96,768]{1,0:T(8,128)(2,1)S(1)}, bf16[96,768]{1,0:T(8,128)(2,1)S(1)}, u32[]{:S(2)}, u32[]{:S(2)}) collective-permute-start(bf16[96,768]{1,0:T(8,128)(2,1)S(1)} %get-tuple-element.77), channel_id=1, source_target_pairs={{0,8},{8,0},{16,24},{24,16},{1,9},{9,1},{17,25},{25,17},{2,10},{10... | collective-permute-start | bytes 442376 | tf_op jit(solution)/shard_map/ppermute | solution.py:33
  51.8 6.4 %copy-start = (bf16[352,1024]{1,0:T(8,128)(2,1)S(1)}, bf16[352,1024]{1,0:T(8,128)(2,1)}, u32[]{:S(2)}) copy-start(bf16[352,1024]{1,0:T(8,128)(2,1)} %refs_2_.3) | copy-start | bytes 2162692
  59.2 1.8 %collective-permute-start.23 = (bf16[96,2048]{1,0:T(8,128)(2,1)S(1)}, bf16[96,2048]{1,0:T(8,128)(2,1)S(1)}, u32[]{:S(2)}, u32[]{:S(2)}) collective-permute-start(bf16[96,2048]{1,0:T(8,128)(2,1)S(1)} %get-tuple-element.81), channel_id=1, source_target_pairs={{0,1},{1,0},{2,3},{3,2},{4,5},{5,4},{6,7},{7,6},{8,9},{9,8},{10,11... | collective-permute-start | bytes 1179656 | tf_op jit(solution)/shard_map/ppermute | solution.py:33
  61.0 5.1 %collective-permute-start.24 = (bf16[24,2048]{1,0:T(8,128)(2,1)S(1)}, bf16[24,2048]{1,0:T(8,128)(2,1)S(1)}, u32[]{:S(2)}, u32[]{:S(2)}) collective-permute-start(bf16[24,2048]{1,0:T(8,128)(2,1)S(1)} %get-tuple-element.83), channel_id=1, source_target_pairs={{0,8},{8,0},{16,24},{24,16},{1,9},{9,1},{17,25},{25,17},{2,10},{10... | collective-permute-start | bytes 294920 | tf_op jit(solution)/shard_map/ppermute | solution.py:33
  62.1 6.7 %collective-permute-start.25 = (bf16[24,2048]{1,0:T(8,128)(2,1)S(1)}, bf16[24,2048]{1,0:T(8,128)(2,1)S(1)}, u32[]{:S(2)}, u32[]{:S(2)}) collective-permute-start(bf16[24,2048]{1,0:T(8,128)(2,1)S(1)} %get-tuple-element.84), channel_id=1, source_target_pairs={{0,16},{8,24},{16,0},{24,8},{1,17},{9,25},{17,1},{25,9},{2,18},{10... | collective-permute-start | bytes 294920 | tf_op jit(solution)/shard_map/ppermute | solution.py:33
  63.2 5.6 %collective-permute-start.26 = (bf16[24,2048]{1,0:T(8,128)(2,1)S(1)}, bf16[24,2048]{1,0:T(8,128)(2,1)S(1)}, u32[]{:S(2)}, u32[]{:S(2)}) collective-permute-start(bf16[24,2048]{1,0:T(8,128)(2,1)S(1)} %get-tuple-element.85), channel_id=1, source_target_pairs={{0,24},{8,16},{16,8},{24,0},{1,25},{9,17},{17,9},{25,1},{2,26},{10... | collective-permute-start | bytes 294920 | tf_op jit(solution)/shard_map/ppermute | solution.py:33
  68.9 4.5 %collective-permute-start.27 = (bf16[24,512]{1,0:T(8,128)(2,1)S(1)}, bf16[24,512]{1,0:T(8,128)(2,1)S(1)}, u32[]{:S(2)}, u32[]{:S(2)}) collective-permute-start(bf16[24,512]{1,0:T(8,128)(2,1)S(1)} %get-tuple-element.88), channel_id=1, source_target_pairs={{0,2},{1,3},{2,0},{3,1},{4,6},{5,7},{6,4},{7,5},{8,10},{9,11},{10,... | collective-permute-start | bytes 73736 | tf_op jit(solution)/shard_map/ppermute | solution.py:33
  69.5 4.7 %collective-permute-start.28 = (bf16[24,512]{1,0:T(8,128)(2,1)S(1)}, bf16[24,512]{1,0:T(8,128)(2,1)S(1)}, u32[]{:S(2)}, u32[]{:S(2)}) collective-permute-start(bf16[24,512]{1,0:T(8,128)(2,1)S(1)} %get-tuple-element.89), channel_id=1, source_target_pairs={{0,4},{1,5},{2,6},{3,7},{4,0},{5,1},{6,2},{7,3},{8,12},{9,13},{10,... | collective-permute-start | bytes 73736 | tf_op jit(solution)/shard_map/ppermute | solution.py:33
  72.0 5.6 %collective-permute-start.29 = (bf16[24,512]{1,0:T(8,128)(2,1)S(1)}, bf16[24,512]{1,0:T(8,128)(2,1)S(1)}, u32[]{:S(2)}, u32[]{:S(2)}) collective-permute-start(bf16[24,512]{1,0:T(8,128)(2,1)S(1)} %get-tuple-element.90), channel_id=1, source_target_pairs={{0,6},{1,7},{2,4},{3,5},{4,2},{5,3},{6,0},{7,1},{8,14},{9,15},{10,... | collective-permute-start | bytes 73736 | tf_op jit(solution)/shard_map/ppermute | solution.py:33
where the time goes:
time: 78.6 us; the launch traced here: 78.3 us
  starting transfers between devices  31.9 us (41%)
  Pallas kernels  22.8 us (29%)
  waiting for transfers between devices  21.9 us (28%)
  between operations  0.91 us (1%)
    ppermute x30, starting transfers between devices, swap(): return lax.ppermute(value, axis, [(s, s ^ step) for s in range(size)])  31.9 us
    ppermute x30, waiting for transfers between devices, swap(): return lax.ppermute(value, axis, [(s, s ^ step) for s in range(size)])  21.9 us
    pallas_call x17, Pallas kernels, call(): pl.pallas_call(body, out_shape=[jax.ShapeDtypeStruct(s, d) for s, d in ou...  20.1 us
    pallas_call x1, Pallas kernels, body(): pl.pallas_call(functools.partial(update_kernel, group), out_shape=[jax.Sh...  2.71 us
  transfers between devices with their start and end apart: 30, of which 12 were waited for; matrix products, arithmetic and copies ran while one was open for 1% of the time, Pallas kernels for 23%

commit v1 on v0

--- a/solution.py
+++ b/solution.py
@@ -39,6 +39,11 @@
 
 def lane_slice(index, size):
     return pl.ds(pl.multiple_of(index * size, LANES), size)
+
+
+def half_index():
+    t = lax.axis_index("tp")
+    return lax.rem(t + lax.div(t, 2) + lax.axis_index("ep"), 2)
 
 
 def call(body, outs, ins, args, scratch=(), flops=0, limit=24):
@@ -201,7 +206,7 @@
 
 def output_kernel(n_ep, *refs):
     mixed, weight, give, keep = refs[:n_ep], refs[n_ep], refs[-2], refs[-1]
-    c = lax.rem(lax.axis_index("tp"), 2)
+    c = half_index()
     half = keep.shape[1]
     rows = jnp.concatenate([m[...].astype(F32) for m in mixed], axis=0).astype(BF16)
     rows = rows[:, : weight.shape[0]]
@@ -216,7 +221,7 @@
 def hidden_kernel(n_ep, *refs):
     payloads, keep, core, others = refs[:n_ep], refs[n_ep], refs[n_ep + 1], refs[n_ep + 2 : -2]
     out = refs[-1]
-    c = lax.rem(lax.axis_index("tp"), 2)
+    c = half_index()
     half = keep.shape[1]
     total = jnp.concatenate([p[:, lane_slice(c, half)].astype(F32) for p in payloads], axis=0)
     mixed = keep[...] + core[...].astype(F32)
@@ -226,7 +231,7 @@
 
 
 def shared_kernel(mine, other, gain, gate_t, up_t, own, sent):
-    c = lax.rem(lax.axis_index("tp"), 2)
+    c = half_index()
     e = lax.axis_index("ep")
     half = mine.shape[1]
     inner, padded = gate_t.shape[0], own.shape[1] // 2
@@ -247,15 +252,17 @@
     pieces, others, payloads = refs[:n_ep], refs[n_ep : 2 * n_ep], refs[2 * n_ep : 3 * n_ep]
     gain, router, gate_w, up_w, down = refs[3 * n_ep : 3 * n_ep + 5]
     inner, scales, own_hidden, down_out, x_ref, n_ref, sems = refs[3 * n_ep + 5 :]
-    local = inner.shape[0]
+    local, inner_width = gate_w.shape[:2]
+    spans = [slice(i * inner_width, (i + 1) * inner_width) for i in range(local)]
     fetches = [
-        pltpu.make_async_copy(down.at[i], down_out.at[i], sems.at[i]) for i in range(local)
+        pltpu.make_async_copy(down.at[i], down_out.at[spans[i]], sems.at[i])
+        for i in range(local)
     ]
     for copy in fetches:
         copy.start()
     e = lax.axis_index("ep")
     t = lax.axis_index("tp")
-    c = lax.rem(t, 2)
+    c = half_index()
     rows, half = pieces[0].shape
     batch = rows // n_ep
     squares = jnp.zeros((rows, half), F32)
@@ -285,7 +292,7 @@
         combine = jnp.sum(jnp.where(lane == e * local + i, weights, 0.0), axis=1, keepdims=True)
         gate = dot_t(n_ref[...], gate_w[i])
         up = dot_t(n_ref[...], up_w[i])
-        inner[i] = (silu(gate) * up * combine).astype(BF16)
+        inner[:, spans[i]] = (silu(gate) * up * combine).astype(BF16)
     for copy in fetches:
         copy.wait()
 
@@ -315,14 +322,11 @@
     e = lax.axis_index("ep")
     c = lax.rem(lax.axis_index("tp"), 2)
     h = c if mine else 1 - c
-    size = weight.shape[2] // (2 * n_z)
-    local = inner.shape[0]
+    size = weight.shape[1] // (2 * n_z)
     ratio = shared_down.shape[1] // size
     for z in range(n_z):
         lanes = lane_slice(2 * z + h, size)
-        part = dot(inner[0], weight[0, :, lanes])
-        for i in range(1, local):
-            part = part + dot(inner[i], weight[i, :, lanes])
+        part = dot(inner[...], weight[:, lanes])
         out[:, z * size : (z + 1) * size] = part.astype(out.dtype)
     for z in range(n_z):
         q = 2 * z + h
@@ -369,8 +373,14 @@
     def ep_swap(value, k):
         return swap(value, "ep", n_ep, k)
 
-    def z_swap(value, m):
-        return swap(value, "tp", n_tp, 2 * m)
+    def cross_swap(value, k, flip):
+        pairs = [
+            (e * n_tp + t, (e ^ k) * n_tp + (t ^ flip)) for e in range(n_ep) for t in range(n_tp)
+        ]
+        return lax.ppermute(value, ("ep", "tp"), pairs)
+
+    def z_swap(value, m, flip=0):
+        return swap(value, "tp", n_tp, 2 * m | flip)
 
     def core_swap(value):
         return swap(value, "tp", n_tp, 1)
@@ -400,7 +410,7 @@
             [pltpu.SemaphoreType.DMA((n_ep,))],
         )
         own_payload = payloads[0]
-        payloads = [own_payload] + [ep_swap(payloads[k], k) for k in others]
+        payloads = [own_payload] + [cross_swap(payloads[k], k, 1) for k in others]
 
         (*weights, gain), token = fetch(
             (w_query, w_forget, w_input, w_outgate, norm_gain[None]), own_payload
@@ -458,7 +468,7 @@
         )
         core = core_swap(give)
         (summed,) = call(add_kernel, [((rows, half), BF16)], [VMEM] * 2, (keep, core))
-        along = [z_swap(summed, m) for m in range(1, n_z)]
+        along = [z_swap(summed, m, m & 1) for m in range(1, n_z)]
         (gate_w, up_w), token = fetch(
             (jnp.swapaxes(expert_gate, 1, 2), jnp.swapaxes(expert_up, 1, 2)), summed
         )
@@ -469,7 +479,7 @@
             (*payloads, keep, core, *along, token),
         )
 
-        pieces = [part] + [ep_swap(part, k) for k in others]
+        pieces = [part] + [cross_swap(part, k, k & 1) for k in others]
         sibling = core_swap(part)
         padded = -(-shared_width // LANES) * LANES
         shared_own, shared_sent = call(
@@ -488,10 +498,10 @@
         inner, scales, own_hidden, down_w = call(
             functools.partial(expert_kernel, n_ep),
             [
-                ((local, rows, inner_width), BF16),
+                ((rows, local * inner_width), BF16),
                 ((rows, LANES), F32),
                 ((batch, slice_width), F32),
-                (expert_down.shape, BF16),
+                ((local * inner_width, width), BF16),
             ],
             [VMEM] * (3 * n_ep + 4) + [HBM],
             (

time: 78.6 us -> 79.4 us (1.010)
  waiting for transfers between devices: 21.9 us -> 24.2 us
  starting transfers between devices: 31.9 us -> 30.6 us
    ppermute x30 -> x24, starting transfers between devices: 31.9 us -> 23.3 us  [swap(): return lax.ppermute(value, axis, [(s, s ^ step) for s in range(size)])]
    ppermute x0 -> x6, starting transfers between devices: none -> 7.29 us  [cross_swap(): return lax.ppermute(value, ('ep', 'tp'), pairs)]
    ppermute x0 -> x6, waiting for transfers between devices: none -> 7.28 us  [cross_swap(): return lax.ppermute(value, ('ep', 'tp'), pairs)]
    ppermute x30 -> x24, waiting for transfers between devices: 21.9 us -> 16.9 us  [swap(): return lax.ppermute(value, axis, [(s, s ^ step) for s in range(size)])]
where the time goes in v1:
time: 79.4 us; the launch traced here: 79.1 us
  starting transfers between devices  30.6 us (39%)
  waiting for transfers between devices  24.2 us (30%)
  Pallas kernels  22.7 us (29%)
  between operations  0.91 us (1%)
    ppermute x24, starting transfers between devices, swap(): return lax.ppermute(value, axis, [(s, s ^ step) for s in range(size)])  23.3 us
    pallas_call x17, Pallas kernels, call(): pl.pallas_call(body, out_shape=[jax.ShapeDtypeStruct(s, d) for s, d in ou...  20 us
    ppermute x24, waiting for transfers between devices, swap(): return lax.ppermute(value, axis, [(s, s ^ step) for s in range(size)])  16.9 us
    ppermute x6, starting transfers between devices, cross_swap(): return lax.ppermute(value, ('ep', 'tp'), pairs)  7.29 us
    ppermute x6, waiting for transfers between devices, cross_swap(): return lax.ppermute(value, ('ep', 'tp'), pairs)  7.28 us
    pallas_call x1, Pallas kernels, body(): pl.pallas_call(functools.partial(update_kernel, group), out_shape=[jax.Sh...  2.71 us
  transfers between devices with their start and end apart: 30, of which 12 were waited for; matrix products, arithmetic and copies ran while one was open for 1% of the time, Pallas kernels for 23%

profile of v1, /device:TPU:0, one launch (start us, length us, event | category | flops | bytes accessed | tf_op | source)
XLA Modules:
  0.0 79.1 jit_solution(9621307853773894668)
XLA Ops:
  0.7 0.9 %shard_map.203 = (bf16[24,1024]{1,0:T(8,128)(2,1)S(1)}, bf16[24,1024]{1,0:T(8,128)(2,1)S(1)}, bf16[24,1024]{1,0:T(8,128)(2,1)S(1)}, bf16[24,1024]{1,0:T(8,128)(2,1)S(1)}) custom-call(bf16[24,4096]{1,0:T(8,128)(2,1)} %refs_1_.3), custom_call_target="tpu_custom_call" | custom-call | tf_op jit(solution)/shard_map/pallas_call | solution.py:50
  1.6 2.5 %collective-permute-start = (bf16[24,1024]{1,0:T(8,128)(2,1)S(1)}, bf16[24,1024]{1,0:T(8,128)(2,1)S(1)}, u32[]{:S(2)}, u32[]{:S(2)}) collective-permute-start(bf16[24,1024]{1,0:T(8,128)(2,1)S(1)} %get-tuple-element.48), channel_id=1, source_target_pairs={{0,9},{1,8},{2,11},{3,10},{4,13},{5,12},{6,15},{7,14},{8,1},{9,0},... | collective-permute-start | bytes 147464 | tf_op jit(solution)/shard_map/ppermute | solution.py:380
  4.1 1.8 %collective-permute-start.1 = (bf16[24,1024]{1,0:T(8,128)(2,1)S(1)}, bf16[24,1024]{1,0:T(8,128)(2,1)S(1)}, u32[]{:S(2)}, u32[]{:S(2)}) collective-permute-start(bf16[24,1024]{1,0:T(8,128)(2,1)S(1)} %get-tuple-element.49), channel_id=1, source_target_pairs={{0,17},{1,16},{2,19},{3,18},{4,21},{5,20},{6,23},{7,22},{8,25},{9,... | collective-permute-start | bytes 147464 | tf_op jit(solution)/shard_map/ppermute | solution.py:380
  5.9 2.7 %shard_map.204 = (bf16[1024,256]{1,0:T(8,128)(2,1)S(1)}, bf16[1024,256]{1,0:T(8,128)(2,1)S(1)}, bf16[1024,256]{1,0:T(8,128)(2,1)S(1)}, bf16[1024,256]{1,0:T(8,12...) custom-call(bf16[1024,256]{1,0:T(8,128)(2,1)} %refs_0_.2, bf16[1024,256]{1,0:T(8,128)(2,1)} %refs_1_.2, ...), custom_call_target="tpu_custom_call" | custom-call | flops 67108864 | tf_op jit(solution)/shard_map/pallas_call | solution.py:50
  8.6 2.2 %collective-permute-done.2.refs_3_ = bf16[24,1024]{1,0:T(8,128)(2,1)S(1)} collective-permute-done((bf16[24,1024]{1,0:T(8,128)(2,1)S(1)}, bf16[24,1024]{1,0:T(8,128)(2,1)S(1)}, u32[]{:S(2)}, u32[]{:S(2)}) %collective-permute-start.2) | collective-permute-done | bytes 49184 | tf_op jit(solution)/shard_map/ppermute | solution.py:380
  10.8 0.5 shard_map.205
  11.3 0.5 collective-permute-start.3
  11.8 0.3 collective-permute-start.4
  12.1 2.8 %collective-permute-start.5 = (bf16[24,1024]{1,0:T(8,128)(2,1)S(1)}, bf16[24,1024]{1,0:T(8,128)(2,1)S(1)}, u32[]{:S(2)}, u32[]{:S(2)}) collective-permute-start(bf16[24,1024]{1,0:T(8,128)(2,1)S(1)} %get-tuple-element.60), channel_id=1, source_target_pairs={{0,24},{8,16},{16,8},{24,0},{1,25},{9,17},{17,9},{25,1},{2,26},{10... | collective-permute-start | bytes 147464 | tf_op jit(solution)/shard_map/ppermute | solution.py:33
  14.8 0.7 broadcast_in_dim.17.branch
  15.5 2.5 %shard_map.206 = (f32[24,2,128,128]{3,2,1,0:T(8,128)S(1)}, bf16[24,4096]{1,0:T(8,128)(2,1)S(1)}, bf16[8,4096]{1,0:T(8,128)(2,1)S(1)}, f32[8,128]{1,0:T(8,128)S(1)}) custom-call(f32[24,2,128,128]{3,2,1,0:T(8,128)} %refs_0_.3, bf16[24,4096]{1,0:T(8,128)(2,1)} %refs_1_.3, bf16[8,4096]{1,0:T(8,128)(2,1)} %bitcast.19, ...), custom_call_target="tpu_custom_call" | custom-call | flops 67108864 | tf_op jit(solution)/shard_map/pallas_call | solution.py:50
  18.2 1.2 %shard_map.208 = (bf16[24,384]{1,0:T(8,128)(2,1)S(1)}, f32[24,768]{1,0:T(8,128)S(1)}) custom-call(f32[24,1024]{1,0:T(8,128)S(1)} %get-tuple-element.57.refs_3_.refs_0_, bf16[24,1024]{1,0:T(8,128)(2,1)S(1)} %collective-permute-done.3.refs_1_, bf16[24,1024]{1,0:T(8,128)(2,1)S(1)} %collective-permute-done.4.refs_2_, ...), custom_call_target="tpu_custom_call" | custom-call | flops 16777216 | tf_op jit(solution)/shard_map/pallas_call | solution.py:50
  19.5 1.6 %collective-permute-start.8 = (bf16[24,384]{1,0:T(8,128)(2,1)S(1)}, bf16[24,384]{1,0:T(8,128)(2,1)S(1)}, u32[]{:S(2)}, u32[]{:S(2)}) collective-permute-start(bf16[24,384]{1,0:T(8,128)(2,1)S(1)} %get-tuple-element.66.refs_0_.refs_8_), channel_id=1, source_target_pairs={{0,24},{8,16},{16,8},{24,0},{1,25},{9,17},{17,9},{25,1},{2,26},{10... | collective-permute-start | bytes 55304 | tf_op jit(solution)/shard_map/ppermute | solution.py:33
  21.1 0.5 collective-permute-start.7
  21.6 1.5 %collective-permute-start.6 = (bf16[24,384]{1,0:T(8,128)(2,1)S(1)}, bf16[24,384]{1,0:T(8,128)(2,1)S(1)}, u32[]{:S(2)}, u32[]{:S(2)}) collective-permute-start(bf16[24,384]{1,0:T(8,128)(2,1)S(1)} %get-tuple-element.66.refs_0_.refs_8_), channel_id=1, source_target_pairs={{0,8},{8,0},{16,24},{24,16},{1,9},{9,1},{17,25},{25,17},{2,10},{10... | collective-permute-start | bytes 55304 | tf_op jit(solution)/shard_map/ppermute | solution.py:33
  23.0 2.7 %shard_map.209 = (f32[24,2,128,128]{3,2,1,0:T(8,128)}, f32[8,128]{1,0:T(8,128)S(1)}) custom-call(f32[24,768]{1,0:T(8,128)S(1)} %get-tuple-element.67.gates, f32[24,2,128,128]{3,2,1,0:T(8,128)S(1)} %get-tuple-element.64.refs_7_.state), custom_call_target="tpu_custom_call" | custom-call | flops 67108864 | tf_op jit(solution)/shard_map/pallas_call | solution.py:446
  26.1 1.3 %collective-permute-done.9.got.refs_5_ = bf16[96,512]{1,0:T(8,128)(2,1)S(1)} collective-permute-done((bf16[96,512]{1,0:T(8,128)(2,1)S(1)}, bf16[96,512]{1,0:T(8,128)(2,1)S(1)}, u32[]{:S(2)}, u32[]{:S(2)}) %collective-permute-start.9) | collective-permute-done | bytes 98336 | tf_op jit(solution)/shard_map/ppermute | solution.py:33
  27.4 3.4 %collective-permute-start.12 = (bf16[96,512]{1,0:T(8,128)(2,1)S(1)}, bf16[96,512]{1,0:T(8,128)(2,1)S(1)}, u32[]{:S(2)}, u32[]{:S(2)}) collective-permute-start(bf16[96,512]{1,0:T(8,128)(2,1)S(1)} %shard_map.211.refs_2_), channel_id=1, source_target_pairs={{0,7},{1,6},{2,5},{3,4},{4,3},{5,2},{6,1},{7,0},{8,15},{9,14},{10,... | collective-permute-start | bytes 294920 | tf_op jit(solution)/shard_map/ppermute | solution.py:33
  30.8 0.5 collective-permute-start.10
  31.3 4.9 %shard_map.212 = (bf16[2,352,4096]{2,1,0:T(8,128)(2,1)S(1)}, bf16[2,352,4096]{2,1,0:T(8,128)(2,1)S(1)}, f32[8,128]{1,0:T(8,128)S(1)}) custom-call(bf16[2,352,4096]{2,1,0:T(8,128)(2,1)} %bitcast.17, bf16[2,352,4096]{2,1,0:T(8,128)(2,1)} %bitcast.18, bf16[96,512]{1,0:T(8,128)(2,1)S(1)} %shard_map.211.refs_2_), custom_call_target="tpu_custom_call" | custom-call | flops 67108864 | tf_op jit(solution)/shard_map/pallas_call | solution.py:50
  36.2 3.7 %collective-permute-done.11.refs_7_ = bf16[96,512]{1,0:T(8,128)(2,1)S(1)} collective-permute-done((bf16[96,512]{1,0:T(8,128)(2,1)S(1)}, bf16[96,512]{1,0:T(8,128)(2,1)S(1)}, u32[]{:S(2)}, u32[]{:S(2)}) %collective-permute-start.11) | collective-permute-done | bytes 98336 | tf_op jit(solution)/shard_map/ppermute | solution.py:33
  40.0 1.0 %collective-permute-start.15 = (bf16[96,512]{1,0:T(8,128)(2,1)S(1)}, bf16[96,512]{1,0:T(8,128)(2,1)S(1)}, u32[]{:S(2)}, u32[]{:S(2)}) collective-permute-start(bf16[96,512]{1,0:T(8,128)(2,1)S(1)} %shard_map.213.refs_0_.mine), channel_id=1, source_target_pairs={{0,25},{1,24},{2,27},{3,26},{4,29},{5,28},{6,31},{7,30},{8,17},{9,... | collective-permute-start | bytes 294920 | tf_op jit(solution)/shard_map/ppermute | solution.py:380
  41.0 0.9 %collective-permute-start.14 = (bf16[96,512]{1,0:T(8,128)(2,1)S(1)}, bf16[96,512]{1,0:T(8,128)(2,1)S(1)}, u32[]{:S(2)}, u32[]{:S(2)}) collective-permute-start(bf16[96,512]{1,0:T(8,128)(2,1)S(1)} %shard_map.213.refs_0_.mine), channel_id=1, source_target_pairs={{0,16},{1,17},{2,18},{3,19},{4,20},{5,21},{6,22},{7,23},{8,24},{9,... | collective-permute-start | bytes 294920 | tf_op jit(solution)/shard_map/ppermute | solution.py:380
  41.9 1.1 %collective-permute-start.13 = (bf16[96,512]{1,0:T(8,128)(2,1)S(1)}, bf16[96,512]{1,0:T(8,128)(2,1)S(1)}, u32[]{:S(2)}, u32[]{:S(2)}) collective-permute-start(bf16[96,512]{1,0:T(8,128)(2,1)S(1)} %shard_map.213.refs_0_.mine), channel_id=1, source_target_pairs={{0,9},{1,8},{2,11},{3,10},{4,13},{5,12},{6,15},{7,14},{8,1},{9,0},... | collective-permute-start | bytes 294920 | tf_op jit(solution)/shard_map/ppermute | solution.py:380
  43.0 3.1 %collective-permute-done.15.refs_3_ = bf16[96,512]{1,0:T(8,128)(2,1)S(1)} collective-permute-done((bf16[96,512]{1,0:T(8,128)(2,1)S(1)}, bf16[96,512]{1,0:T(8,128)(2,1)S(1)}, u32[]{:S(2)}, u32[]{:S(2)}) %collective-permute-start.15) | collective-permute-done | bytes 98336 | tf_op jit(solution)/shard_map/ppermute | solution.py:380
  46.1 2.0 %collective-permute-done.14.refs_2_ = bf16[96,512]{1,0:T(8,128)(2,1)S(1)} collective-permute-done((bf16[96,512]{1,0:T(8,128)(2,1)S(1)}, bf16[96,512]{1,0:T(8,128)(2,1)S(1)}, u32[]{:S(2)}, u32[]{:S(2)}) %collective-permute-start.14) | collective-permute-done | bytes 98336 | tf_op jit(solution)/shard_map/ppermute | solution.py:380
  48.2 0.4 collective-permute-start.17
  48.7 0.6 shard_map.215
  49.2 1.6 %collective-permute-start.22 = (bf16[96,768]{1,0:T(8,128)(2,1)S(1)}, bf16[96,768]{1,0:T(8,128)(2,1)S(1)}, u32[]{:S(2)}, u32[]{:S(2)}) collective-permute-start(bf16[96,768]{1,0:T(8,128)(2,1)S(1)} %get-tuple-element.77), channel_id=1, source_target_pairs={{0,24},{8,16},{16,8},{24,0},{1,25},{9,17},{17,9},{25,1},{2,26},{10... | collective-permute-start | bytes 442376 | tf_op jit(solution)/shard_map/ppermute | solution.py:33
  50.9 0.9 %collective-permute-start.21 = (bf16[96,768]{1,0:T(8,128)(2,1)S(1)}, bf16[96,768]{1,0:T(8,128)(2,1)S(1)}, u32[]{:S(2)}, u32[]{:S(2)}) collective-permute-start(bf16[96,768]{1,0:T(8,128)(2,1)S(1)} %get-tuple-element.77), channel_id=1, source_target_pairs={{0,16},{8,24},{16,0},{24,8},{1,17},{9,25},{17,1},{25,9},{2,18},{10... | collective-permute-start | bytes 442376 | tf_op jit(solution)/shard_map/ppermute | solution.py:33
  51.7 1.0 %collective-permute-start.20 = (bf16[96,768]{1,0:T(8,128)(2,1)S(1)}, bf16[96,768]{1,0:T(8,128)(2,1)S(1)}, u32[]{:S(2)}, u32[]{:S(2)}) collective-permute-start(bf16[96,768]{1,0:T(8,128)(2,1)S(1)} %get-tuple-element.77), channel_id=1, source_target_pairs={{0,8},{8,0},{16,24},{24,16},{1,9},{9,1},{17,25},{25,17},{2,10},{10... | collective-permute-start | bytes 442376 | tf_op jit(solution)/shard_map/ppermute | solution.py:33
  52.8 3.8 %shard_map.214 = (bf16[96,704]{1,0:T(8,128)(2,1)S(1)}, f32[96,128]{1,0:T(8,128)S(1)}, f32[24,512]{1,0:T(8,128)S(1)}, bf16[704,4096]{1,0:T(8,128)(2,1)S(1)}) custom-call(bf16[96,512]{1,0:T(8,128)(2,1)S(1)} %shard_map.213.refs_0_.mine, bf16[96,512]{1,0:T(8,128)(2,1)S(1)} %collective-permute-done.13.refs_1_, ...), custom_call_target="tpu_custom_call" | custom-call | flops 1107296256 | tf_op jit(solution)/shard_map/pallas_call | solution.py:50
  56.7 0.3 collective-permute-done.22.refs_3_
  57.0 2.2 %collective-permute-done.21.refs_2_ = bf16[96,768]{1,0:T(8,128)(2,1)S(1)} collective-permute-done((bf16[96,768]{1,0:T(8,128)(2,1)S(1)}, bf16[96,768]{1,0:T(8,128)(2,1)S(1)}, u32[]{:S(2)}, u32[]{:S(2)}) %collective-permute-start.21) | collective-permute-done | bytes 147488 | tf_op jit(solution)/shard_map/ppermute | solution.py:33
  59.2 0.9 %shard_map.216 = (bf16[96,2048]{1,0:T(8,128)(2,1)S(1)}, bf16[96,352]{1,0:T(8,128)(2,1)S(1)}) custom-call(bf16[96,704]{1,0:T(8,128)(2,1)S(1)} %get-tuple-element.75.inner, f32[96,768]{1,0:T(8,128)S(1)} %get-tuple-element.76.refs_0_, bf16[96,768]{1,0:T(8,128)(2,1)S(1)} %collective-permute-done.20.refs_1_, bf16[96,768]{1,0:T(8,128)(2,1)S(1)} %collective-permute-done.21.refs_2_, ...), custom_call_target="tpu_custom_call" | custom-call | flops 276824064 | tf_op jit(solution)/shard_map/pallas_call | solution.py:50
  60.2 0.8 %shard_map.217.keep = f32[96,2048]{1,0:T(8,128)S(1)} custom-call(bf16[96,704]{1,0:T(8,128)(2,1)S(1)} %get-tuple-element.75.inner, bf16[96,352]{1,0:T(8,128)(2,1)S(1)} %get-tuple-element.80.refs_0_, bf16[704,4096]{1,0:T(8,128)(2,1)S(1)} %get-tuple-element.79.refs_5_.refs_1_, bf16[352,1024]{1,0:T(8,128)(2,1)S(1)} %copy-done), custom_call_target="tpu_custom_call" | custom-call | flops 276824064 | tf_op jit(solution)/shard_map/pallas_call | solution.py:50
  61.0 0.9 %collective-permute-done.23.got = bf16[96,2048]{1,0:T(8,128)(2,1)S(1)} collective-permute-done((bf16[96,2048]{1,0:T(8,128)(2,1)S(1)}, bf16[96,2048]{1,0:T(8,128)(2,1)S(1)}, u32[]{:S(2)}, u32[]{:S(2)}) %collective-permute-start.23) | collective-permute-done | bytes 393248 | tf_op jit(solution)/shard_map/ppermute | solution.py:33
  61.9 1.1 %collective-permute-start.24 = (bf16[24,2048]{1,0:T(8,128)(2,1)S(1)}, bf16[24,2048]{1,0:T(8,128)(2,1)S(1)}, u32[]{:S(2)}, u32[]{:S(2)}) collective-permute-start(bf16[24,2048]{1,0:T(8,128)(2,1)S(1)} %get-tuple-element.83), channel_id=1, source_target_pairs={{0,8},{8,0},{16,24},{24,16},{1,9},{9,1},{17,25},{25,17},{2,10},{10... | collective-permute-start | bytes 294920 | tf_op jit(solution)/shard_map/ppermute | solution.py:33
  63.0 1.1 %collective-permute-start.25 = (bf16[24,2048]{1,0:T(8,128)(2,1)S(1)}, bf16[24,2048]{1,0:T(8,128)(2,1)S(1)}, u32[]{:S(2)}, u32[]{:S(2)}) collective-permute-start(bf16[24,2048]{1,0:T(8,128)(2,1)S(1)} %get-tuple-element.84), channel_id=1, source_target_pairs={{0,16},{8,24},{16,0},{24,8},{1,17},{9,25},{17,1},{25,9},{2,18},{10... | collective-permute-start | bytes 294920 | tf_op jit(solution)/shard_map/ppermute | solution.py:33
  64.1 1.4 %collective-permute-start.26 = (bf16[24,2048]{1,0:T(8,128)(2,1)S(1)}, bf16[24,2048]{1,0:T(8,128)(2,1)S(1)}, u32[]{:S(2)}, u32[]{:S(2)}) collective-permute-start(bf16[24,2048]{1,0:T(8,128)(2,1)S(1)} %get-tuple-element.85), channel_id=1, source_target_pairs={{0,24},{8,16},{16,8},{24,0},{1,25},{9,17},{17,9},{25,1},{2,26},{10... | collective-permute-start | bytes 294920 | tf_op jit(solution)/shard_map/ppermute | solution.py:33
  65.5 1.6 %collective-permute-done.24.refs_1_ = bf16[24,2048]{1,0:T(8,128)(2,1)S(1)} collective-permute-done((bf16[24,2048]{1,0:T(8,128)(2,1)S(1)}, bf16[24,2048]{1,0:T(8,128)(2,1)S(1)}, u32[]{:S(2)}, u32[]{:S(2)}) %collective-permute-start.24) | collective-permute-done | bytes 98336 | tf_op jit(solution)/shard_map/ppermute | solution.py:33
  67.0 2.7 %collective-permute-done.25.refs_2_ = bf16[24,2048]{1,0:T(8,128)(2,1)S(1)} collective-permute-done((bf16[24,2048]{1,0:T(8,128)(2,1)S(1)}, bf16[24,2048]{1,0:T(8,128)(2,1)S(1)}, u32[]{:S(2)}, u32[]{:S(2)}) %collective-permute-start.25) | collective-permute-done | bytes 98336 | tf_op jit(solution)/shard_map/ppermute | solution.py:33
  69.8 0.3 collective-permute-start.27
  70.1 2.8 %collective-permute-start.28 = (bf16[24,512]{1,0:T(8,128)(2,1)S(1)}, bf16[24,512]{1,0:T(8,128)(2,1)S(1)}, u32[]{:S(2)}, u32[]{:S(2)}) collective-permute-start(bf16[24,512]{1,0:T(8,128)(2,1)S(1)} %get-tuple-element.89), channel_id=1, source_target_pairs={{0,4},{1,5},{2,6},{3,7},{4,0},{5,1},{6,2},{7,3},{8,12},{9,13},{10,... | collective-permute-start | bytes 73736 | tf_op jit(solution)/shard_map/ppermute | solution.py:33
  72.9 1.3 %collective-permute-start.29 = (bf16[24,512]{1,0:T(8,128)(2,1)S(1)}, bf16[24,512]{1,0:T(8,128)(2,1)S(1)}, u32[]{:S(2)}, u32[]{:S(2)}) collective-permute-start(bf16[24,512]{1,0:T(8,128)(2,1)S(1)} %get-tuple-element.90), channel_id=1, source_target_pairs={{0,6},{1,7},{2,4},{3,5},{4,2},{5,3},{6,0},{7,1},{8,14},{9,15},{10,... | collective-permute-start | bytes 73736 | tf_op jit(solution)/shard_map/ppermute | solution.py:33
  74.2 0.5 collective-permute-done.28.refs_2_
  74.8 3.7 %collective-permute-done.29.refs_3_ = bf16[24,512]{1,0:T(8,128)(2,1)S(1)} collective-permute-done((bf16[24,512]{1,0:T(8,128)(2,1)S(1)}, bf16[24,512]{1,0:T(8,128)(2,1)S(1)}, u32[]{:S(2)}, u32[]{:S(2)}) %collective-permute-start.29) | collective-permute-done | bytes 24608 | tf_op jit(solution)/shard_map/ppermute | solution.py:33
  78.5 0.6 shard_map.220
  (47 shorter events, 1.0 us)
Async XLA Ops:
  0.6 17.6 %copy-start.7 = (s32[24,2]{0,1:T(2,128)S(1)}, s32[24,2]{0,1:T(2,128)}, u32[]{:S(2)}) copy-start(s32[24,2]{0,1:T(2,128)} %param.32) | copy-start | bytes 580
  0.6 17.6 %copy-start.6 = (f32[256]{0:T(256)S(1)}, f32[256]{0:T(256)}, u32[]{:S(2)}) copy-start(f32[256]{0:T(256)} %param.27) | copy-start | bytes 3076
  0.7 17.6 %copy-start.5 = (f32[256]{0:T(256)S(1)}, f32[256]{0:T(256)}, u32[]{:S(2)}) copy-start(f32[256]{0:T(256)} %param.26) | copy-start | bytes 3076
  1.6 7.0 %collective-permute-start = (bf16[24,1024]{1,0:T(8,128)(2,1)S(1)}, bf16[24,1024]{1,0:T(8,128)(2,1)S(1)}, u32[]{:S(2)}, u32[]{:S(2)}) collective-permute-start(bf16[24,1024]{1,0:T(8,128)(2,1)S(1)} %get-tuple-element.48), channel_id=1, source_target_pairs={{0,9},{1,8},{2,11},{3,10},{4,13},{5,12},{6,15},{7,14},{8,1},{9,0},... | collective-permute-start | bytes 147464 | tf_op jit(solution)/shard_map/ppermute | solution.py:380
  4.1 4.5 %collective-permute-start.1 = (bf16[24,1024]{1,0:T(8,128)(2,1)S(1)}, bf16[24,1024]{1,0:T(8,128)(2,1)S(1)}, u32[]{:S(2)}, u32[]{:S(2)}) collective-permute-start(bf16[24,1024]{1,0:T(8,128)(2,1)S(1)} %get-tuple-element.49), channel_id=1, source_target_pairs={{0,17},{1,16},{2,19},{3,18},{4,21},{5,20},{6,23},{7,22},{8,25},{9,... | collective-permute-start | bytes 147464 | tf_op jit(solution)/shard_map/ppermute | solution.py:380
  5.9 4.9 %collective-permute-start.2 = (bf16[24,1024]{1,0:T(8,128)(2,1)S(1)}, bf16[24,1024]{1,0:T(8,128)(2,1)S(1)}, u32[]{:S(2)}, u32[]{:S(2)}) collective-permute-start(bf16[24,1024]{1,0:T(8,128)(2,1)S(1)} %get-tuple-element.50), channel_id=1, source_target_pairs={{0,25},{1,24},{2,27},{3,26},{4,29},{5,28},{6,31},{7,30},{8,17},{9,... | collective-permute-start | bytes 147464 | tf_op jit(solution)/shard_map/ppermute | solution.py:380
  11.3 14.5 %copy-start.3 = (bf16[256,1024]{1,0:T(8,128)(2,1)S(1)}, bf16[256,1024]{1,0:T(8,128)(2,1)}, u32[]{:S(2)}) copy-start(bf16[256,1024]{1,0:T(8,128)(2,1)} %refs_4_.1) | copy-start | bytes 1572868
  11.3 6.9 %collective-permute-start.3 = (bf16[24,1024]{1,0:T(8,128)(2,1)S(1)}, bf16[24,1024]{1,0:T(8,128)(2,1)S(1)}, u32[]{:S(2)}, u32[]{:S(2)}) collective-permute-start(bf16[24,1024]{1,0:T(8,128)(2,1)S(1)} %get-tuple-element.58), channel_id=1, source_target_pairs={{0,8},{8,0},{16,24},{24,16},{1,9},{9,1},{17,25},{25,17},{2,10},{10... | collective-permute-start | bytes 147464 | tf_op jit(solution)/shard_map/ppermute | solution.py:33
  11.8 6.4 %collective-permute-start.4 = (bf16[24,1024]{1,0:T(8,128)(2,1)S(1)}, bf16[24,1024]{1,0:T(8,128)(2,1)S(1)}, u32[]{:S(2)}, u32[]{:S(2)}) collective-permute-start(bf16[24,1024]{1,0:T(8,128)(2,1)S(1)} %get-tuple-element.59), channel_id=1, source_target_pairs={{0,16},{8,24},{16,0},{24,8},{1,17},{9,25},{17,1},{25,9},{2,18},{10... | collective-permute-start | bytes 147464 | tf_op jit(solution)/shard_map/ppermute | solution.py:33
  12.1 6.2 %collective-permute-start.5 = (bf16[24,1024]{1,0:T(8,128)(2,1)S(1)}, bf16[24,1024]{1,0:T(8,128)(2,1)S(1)}, u32[]{:S(2)}, u32[]{:S(2)}) collective-permute-start(bf16[24,1024]{1,0:T(8,128)(2,1)S(1)} %get-tuple-element.60), channel_id=1, source_target_pairs={{0,24},{8,16},{16,8},{24,0},{1,25},{9,17},{17,9},{25,1},{2,26},{10... | collective-permute-start | bytes 147464 | tf_op jit(solution)/shard_map/ppermute | solution.py:33
  19.5 6.3 %collective-permute-start.8 = (bf16[24,384]{1,0:T(8,128)(2,1)S(1)}, bf16[24,384]{1,0:T(8,128)(2,1)S(1)}, u32[]{:S(2)}, u32[]{:S(2)}) collective-permute-start(bf16[24,384]{1,0:T(8,128)(2,1)S(1)} %get-tuple-element.66.refs_0_.refs_8_), channel_id=1, source_target_pairs={{0,24},{8,16},{16,8},{24,0},{1,25},{9,17},{17,9},{25,1},{2,26},{10... | collective-permute-start | bytes 55304 | tf_op jit(solution)/shard_map/ppermute | solution.py:33
  21.1 4.6 %collective-permute-start.7 = (bf16[24,384]{1,0:T(8,128)(2,1)S(1)}, bf16[24,384]{1,0:T(8,128)(2,1)S(1)}, u32[]{:S(2)}, u32[]{:S(2)}) collective-permute-start(bf16[24,384]{1,0:T(8,128)(2,1)S(1)} %get-tuple-element.66.refs_0_.refs_8_), channel_id=1, source_target_pairs={{0,16},{8,24},{16,0},{24,8},{1,17},{9,25},{17,1},{25,9},{2,18},{10... | collective-permute-start | bytes 55304 | tf_op jit(solution)/shard_map/ppermute | solution.py:33
  21.6 4.2 %collective-permute-start.6 = (bf16[24,384]{1,0:T(8,128)(2,1)S(1)}, bf16[24,384]{1,0:T(8,128)(2,1)S(1)}, u32[]{:S(2)}, u32[]{:S(2)}) collective-permute-start(bf16[24,384]{1,0:T(8,128)(2,1)S(1)} %get-tuple-element.66.refs_0_.refs_8_), channel_id=1, source_target_pairs={{0,8},{8,0},{16,24},{24,16},{1,9},{9,1},{17,25},{25,17},{2,10},{10... | collective-permute-start | bytes 55304 | tf_op jit(solution)/shard_map/ppermute | solution.py:33
  26.0 1.4 %collective-permute-start.9 = (bf16[96,512]{1,0:T(8,128)(2,1)S(1)}, bf16[96,512]{1,0:T(8,128)(2,1)S(1)}, u32[]{:S(2)}, u32[]{:S(2)}) collective-permute-start(bf16[96,512]{1,0:T(8,128)(2,1)S(1)} %get-tuple-element.70), channel_id=1, source_target_pairs={{0,1},{1,0},{2,3},{3,2},{4,5},{5,4},{6,7},{7,6},{8,9},{9,8},{10,11... | collective-permute-start | bytes 294920 | tf_op jit(solution)/shard_map/ppermute | solution.py:33
  27.4 8.8 %collective-permute-start.12 = (bf16[96,512]{1,0:T(8,128)(2,1)S(1)}, bf16[96,512]{1,0:T(8,128)(2,1)S(1)}, u32[]{:S(2)}, u32[]{:S(2)}) collective-permute-start(bf16[96,512]{1,0:T(8,128)(2,1)S(1)} %shard_map.211.refs_2_), channel_id=1, source_target_pairs={{0,7},{1,6},{2,5},{3,4},{4,3},{5,2},{6,1},{7,0},{8,15},{9,14},{10,... | collective-permute-start | bytes 294920 | tf_op jit(solution)/shard_map/ppermute | solution.py:33
  30.8 9.1 %collective-permute-start.11 = (bf16[96,512]{1,0:T(8,128)(2,1)S(1)}, bf16[96,512]{1,0:T(8,128)(2,1)S(1)}, u32[]{:S(2)}, u32[]{:S(2)}) collective-permute-start(bf16[96,512]{1,0:T(8,128)(2,1)S(1)} %shard_map.211.refs_2_), channel_id=1, source_target_pairs={{0,4},{1,5},{2,6},{3,7},{4,0},{5,1},{6,2},{7,3},{8,12},{9,13},{10,... | collective-permute-start | bytes 294920 | tf_op jit(solution)/shard_map/ppermute | solution.py:33
  30.8 9.1 %collective-permute-start.10 = (bf16[96,512]{1,0:T(8,128)(2,1)S(1)}, bf16[96,512]{1,0:T(8,128)(2,1)S(1)}, u32[]{:S(2)}, u32[]{:S(2)}) collective-permute-start(bf16[96,512]{1,0:T(8,128)(2,1)S(1)} %shard_map.211.refs_2_), channel_id=1, source_target_pairs={{0,3},{1,2},{2,1},{3,0},{4,7},{5,6},{6,5},{7,4},{8,11},{9,10},{10,... | collective-permute-start | bytes 294920 | tf_op jit(solution)/shard_map/ppermute | solution.py:33
  31.3 17.3 %copy-start.1 = (bf16[1024,352]{0,1:T(8,128)(2,1)S(1)}, bf16[1024,352]{0,1:T(8,128)(2,1)}, u32[]{:S(2)}) copy-start(bf16[1024,352]{0,1:T(8,128)(2,1)} %param.36) | copy-start | bytes 2162692
  31.3 17.3 %copy-start.2 = (bf16[1024,352]{0,1:T(8,128)(2,1)S(1)}, bf16[1024,352]{0,1:T(8,128)(2,1)}, u32[]{:S(2)}) copy-start(bf16[1024,352]{0,1:T(8,128)(2,1)} %param.37) | copy-start | bytes 2162692
  31.3 17.3 %copy-start.4 = (f32[4096]{0:T(1024)S(1)}, f32[4096]{0:T(1024)}, u32[]{:S(2)}) copy-start(f32[4096]{0:T(1024)} %param.30) | copy-start | bytes 49156
  40.0 6.1 %collective-permute-start.15 = (bf16[96,512]{1,0:T(8,128)(2,1)S(1)}, bf16[96,512]{1,0:T(8,128)(2,1)S(1)}, u32[]{:S(2)}, u32[]{:S(2)}) collective-permute-start(bf16[96,512]{1,0:T(8,128)(2,1)S(1)} %shard_map.213.refs_0_.mine), channel_id=1, source_target_pairs={{0,25},{1,24},{2,27},{3,26},{4,29},{5,28},{6,31},{7,30},{8,17},{9,... | collective-permute-start | bytes 294920 | tf_op jit(solution)/shard_map/ppermute | solution.py:380
  41.0 7.1 %collective-permute-start.14 = (bf16[96,512]{1,0:T(8,128)(2,1)S(1)}, bf16[96,512]{1,0:T(8,128)(2,1)S(1)}, u32[]{:S(2)}, u32[]{:S(2)}) collective-permute-start(bf16[96,512]{1,0:T(8,128)(2,1)S(1)} %shard_map.213.refs_0_.mine), channel_id=1, source_target_pairs={{0,16},{1,17},{2,18},{3,19},{4,20},{5,21},{6,22},{7,23},{8,24},{9,... | collective-permute-start | bytes 294920 | tf_op jit(solution)/shard_map/ppermute | solution.py:380
  41.9 6.3 %collective-permute-start.13 = (bf16[96,512]{1,0:T(8,128)(2,1)S(1)}, bf16[96,512]{1,0:T(8,128)(2,1)S(1)}, u32[]{:S(2)}, u32[]{:S(2)}) collective-permute-start(bf16[96,512]{1,0:T(8,128)(2,1)S(1)} %shard_map.213.refs_0_.mine), channel_id=1, source_target_pairs={{0,9},{1,8},{2,11},{3,10},{4,13},{5,12},{6,15},{7,14},{8,1},{9,0},... | collective-permute-start | bytes 294920 | tf_op jit(solution)/shard_map/ppermute | solution.py:380
  43.0 5.7 %collective-permute-start.16 = (bf16[96,512]{1,0:T(8,128)(2,1)S(1)}, bf16[96,512]{1,0:T(8,128)(2,1)S(1)}, u32[]{:S(2)}, u32[]{:S(2)}) collective-permute-start(bf16[96,512]{1,0:T(8,128)(2,1)S(1)} %shard_map.213.refs_0_.mine), channel_id=1, source_target_pairs={{0,1},{1,0},{2,3},{3,2},{4,5},{5,4},{6,7},{7,6},{8,9},{9,8},{10,11... | collective-permute-start | bytes 294920 | tf_op jit(solution)/shard_map/ppermute | solution.py:33
  46.1 5.6 %collective-permute-start.19 = (bf16[96,512]{1,0:T(8,128)(2,1)S(1)}, bf16[96,512]{1,0:T(8,128)(2,1)S(1)}, u32[]{:S(2)}, u32[]{:S(2)}) collective-permute-start(bf16[96,512]{1,0:T(8,128)(2,1)S(1)} %collective-permute-done.15.refs_3_), channel_id=1, source_target_pairs={{0,1},{1,0},{2,3},{3,2},{4,5},{5,4},{6,7},{7,6},{8,9},{9,8},{10,11... | collective-permute-start | bytes 294920 | tf_op jit(solution)/shard_map/ppermute | solution.py:33
  48.1 4.7 %collective-permute-start.18 = (bf16[96,512]{1,0:T(8,128)(2,1)S(1)}, bf16[96,512]{1,0:T(8,128)(2,1)S(1)}, u32[]{:S(2)}, u32[]{:S(2)}) collective-permute-start(bf16[96,512]{1,0:T(8,128)(2,1)S(1)} %collective-permute-done.14.refs_2_), channel_id=1, source_target_pairs={{0,1},{1,0},{2,3},{3,2},{4,5},{5,4},{6,7},{7,6},{8,9},{9,8},{10,11... | collective-permute-start | bytes 294920 | tf_op jit(solution)/shard_map/ppermute | solution.py:33
  48.2 4.6 %collective-permute-start.17 = (bf16[96,512]{1,0:T(8,128)(2,1)S(1)}, bf16[96,512]{1,0:T(8,128)(2,1)S(1)}, u32[]{:S(2)}, u32[]{:S(2)}) collective-permute-start(bf16[96,512]{1,0:T(8,128)(2,1)S(1)} %collective-permute-done.13.refs_1_), channel_id=1, source_target_pairs={{0,1},{1,0},{2,3},{3,2},{4,5},{5,4},{6,7},{7,6},{8,9},{9,8},{10,11... | collective-permute-start | bytes 294920 | tf_op jit(solution)/shard_map/ppermute | solution.py:33
  49.2 7.7 %collective-permute-start.22 = (bf16[96,768]{1,0:T(8,128)(2,1)S(1)}, bf16[96,768]{1,0:T(8,128)(2,1)S(1)}, u32[]{:S(2)}, u32[]{:S(2)}) collective-permute-start(bf16[96,768]{1,0:T(8,128)(2,1)S(1)} %get-tuple-element.77), channel_id=1, source_target_pairs={{0,24},{8,16},{16,8},{24,0},{1,25},{9,17},{17,9},{25,1},{2,26},{10... | collective-permute-start | bytes 442376 | tf_op jit(solution)/shard_map/ppermute | solution.py:33
  50.9 8.3 %collective-permute-start.21 = (bf16[96,768]{1,0:T(8,128)(2,1)S(1)}, bf16[96,768]{1,0:T(8,128)(2,1)S(1)}, u32[]{:S(2)}, u32[]{:S(2)}) collective-permute-start(bf16[96,768]{1,0:T(8,128)(2,1)S(1)} %get-tuple-element.77), channel_id=1, source_target_pairs={{0,16},{8,24},{16,0},{24,8},{1,17},{9,25},{17,1},{25,9},{2,18},{10... | collective-permute-start | bytes 442376 | tf_op jit(solution)/shard_map/ppermute | solution.py:33
  51.7 7.5 %collective-permute-start.20 = (bf16[96,768]{1,0:T(8,128)(2,1)S(1)}, bf16[96,768]{1,0:T(8,128)(2,1)S(1)}, u32[]{:S(2)}, u32[]{:S(2)}) collective-permute-start(bf16[96,768]{1,0:T(8,128)(2,1)S(1)} %get-tuple-element.77), channel_id=1, source_target_pairs={{0,8},{8,0},{16,24},{24,16},{1,9},{9,1},{17,25},{25,17},{2,10},{10... | collective-permute-start | bytes 442376 | tf_op jit(solution)/shard_map/ppermute | solution.py:33
  52.8 6.4 %copy-start = (bf16[352,1024]{1,0:T(8,128)(2,1)S(1)}, bf16[352,1024]{1,0:T(8,128)(2,1)}, u32[]{:S(2)}) copy-start(bf16[352,1024]{1,0:T(8,128)(2,1)} %refs_2_.3) | copy-start | bytes 2162692
  60.1 1.8 %collective-permute-start.23 = (bf16[96,2048]{1,0:T(8,128)(2,1)S(1)}, bf16[96,2048]{1,0:T(8,128)(2,1)S(1)}, u32[]{:S(2)}, u32[]{:S(2)}) collective-permute-start(bf16[96,2048]{1,0:T(8,128)(2,1)S(1)} %get-tuple-element.81), channel_id=1, source_target_pairs={{0,1},{1,0},{2,3},{3,2},{4,5},{5,4},{6,7},{7,6},{8,9},{9,8},{10,11... | collective-permute-start | bytes 1179656 | tf_op jit(solution)/shard_map/ppermute | solution.py:33
  61.9 5.1 %collective-permute-start.24 = (bf16[24,2048]{1,0:T(8,128)(2,1)S(1)}, bf16[24,2048]{1,0:T(8,128)(2,1)S(1)}, u32[]{:S(2)}, u32[]{:S(2)}) collective-permute-start(bf16[24,2048]{1,0:T(8,128)(2,1)S(1)} %get-tuple-element.83), channel_id=1, source_target_pairs={{0,8},{8,0},{16,24},{24,16},{1,9},{9,1},{17,25},{25,17},{2,10},{10... | collective-permute-start | bytes 294920 | tf_op jit(solution)/shard_map/ppermute | solution.py:33
  63.0 6.7 %collective-permute-start.25 = (bf16[24,2048]{1,0:T(8,128)(2,1)S(1)}, bf16[24,2048]{1,0:T(8,128)(2,1)S(1)}, u32[]{:S(2)}, u32[]{:S(2)}) collective-permute-start(bf16[24,2048]{1,0:T(8,128)(2,1)S(1)} %get-tuple-element.84), channel_id=1, source_target_pairs={{0,16},{8,24},{16,0},{24,8},{1,17},{9,25},{17,1},{25,9},{2,18},{10... | collective-permute-start | bytes 294920 | tf_op jit(solution)/shard_map/ppermute | solution.py:33
  64.1 5.6 %collective-permute-start.26 = (bf16[24,2048]{1,0:T(8,128)(2,1)S(1)}, bf16[24,2048]{1,0:T(8,128)(2,1)S(1)}, u32[]{:S(2)}, u32[]{:S(2)}) collective-permute-start(bf16[24,2048]{1,0:T(8,128)(2,1)S(1)} %get-tuple-element.85), channel_id=1, source_target_pairs={{0,24},{8,16},{16,8},{24,0},{1,25},{9,17},{17,9},{25,1},{2,26},{10... | collective-permute-start | bytes 294920 | tf_op jit(solution)/shard_map/ppermute | solution.py:33
  69.8 4.5 %collective-permute-start.27 = (bf16[24,512]{1,0:T(8,128)(2,1)S(1)}, bf16[24,512]{1,0:T(8,128)(2,1)S(1)}, u32[]{:S(2)}, u32[]{:S(2)}) collective-permute-start(bf16[24,512]{1,0:T(8,128)(2,1)S(1)} %get-tuple-element.88), channel_id=1, source_target_pairs={{0,2},{1,3},{2,0},{3,1},{4,6},{5,7},{6,4},{7,5},{8,10},{9,11},{10,... | collective-permute-start | bytes 73736 | tf_op jit(solution)/shard_map/ppermute | solution.py:33
  70.1 4.7 %collective-permute-start.28 = (bf16[24,512]{1,0:T(8,128)(2,1)S(1)}, bf16[24,512]{1,0:T(8,128)(2,1)S(1)}, u32[]{:S(2)}, u32[]{:S(2)}) collective-permute-start(bf16[24,512]{1,0:T(8,128)(2,1)S(1)} %get-tuple-element.89), channel_id=1, source_target_pairs={{0,4},{1,5},{2,6},{3,7},{4,0},{5,1},{6,2},{7,3},{8,12},{9,13},{10,... | collective-permute-start | bytes 73736 | tf_op jit(solution)/shard_map/ppermute | solution.py:33
  72.9 5.6 %collective-permute-start.29 = (bf16[24,512]{1,0:T(8,128)(2,1)S(1)}, bf16[24,512]{1,0:T(8,128)(2,1)S(1)}, u32[]{:S(2)}, u32[]{:S(2)}) collective-permute-start(bf16[24,512]{1,0:T(8,128)(2,1)S(1)} %get-tuple-element.90), channel_id=1, source_target_pairs={{0,6},{1,7},{2,4},{3,5},{4,2},{5,3},{6,0},{7,1},{8,14},{9,15},{10,... | collective-permute-start | bytes 73736 | tf_op jit(solution)/shard_map/ppermute | solution.py:33

commit v2 on v1

--- a/solution.py
+++ b/solution.py
@@ -43,7 +43,7 @@
 
 def half_index():
     t = lax.axis_index("tp")
-    return lax.rem(t + lax.div(t, 2) + lax.axis_index("ep"), 2)
+    return lax.rem(t + lax.div(t, 4) + lax.div(lax.axis_index("ep"), 2), 2)
 
 
 def call(body, outs, ins, args, scratch=(), flops=0, limit=24):
@@ -109,8 +109,8 @@
     *copied, token = call(
         functools.partial(fetch_kernel, len(arrays)),
         [(a.shape, a.dtype) for a in arrays] + [((8, LANES), F32)],
-        [HBM] * len(arrays) + [VMEM],
-        (*arrays, after),
+        [HBM] * len(arrays) + [VMEM] * len(after),
+        (*arrays, *after),
         [pltpu.SemaphoreType.DMA((24 * len(arrays),))],
         flops=1 << 26,
         limit=1,
@@ -118,7 +118,8 @@
     return copied, token
 
 
-def inverse_kernel(tokens, router_t, branch, out, router):
+def inverse_kernel(tokens, router_t, branch, routes_t, out, router, mask):
+    mask[...] = route_mask(routes_t[...]).astype(BF16)
     out[...] = jnp.broadcast_to(inverse_rms(tokens[...].astype(F32)), out.shape)
     extra = jnp.broadcast_to(branch[...].astype(F32), (8, branch.shape[1]))
     router[...] = jnp.concatenate([router_t[...].astype(F32), extra], axis=0).astype(BF16)
@@ -147,7 +148,7 @@
 
 def read_kernel(n_ep, *refs):
     own, got = refs[0], refs[1:n_ep]
-    inverse, floor, head_gain, state, routes_t = refs[n_ep : n_ep + 5]
+    inverse, floor, head_gain, state, mask = refs[n_ep : n_ep + 5]
     mixed, gates, scratch = refs[n_ep + 6 :]
     batch, heads, size = state.shape[:3]
     channels = heads * size
@@ -172,7 +173,7 @@
             scratch[b : b + 1, h * size : (h + 1) * size] = jnp.sum(
                 column * state[b, h], axis=0, keepdims=True
             )
-    mixed[:, channels:] = route_mask(routes_t[...]).astype(BF16)
+    mixed[:, channels:] = mask[...]
     scale = head_gain[...] * silu(out_gate)
     for h in range(heads):
         lanes = slice(h * size, (h + 1) * size)
@@ -412,8 +413,9 @@
         own_payload = payloads[0]
         payloads = [own_payload] + [cross_swap(payloads[k], k, 1) for k in others]
 
+        branch_row = branch_gate[None]
         (*weights, gain), token = fetch(
-            (w_query, w_forget, w_input, w_outgate, norm_gain[None]), own_payload
+            (w_query, w_forget, w_input, w_outgate, norm_gain[None]), (own_payload, branch_row)
         )
         own, *sent = call(
             functools.partial(project_kernel, n_ep),
@@ -423,12 +425,16 @@
             flops=8 * rows * block * channels,
         )
         got = [ep_swap(sent[k - 1], k) for k in others]
-        (state, full, router_t), token = fetch((recurrent_state, tokens, w_router.T), own)
-        inverse, router = call(
+        (state, full, router_t), token = fetch((recurrent_state, tokens, w_router.T), (own,))
+        inverse, router, mask = call(
             inverse_kernel,
-            [((batch, LANES), F32), ((w_router.shape[1] + 8, width), BF16)],
-            [VMEM] * 3,
-            (full, router_t, branch_gate[None]),
+            [
+                ((batch, LANES), F32),
+                ((w_router.shape[1] + 8, width), BF16),
+                ((batch, LANES), BF16),
+            ],
+            [VMEM] * 4,
+            (full, router_t, branch_row, routes.T),
         )
 
 
@@ -436,7 +442,7 @@
             functools.partial(read_kernel, n_ep),
             [((batch, channels + LANES), BF16), ((batch, 3 * channels), F32)],
             [VMEM] * (n_ep + 6),
-            (own, *got, inverse, forget_floor[None], head_gain[None], state, routes.T, token),
+            (own, *got, inverse, forget_floor[None], head_gain[None], state, mask, token),
             [pltpu.VMEM((batch, channels), F32)],
             flops=1 << 24,
         )
@@ -468,9 +474,9 @@
         )
         core = core_swap(give)
         (summed,) = call(add_kernel, [((rows, half), BF16)], [VMEM] * 2, (keep, core))
-        along = [z_swap(summed, m, m & 1) for m in range(1, n_z)]
+        along = [z_swap(summed, m, (m >> 1) & 1) for m in range(1, n_z)]
         (gate_w, up_w), token = fetch(
-            (jnp.swapaxes(expert_gate, 1, 2), jnp.swapaxes(expert_up, 1, 2)), summed
+            (jnp.swapaxes(expert_gate, 1, 2), jnp.swapaxes(expert_up, 1, 2)), (summed,)
         )
         (part,) = call(
             functools.partial(hidden_kernel, n_ep),
@@ -479,7 +485,7 @@
             (*payloads, keep, core, *along, token),
         )
 
-        pieces = [part] + [cross_swap(part, k, k & 1) for k in others]
+        pieces = [part] + [cross_swap(part, k, (k >> 1) & 1) for k in others]
         sibling = core_swap(part)
         padded = -(-shared_width // LANES) * LANES
         shared_own, shared_sent = call(

time: 79.4 us -> 78.7 us (level)
  waiting for transfers between devices: 24.2 us -> 22.9 us
    ppermute x6, waiting for transfers between devices: 7.28 us -> 6.21 us  [cross_swap(): return lax.ppermute(value, ('ep', 'tp'), pairs)]
  transfers between devices with their start and end apart: 30 -> 30, of which waited for: 12 -> 13; matrix products, arithmetic and copies ran while one was open for 1% -> 1% of each run, Pallas kernels for 23% -> 23%
where the time goes in v2:
time: 78.7 us; the launch traced here: 78.5 us
  starting transfers between devices  31.2 us (40%)
  waiting for transfers between devices  22.9 us (29%)
  Pallas kernels  22.7 us (29%)
  between operations  0.88 us (1%)
    ppermute x24, starting transfers between devices, swap(): return lax.ppermute(value, axis, [(s, s ^ step) for s in range(size)])  23.6 us
    pallas_call x17, Pallas kernels, call(): pl.pallas_call(body, out_shape=[jax.ShapeDtypeStruct(s, d) for s, d in ou...  20 us
    ppermute x24, waiting for transfers between devices, swap(): return lax.ppermute(value, axis, [(s, s ^ step) for s in range(size)])  16.7 us
    ppermute x6, starting transfers between devices, cross_swap(): return lax.ppermute(value, ('ep', 'tp'), pairs)  7.57 us
    ppermute x6, waiting for transfers between devices, cross_swap(): return lax.ppermute(value, ('ep', 'tp'), pairs)  6.21 us
    pallas_call x1, Pallas kernels, body(): pl.pallas_call(functools.partial(update_kernel, group), out_shape=[jax.Sh...  2.71 us
  transfers between devices with their start and end apart: 30, of which 13 were waited for; matrix products, arithmetic and copies ran while one was open for 1% of the time, Pallas kernels for 23%

profile of v2, /device:TPU:0, one launch (start us, length us, event | category | flops | bytes accessed | tf_op | source)
XLA Modules:
  0.0 78.5 jit_solution(11142977531887011892)
XLA Ops:
  0.7 0.9 %shard_map.203 = (bf16[24,1024]{1,0:T(8,128)(2,1)S(1)}, bf16[24,1024]{1,0:T(8,128)(2,1)S(1)}, bf16[24,1024]{1,0:T(8,128)(2,1)S(1)}, bf16[24,1024]{1,0:T(8,128)(2,1)S(1)}) custom-call(bf16[24,4096]{1,0:T(8,128)(2,1)} %refs_1_.3), custom_call_target="tpu_custom_call" | custom-call | tf_op jit(solution)/shard_map/pallas_call | solution.py:50
  1.6 2.5 %collective-permute-start = (bf16[24,1024]{1,0:T(8,128)(2,1)S(1)}, bf16[24,1024]{1,0:T(8,128)(2,1)S(1)}, u32[]{:S(2)}, u32[]{:S(2)}) collective-permute-start(bf16[24,1024]{1,0:T(8,128)(2,1)S(1)} %get-tuple-element.49), channel_id=1, source_target_pairs={{0,9},{1,8},{2,11},{3,10},{4,13},{5,12},{6,15},{7,14},{8,1},{9,0},... | collective-permute-start | bytes 147464 | tf_op jit(solution)/shard_map/ppermute | solution.py:381
  4.1 1.8 %collective-permute-start.1 = (bf16[24,1024]{1,0:T(8,128)(2,1)S(1)}, bf16[24,1024]{1,0:T(8,128)(2,1)S(1)}, u32[]{:S(2)}, u32[]{:S(2)}) collective-permute-start(bf16[24,1024]{1,0:T(8,128)(2,1)S(1)} %get-tuple-element.50), channel_id=1, source_target_pairs={{0,17},{1,16},{2,19},{3,18},{4,21},{5,20},{6,23},{7,22},{8,25},{9,... | collective-permute-start | bytes 147464 | tf_op jit(solution)/shard_map/ppermute | solution.py:381
  5.9 0.7 broadcast_in_dim.17.refs_6_.branch
  6.6 2.7 %shard_map.204 = (bf16[1024,256]{1,0:T(8,128)(2,1)S(1)}, bf16[1024,256]{1,0:T(8,128)(2,1)S(1)}, bf16[1024,256]{1,0:T(8,128)(2,1)S(1)}, bf16[1024,256]{1,0:T(8,12...) custom-call(bf16[1024,256]{1,0:T(8,128)(2,1)} %refs_0_.2, bf16[1024,256]{1,0:T(8,128)(2,1)} %refs_1_.2, ...), custom_call_target="tpu_custom_call" | custom-call | flops 67108864 | tf_op jit(solution)/shard_map/pallas_call | solution.py:50
  9.3 1.5 %collective-permute-done.2.refs_3_ = bf16[24,1024]{1,0:T(8,128)(2,1)S(1)} collective-permute-done((bf16[24,1024]{1,0:T(8,128)(2,1)S(1)}, bf16[24,1024]{1,0:T(8,128)(2,1)S(1)}, u32[]{:S(2)}, u32[]{:S(2)}) %collective-permute-start.2) | collective-permute-done | bytes 49184 | tf_op jit(solution)/shard_map/ppermute | solution.py:381
  10.8 0.5 shard_map.205
  11.3 0.5 collective-permute-start.3
  11.8 1.0 %collective-permute-start.4 = (bf16[24,1024]{1,0:T(8,128)(2,1)S(1)}, bf16[24,1024]{1,0:T(8,128)(2,1)S(1)}, u32[]{:S(2)}, u32[]{:S(2)}) collective-permute-start(bf16[24,1024]{1,0:T(8,128)(2,1)S(1)} %get-tuple-element.60), channel_id=1, source_target_pairs={{0,16},{8,24},{16,0},{24,8},{1,17},{9,25},{17,1},{25,9},{2,18},{10... | collective-permute-start | bytes 147464 | tf_op jit(solution)/shard_map/ppermute | solution.py:33
  12.8 2.1 %collective-permute-start.5 = (bf16[24,1024]{1,0:T(8,128)(2,1)S(1)}, bf16[24,1024]{1,0:T(8,128)(2,1)S(1)}, u32[]{:S(2)}, u32[]{:S(2)}) collective-permute-start(bf16[24,1024]{1,0:T(8,128)(2,1)S(1)} %get-tuple-element.61), channel_id=1, source_target_pairs={{0,24},{8,16},{16,8},{24,0},{1,25},{9,17},{17,9},{25,1},{2,26},{10... | collective-permute-start | bytes 147464 | tf_op jit(solution)/shard_map/ppermute | solution.py:33
  14.8 2.5 %shard_map.206 = (f32[24,2,128,128]{3,2,1,0:T(8,128)S(1)}, bf16[24,4096]{1,0:T(8,128)(2,1)S(1)}, bf16[8,4096]{1,0:T(8,128)(2,1)S(1)}, f32[8,128]{1,0:T(8,128)S(1)}) custom-call(f32[24,2,128,128]{3,2,1,0:T(8,128)} %refs_0_.3, bf16[24,4096]{1,0:T(8,128)(2,1)} %refs_1_.3, bf16[8,4096]{1,0:T(8,128)(2,1)} %bitcast.19, ...), custom_call_target="tpu_custom_call" | custom-call | flops 67108864 | tf_op jit(solution)/shard_map/pallas_call | solution.py:50
  17.8 1.2 %shard_map.208 = (bf16[24,384]{1,0:T(8,128)(2,1)S(1)}, f32[24,768]{1,0:T(8,128)S(1)}) custom-call(f32[24,1024]{1,0:T(8,128)S(1)} %get-tuple-element.58.refs_3_.refs_0_, bf16[24,1024]{1,0:T(8,128)(2,1)S(1)} %collective-permute-done.3.refs_1_, bf16[24,1024]{1,0:T(8,128)(2,1)S(1)} %collective-permute-done.4.refs_2_, ...), custom_call_target="tpu_custom_call" | custom-call | flops 16777216 | tf_op jit(solution)/shard_map/pallas_call | solution.py:50
  19.0 2.1 %collective-permute-start.8 = (bf16[24,384]{1,0:T(8,128)(2,1)S(1)}, bf16[24,384]{1,0:T(8,128)(2,1)S(1)}, u32[]{:S(2)}, u32[]{:S(2)}) collective-permute-start(bf16[24,384]{1,0:T(8,128)(2,1)S(1)} %get-tuple-element.68.refs_0_.refs_8_), channel_id=1, source_target_pairs={{0,24},{8,16},{16,8},{24,0},{1,25},{9,17},{17,9},{25,1},{2,26},{10... | collective-permute-start | bytes 55304 | tf_op jit(solution)/shard_map/ppermute | solution.py:33
  21.1 0.5 collective-permute-start.7
  21.6 1.0 %collective-permute-start.6 = (bf16[24,384]{1,0:T(8,128)(2,1)S(1)}, bf16[24,384]{1,0:T(8,128)(2,1)S(1)}, u32[]{:S(2)}, u32[]{:S(2)}) collective-permute-start(bf16[24,384]{1,0:T(8,128)(2,1)S(1)} %get-tuple-element.68.refs_0_.refs_8_), channel_id=1, source_target_pairs={{0,8},{8,0},{16,24},{24,16},{1,9},{9,1},{17,25},{25,17},{2,10},{10... | collective-permute-start | bytes 55304 | tf_op jit(solution)/shard_map/ppermute | solution.py:33
  22.5 2.7 %shard_map.209 = (f32[24,2,128,128]{3,2,1,0:T(8,128)}, f32[8,128]{1,0:T(8,128)S(1)}) custom-call(f32[24,768]{1,0:T(8,128)S(1)} %get-tuple-element.69.gates, f32[24,2,128,128]{3,2,1,0:T(8,128)S(1)} %get-tuple-element.65.refs_7_.state), custom_call_target="tpu_custom_call" | custom-call | flops 67108864 | tf_op jit(solution)/shard_map/pallas_call | solution.py:452
  25.6 1.3 %collective-permute-done.9.got.refs_5_ = bf16[96,512]{1,0:T(8,128)(2,1)S(1)} collective-permute-done((bf16[96,512]{1,0:T(8,128)(2,1)S(1)}, bf16[96,512]{1,0:T(8,128)(2,1)S(1)}, u32[]{:S(2)}, u32[]{:S(2)}) %collective-permute-start.9) | collective-permute-done | bytes 98336 | tf_op jit(solution)/shard_map/ppermute | solution.py:33
  26.9 3.4 %collective-permute-start.12 = (bf16[96,512]{1,0:T(8,128)(2,1)S(1)}, bf16[96,512]{1,0:T(8,128)(2,1)S(1)}, u32[]{:S(2)}, u32[]{:S(2)}) collective-permute-start(bf16[96,512]{1,0:T(8,128)(2,1)S(1)} %shard_map.211.refs_2_), channel_id=1, source_target_pairs={{0,7},{1,6},{2,5},{3,4},{4,3},{5,2},{6,1},{7,0},{8,15},{9,14},{10,... | collective-permute-start | bytes 294920 | tf_op jit(solution)/shard_map/ppermute | solution.py:33
  30.4 0.7 collective-permute-start.10
  31.1 4.9 %shard_map.212 = (bf16[2,352,4096]{2,1,0:T(8,128)(2,1)S(1)}, bf16[2,352,4096]{2,1,0:T(8,128)(2,1)S(1)}, f32[8,128]{1,0:T(8,128)S(1)}) custom-call(bf16[2,352,4096]{2,1,0:T(8,128)(2,1)} %bitcast.17, bf16[2,352,4096]{2,1,0:T(8,128)(2,1)} %bitcast.18, bf16[96,512]{1,0:T(8,128)(2,1)S(1)} %shard_map.211.refs_2_), custom_call_target="tpu_custom_call" | custom-call | flops 67108864 | tf_op jit(solution)/shard_map/pallas_call | solution.py:50
  36.0 3.1 %collective-permute-done.11.refs_7_ = bf16[96,512]{1,0:T(8,128)(2,1)S(1)} collective-permute-done((bf16[96,512]{1,0:T(8,128)(2,1)S(1)}, bf16[96,512]{1,0:T(8,128)(2,1)S(1)}, u32[]{:S(2)}, u32[]{:S(2)}) %collective-permute-start.11) | collective-permute-done | bytes 98336 | tf_op jit(solution)/shard_map/ppermute | solution.py:33
  39.2 1.9 %collective-permute-start.15 = (bf16[96,512]{1,0:T(8,128)(2,1)S(1)}, bf16[96,512]{1,0:T(8,128)(2,1)S(1)}, u32[]{:S(2)}, u32[]{:S(2)}) collective-permute-start(bf16[96,512]{1,0:T(8,128)(2,1)S(1)} %shard_map.213.refs_0_.mine), channel_id=1, source_target_pairs={{0,25},{1,24},{2,27},{3,26},{4,29},{5,28},{6,31},{7,30},{8,17},{9,... | collective-permute-start | bytes 294920 | tf_op jit(solution)/shard_map/ppermute | solution.py:381
  41.1 0.4 collective-permute-start.14
  41.5 1.0 %collective-permute-start.13 = (bf16[96,512]{1,0:T(8,128)(2,1)S(1)}, bf16[96,512]{1,0:T(8,128)(2,1)S(1)}, u32[]{:S(2)}, u32[]{:S(2)}) collective-permute-start(bf16[96,512]{1,0:T(8,128)(2,1)S(1)} %shard_map.213.refs_0_.mine), channel_id=1, source_target_pairs={{0,8},{1,9},{2,10},{3,11},{4,12},{5,13},{6,14},{7,15},{8,0},{9,1},... | collective-permute-start | bytes 294920 | tf_op jit(solution)/shard_map/ppermute | solution.py:381
  42.5 2.5 %collective-permute-done.15.refs_3_ = bf16[96,512]{1,0:T(8,128)(2,1)S(1)} collective-permute-done((bf16[96,512]{1,0:T(8,128)(2,1)S(1)}, bf16[96,512]{1,0:T(8,128)(2,1)S(1)}, u32[]{:S(2)}, u32[]{:S(2)}) %collective-permute-start.15) | collective-permute-done | bytes 98336 | tf_op jit(solution)/shard_map/ppermute | solution.py:381
  45.2 2.1 %collective-permute-done.14.refs_2_ = bf16[96,512]{1,0:T(8,128)(2,1)S(1)} collective-permute-done((bf16[96,512]{1,0:T(8,128)(2,1)S(1)}, bf16[96,512]{1,0:T(8,128)(2,1)S(1)}, u32[]{:S(2)}, u32[]{:S(2)}) %collective-permute-start.14) | collective-permute-done | bytes 98336 | tf_op jit(solution)/shard_map/ppermute | solution.py:381
  47.5 0.3 collective-permute-start.17
  47.8 0.6 shard_map.215
  48.4 1.5 %collective-permute-start.22 = (bf16[96,768]{1,0:T(8,128)(2,1)S(1)}, bf16[96,768]{1,0:T(8,128)(2,1)S(1)}, u32[]{:S(2)}, u32[]{:S(2)}) collective-permute-start(bf16[96,768]{1,0:T(8,128)(2,1)S(1)} %get-tuple-element.79), channel_id=1, source_target_pairs={{0,24},{8,16},{16,8},{24,0},{1,25},{9,17},{17,9},{25,1},{2,26},{10... | collective-permute-start | bytes 442376 | tf_op jit(solution)/shard_map/ppermute | solution.py:33
  49.9 1.0 %collective-permute-start.21 = (bf16[96,768]{1,0:T(8,128)(2,1)S(1)}, bf16[96,768]{1,0:T(8,128)(2,1)S(1)}, u32[]{:S(2)}, u32[]{:S(2)}) collective-permute-start(bf16[96,768]{1,0:T(8,128)(2,1)S(1)} %get-tuple-element.79), channel_id=1, source_target_pairs={{0,16},{8,24},{16,0},{24,8},{1,17},{9,25},{17,1},{25,9},{2,18},{10... | collective-permute-start | bytes 442376 | tf_op jit(solution)/shard_map/ppermute | solution.py:33
  51.0 1.0 %collective-permute-start.20 = (bf16[96,768]{1,0:T(8,128)(2,1)S(1)}, bf16[96,768]{1,0:T(8,128)(2,1)S(1)}, u32[]{:S(2)}, u32[]{:S(2)}) collective-permute-start(bf16[96,768]{1,0:T(8,128)(2,1)S(1)} %get-tuple-element.79), channel_id=1, source_target_pairs={{0,8},{8,0},{16,24},{24,16},{1,9},{9,1},{17,25},{25,17},{2,10},{10... | collective-permute-start | bytes 442376 | tf_op jit(solution)/shard_map/ppermute | solution.py:33
  52.0 3.9 %shard_map.214 = (bf16[96,704]{1,0:T(8,128)(2,1)S(1)}, f32[96,128]{1,0:T(8,128)S(1)}, f32[24,512]{1,0:T(8,128)S(1)}, bf16[704,4096]{1,0:T(8,128)(2,1)S(1)}) custom-call(bf16[96,512]{1,0:T(8,128)(2,1)S(1)} %shard_map.213.refs_0_.mine, bf16[96,512]{1,0:T(8,128)(2,1)S(1)} %collective-permute-done.13.refs_1_, ...), custom_call_target="tpu_custom_call" | custom-call | flops 1107296256 | tf_op jit(solution)/shard_map/pallas_call | solution.py:50
  55.8 0.3 collective-permute-done.22.refs_3_
  56.1 2.4 %collective-permute-done.21.refs_2_ = bf16[96,768]{1,0:T(8,128)(2,1)S(1)} collective-permute-done((bf16[96,768]{1,0:T(8,128)(2,1)S(1)}, bf16[96,768]{1,0:T(8,128)(2,1)S(1)}, u32[]{:S(2)}, u32[]{:S(2)}) %collective-permute-start.21) | collective-permute-done | bytes 147488 | tf_op jit(solution)/shard_map/ppermute | solution.py:33
  58.5 0.9 %shard_map.216 = (bf16[96,2048]{1,0:T(8,128)(2,1)S(1)}, bf16[96,352]{1,0:T(8,128)(2,1)S(1)}) custom-call(bf16[96,704]{1,0:T(8,128)(2,1)S(1)} %get-tuple-element.77.inner, f32[96,768]{1,0:T(8,128)S(1)} %get-tuple-element.78.refs_0_, bf16[96,768]{1,0:T(8,128)(2,1)S(1)} %collective-permute-done.20.refs_1_, bf16[96,768]{1,0:T(8,128)(2,1)S(1)} %collective-permute-done.21.refs_2_, ...), custom_call_target="tpu_custom_call" | custom-call | flops 276824064 | tf_op jit(solution)/shard_map/pallas_call | solution.py:50
  59.5 0.8 %shard_map.217.keep = f32[96,2048]{1,0:T(8,128)S(1)} custom-call(bf16[96,704]{1,0:T(8,128)(2,1)S(1)} %get-tuple-element.77.inner, bf16[96,352]{1,0:T(8,128)(2,1)S(1)} %get-tuple-element.82.refs_0_, bf16[704,4096]{1,0:T(8,128)(2,1)S(1)} %get-tuple-element.81.refs_5_.refs_1_, bf16[352,1024]{1,0:T(8,128)(2,1)S(1)} %copy-done), custom_call_target="tpu_custom_call" | custom-call | flops 276824064 | tf_op jit(solution)/shard_map/pallas_call | solution.py:50
  60.3 0.9 %collective-permute-done.23.got = bf16[96,2048]{1,0:T(8,128)(2,1)S(1)} collective-permute-done((bf16[96,2048]{1,0:T(8,128)(2,1)S(1)}, bf16[96,2048]{1,0:T(8,128)(2,1)S(1)}, u32[]{:S(2)}, u32[]{:S(2)}) %collective-permute-start.23) | collective-permute-done | bytes 393248 | tf_op jit(solution)/shard_map/ppermute | solution.py:33
  61.2 1.1 %collective-permute-start.24 = (bf16[24,2048]{1,0:T(8,128)(2,1)S(1)}, bf16[24,2048]{1,0:T(8,128)(2,1)S(1)}, u32[]{:S(2)}, u32[]{:S(2)}) collective-permute-start(bf16[24,2048]{1,0:T(8,128)(2,1)S(1)} %get-tuple-element.85), channel_id=1, source_target_pairs={{0,8},{8,0},{16,24},{24,16},{1,9},{9,1},{17,25},{25,17},{2,10},{10... | collective-permute-start | bytes 294920 | tf_op jit(solution)/shard_map/ppermute | solution.py:33
  62.3 1.0 %collective-permute-start.25 = (bf16[24,2048]{1,0:T(8,128)(2,1)S(1)}, bf16[24,2048]{1,0:T(8,128)(2,1)S(1)}, u32[]{:S(2)}, u32[]{:S(2)}) collective-permute-start(bf16[24,2048]{1,0:T(8,128)(2,1)S(1)} %get-tuple-element.86), channel_id=1, source_target_pairs={{0,16},{8,24},{16,0},{24,8},{1,17},{9,25},{17,1},{25,9},{2,18},{10... | collective-permute-start | bytes 294920 | tf_op jit(solution)/shard_map/ppermute | solution.py:33
  63.3 1.5 %collective-permute-start.26 = (bf16[24,2048]{1,0:T(8,128)(2,1)S(1)}, bf16[24,2048]{1,0:T(8,128)(2,1)S(1)}, u32[]{:S(2)}, u32[]{:S(2)}) collective-permute-start(bf16[24,2048]{1,0:T(8,128)(2,1)S(1)} %get-tuple-element.87), channel_id=1, source_target_pairs={{0,24},{8,16},{16,8},{24,0},{1,25},{9,17},{17,9},{25,1},{2,26},{10... | collective-permute-start | bytes 294920 | tf_op jit(solution)/shard_map/ppermute | solution.py:33
  64.8 1.5 %collective-permute-done.24.refs_1_ = bf16[24,2048]{1,0:T(8,128)(2,1)S(1)} collective-permute-done((bf16[24,2048]{1,0:T(8,128)(2,1)S(1)}, bf16[24,2048]{1,0:T(8,128)(2,1)S(1)}, u32[]{:S(2)}, u32[]{:S(2)}) %collective-permute-start.24) | collective-permute-done | bytes 98336 | tf_op jit(solution)/shard_map/ppermute | solution.py:33
  66.3 2.8 %collective-permute-done.25.refs_2_ = bf16[24,2048]{1,0:T(8,128)(2,1)S(1)} collective-permute-done((bf16[24,2048]{1,0:T(8,128)(2,1)S(1)}, bf16[24,2048]{1,0:T(8,128)(2,1)S(1)}, u32[]{:S(2)}, u32[]{:S(2)}) %collective-permute-start.25) | collective-permute-done | bytes 98336 | tf_op jit(solution)/shard_map/ppermute | solution.py:33
  69.1 0.9 %collective-permute-start.27 = (bf16[24,512]{1,0:T(8,128)(2,1)S(1)}, bf16[24,512]{1,0:T(8,128)(2,1)S(1)}, u32[]{:S(2)}, u32[]{:S(2)}) collective-permute-start(bf16[24,512]{1,0:T(8,128)(2,1)S(1)} %get-tuple-element.90), channel_id=1, source_target_pairs={{0,2},{1,3},{2,0},{3,1},{4,6},{5,7},{6,4},{7,5},{8,10},{9,11},{10,... | collective-permute-start | bytes 73736 | tf_op jit(solution)/shard_map/ppermute | solution.py:33
  70.0 2.2 %collective-permute-start.28 = (bf16[24,512]{1,0:T(8,128)(2,1)S(1)}, bf16[24,512]{1,0:T(8,128)(2,1)S(1)}, u32[]{:S(2)}, u32[]{:S(2)}) collective-permute-start(bf16[24,512]{1,0:T(8,128)(2,1)S(1)} %get-tuple-element.91), channel_id=1, source_target_pairs={{0,4},{1,5},{2,6},{3,7},{4,0},{5,1},{6,2},{7,3},{8,12},{9,13},{10,... | collective-permute-start | bytes 73736 | tf_op jit(solution)/shard_map/ppermute | solution.py:33
  72.2 1.4 %collective-permute-start.29 = (bf16[24,512]{1,0:T(8,128)(2,1)S(1)}, bf16[24,512]{1,0:T(8,128)(2,1)S(1)}, u32[]{:S(2)}, u32[]{:S(2)}) collective-permute-start(bf16[24,512]{1,0:T(8,128)(2,1)S(1)} %get-tuple-element.92), channel_id=1, source_target_pairs={{0,6},{1,7},{2,4},{3,5},{4,2},{5,3},{6,0},{7,1},{8,14},{9,15},{10,... | collective-permute-start | bytes 73736 | tf_op jit(solution)/shard_map/ppermute | solution.py:33
  73.6 1.4 %collective-permute-done.28.refs_2_ = bf16[24,512]{1,0:T(8,128)(2,1)S(1)} collective-permute-done((bf16[24,512]{1,0:T(8,128)(2,1)S(1)}, bf16[24,512]{1,0:T(8,128)(2,1)S(1)}, u32[]{:S(2)}, u32[]{:S(2)}) %collective-permute-start.28) | collective-permute-done | bytes 24608 | tf_op jit(solution)/shard_map/ppermute | solution.py:33
  75.0 2.9 %collective-permute-done.29.refs_3_ = bf16[24,512]{1,0:T(8,128)(2,1)S(1)} collective-permute-done((bf16[24,512]{1,0:T(8,128)(2,1)S(1)}, bf16[24,512]{1,0:T(8,128)(2,1)S(1)}, u32[]{:S(2)}, u32[]{:S(2)}) %collective-permute-start.29) | collective-permute-done | bytes 24608 | tf_op jit(solution)/shard_map/ppermute | solution.py:33
  77.9 0.6 shard_map.220
  (47 shorter events, 1.5 us)
Async XLA Ops:
  0.6 16.7 %copy-start.5 = (s32[24,2]{0,1:T(2,128)S(1)}, s32[24,2]{0,1:T(2,128)}, u32[]{:S(2)}) copy-start(s32[24,2]{0,1:T(2,128)} %param.32) | copy-start | bytes 580
  0.6 17.1 %copy-start.7 = (f32[256]{0:T(256)S(1)}, f32[256]{0:T(256)}, u32[]{:S(2)}) copy-start(f32[256]{0:T(256)} %param.27) | copy-start | bytes 3076
  0.7 17.1 %copy-start.6 = (f32[256]{0:T(256)S(1)}, f32[256]{0:T(256)}, u32[]{:S(2)}) copy-start(f32[256]{0:T(256)} %param.26) | copy-start | bytes 3076
  1.6 7.7 %collective-permute-start = (bf16[24,1024]{1,0:T(8,128)(2,1)S(1)}, bf16[24,1024]{1,0:T(8,128)(2,1)S(1)}, u32[]{:S(2)}, u32[]{:S(2)}) collective-permute-start(bf16[24,1024]{1,0:T(8,128)(2,1)S(1)} %get-tuple-element.49), channel_id=1, source_target_pairs={{0,9},{1,8},{2,11},{3,10},{4,13},{5,12},{6,15},{7,14},{8,1},{9,0},... | collective-permute-start | bytes 147464 | tf_op jit(solution)/shard_map/ppermute | solution.py:381
  4.1 5.2 %collective-permute-start.1 = (bf16[24,1024]{1,0:T(8,128)(2,1)S(1)}, bf16[24,1024]{1,0:T(8,128)(2,1)S(1)}, u32[]{:S(2)}, u32[]{:S(2)}) collective-permute-start(bf16[24,1024]{1,0:T(8,128)(2,1)S(1)} %get-tuple-element.50), channel_id=1, source_target_pairs={{0,17},{1,16},{2,19},{3,18},{4,21},{5,20},{6,23},{7,22},{8,25},{9,... | collective-permute-start | bytes 147464 | tf_op jit(solution)/shard_map/ppermute | solution.py:381
  5.9 4.9 %collective-permute-start.2 = (bf16[24,1024]{1,0:T(8,128)(2,1)S(1)}, bf16[24,1024]{1,0:T(8,128)(2,1)S(1)}, u32[]{:S(2)}, u32[]{:S(2)}) collective-permute-start(bf16[24,1024]{1,0:T(8,128)(2,1)S(1)} %get-tuple-element.51), channel_id=1, source_target_pairs={{0,25},{1,24},{2,27},{3,26},{4,29},{5,28},{6,31},{7,30},{8,17},{9,... | collective-permute-start | bytes 147464 | tf_op jit(solution)/shard_map/ppermute | solution.py:381
  11.3 14.1 %copy-start.3 = (bf16[256,1024]{1,0:T(8,128)(2,1)S(1)}, bf16[256,1024]{1,0:T(8,128)(2,1)}, u32[]{:S(2)}) copy-start(bf16[256,1024]{1,0:T(8,128)(2,1)} %refs_4_.1) | copy-start | bytes 1572868
  11.3 6.2 %collective-permute-start.3 = (bf16[24,1024]{1,0:T(8,128)(2,1)S(1)}, bf16[24,1024]{1,0:T(8,128)(2,1)S(1)}, u32[]{:S(2)}, u32[]{:S(2)}) collective-permute-start(bf16[24,1024]{1,0:T(8,128)(2,1)S(1)} %get-tuple-element.59), channel_id=1, source_target_pairs={{0,8},{8,0},{16,24},{24,16},{1,9},{9,1},{17,25},{25,17},{2,10},{10... | collective-permute-start | bytes 147464 | tf_op jit(solution)/shard_map/ppermute | solution.py:33
  11.8 5.8 %collective-permute-start.4 = (bf16[24,1024]{1,0:T(8,128)(2,1)S(1)}, bf16[24,1024]{1,0:T(8,128)(2,1)S(1)}, u32[]{:S(2)}, u32[]{:S(2)}) collective-permute-start(bf16[24,1024]{1,0:T(8,128)(2,1)S(1)} %get-tuple-element.60), channel_id=1, source_target_pairs={{0,16},{8,24},{16,0},{24,8},{1,17},{9,25},{17,1},{25,9},{2,18},{10... | collective-permute-start | bytes 147464 | tf_op jit(solution)/shard_map/ppermute | solution.py:33
  12.8 5.0 %collective-permute-start.5 = (bf16[24,1024]{1,0:T(8,128)(2,1)S(1)}, bf16[24,1024]{1,0:T(8,128)(2,1)S(1)}, u32[]{:S(2)}, u32[]{:S(2)}) collective-permute-start(bf16[24,1024]{1,0:T(8,128)(2,1)S(1)} %get-tuple-element.61), channel_id=1, source_target_pairs={{0,24},{8,16},{16,8},{24,0},{1,25},{9,17},{17,9},{25,1},{2,26},{10... | collective-permute-start | bytes 147464 | tf_op jit(solution)/shard_map/ppermute | solution.py:33
  19.0 6.3 %collective-permute-start.8 = (bf16[24,384]{1,0:T(8,128)(2,1)S(1)}, bf16[24,384]{1,0:T(8,128)(2,1)S(1)}, u32[]{:S(2)}, u32[]{:S(2)}) collective-permute-start(bf16[24,384]{1,0:T(8,128)(2,1)S(1)} %get-tuple-element.68.refs_0_.refs_8_), channel_id=1, source_target_pairs={{0,24},{8,16},{16,8},{24,0},{1,25},{9,17},{17,9},{25,1},{2,26},{10... | collective-permute-start | bytes 55304 | tf_op jit(solution)/shard_map/ppermute | solution.py:33
  21.1 4.2 %collective-permute-start.7 = (bf16[24,384]{1,0:T(8,128)(2,1)S(1)}, bf16[24,384]{1,0:T(8,128)(2,1)S(1)}, u32[]{:S(2)}, u32[]{:S(2)}) collective-permute-start(bf16[24,384]{1,0:T(8,128)(2,1)S(1)} %get-tuple-element.68.refs_0_.refs_8_), channel_id=1, source_target_pairs={{0,16},{8,24},{16,0},{24,8},{1,17},{9,25},{17,1},{25,9},{2,18},{10... | collective-permute-start | bytes 55304 | tf_op jit(solution)/shard_map/ppermute | solution.py:33
  21.6 3.8 %collective-permute-start.6 = (bf16[24,384]{1,0:T(8,128)(2,1)S(1)}, bf16[24,384]{1,0:T(8,128)(2,1)S(1)}, u32[]{:S(2)}, u32[]{:S(2)}) collective-permute-start(bf16[24,384]{1,0:T(8,128)(2,1)S(1)} %get-tuple-element.68.refs_0_.refs_8_), channel_id=1, source_target_pairs={{0,8},{8,0},{16,24},{24,16},{1,9},{9,1},{17,25},{25,17},{2,10},{10... | collective-permute-start | bytes 55304 | tf_op jit(solution)/shard_map/ppermute | solution.py:33
  25.5 1.4 %collective-permute-start.9 = (bf16[96,512]{1,0:T(8,128)(2,1)S(1)}, bf16[96,512]{1,0:T(8,128)(2,1)S(1)}, u32[]{:S(2)}, u32[]{:S(2)}) collective-permute-start(bf16[96,512]{1,0:T(8,128)(2,1)S(1)} %get-tuple-element.72), channel_id=1, source_target_pairs={{0,1},{1,0},{2,3},{3,2},{4,5},{5,4},{6,7},{7,6},{8,9},{9,8},{10,11... | collective-permute-start | bytes 294920 | tf_op jit(solution)/shard_map/ppermute | solution.py:33
  26.9 9.1 %collective-permute-start.12 = (bf16[96,512]{1,0:T(8,128)(2,1)S(1)}, bf16[96,512]{1,0:T(8,128)(2,1)S(1)}, u32[]{:S(2)}, u32[]{:S(2)}) collective-permute-start(bf16[96,512]{1,0:T(8,128)(2,1)S(1)} %shard_map.211.refs_2_), channel_id=1, source_target_pairs={{0,7},{1,6},{2,5},{3,4},{4,3},{5,2},{6,1},{7,0},{8,15},{9,14},{10,... | collective-permute-start | bytes 294920 | tf_op jit(solution)/shard_map/ppermute | solution.py:33
  30.4 8.7 %collective-permute-start.11 = (bf16[96,512]{1,0:T(8,128)(2,1)S(1)}, bf16[96,512]{1,0:T(8,128)(2,1)S(1)}, u32[]{:S(2)}, u32[]{:S(2)}) collective-permute-start(bf16[96,512]{1,0:T(8,128)(2,1)S(1)} %shard_map.211.refs_2_), channel_id=1, source_target_pairs={{0,5},{1,4},{2,7},{3,6},{4,1},{5,0},{6,3},{7,2},{8,13},{9,12},{10,... | collective-permute-start | bytes 294920 | tf_op jit(solution)/shard_map/ppermute | solution.py:33
  30.4 8.7 %collective-permute-start.10 = (bf16[96,512]{1,0:T(8,128)(2,1)S(1)}, bf16[96,512]{1,0:T(8,128)(2,1)S(1)}, u32[]{:S(2)}, u32[]{:S(2)}) collective-permute-start(bf16[96,512]{1,0:T(8,128)(2,1)S(1)} %shard_map.211.refs_2_), channel_id=1, source_target_pairs={{0,2},{1,3},{2,0},{3,1},{4,6},{5,7},{6,4},{7,5},{8,10},{9,11},{10,... | collective-permute-start | bytes 294920 | tf_op jit(solution)/shard_map/ppermute | solution.py:33
  31.1 16.7 %copy-start.1 = (bf16[1024,352]{0,1:T(8,128)(2,1)S(1)}, bf16[1024,352]{0,1:T(8,128)(2,1)}, u32[]{:S(2)}) copy-start(bf16[1024,352]{0,1:T(8,128)(2,1)} %param.36) | copy-start | bytes 2162692
  31.1 16.7 %copy-start.2 = (bf16[1024,352]{0,1:T(8,128)(2,1)S(1)}, bf16[1024,352]{0,1:T(8,128)(2,1)}, u32[]{:S(2)}) copy-start(bf16[1024,352]{0,1:T(8,128)(2,1)} %param.37) | copy-start | bytes 2162692
  31.1 16.7 %copy-start.4 = (f32[4096]{0:T(1024)S(1)}, f32[4096]{0:T(1024)}, u32[]{:S(2)}) copy-start(f32[4096]{0:T(1024)} %param.30) | copy-start | bytes 49156
  39.2 5.8 %collective-permute-start.15 = (bf16[96,512]{1,0:T(8,128)(2,1)S(1)}, bf16[96,512]{1,0:T(8,128)(2,1)S(1)}, u32[]{:S(2)}, u32[]{:S(2)}) collective-permute-start(bf16[96,512]{1,0:T(8,128)(2,1)S(1)} %shard_map.213.refs_0_.mine), channel_id=1, source_target_pairs={{0,25},{1,24},{2,27},{3,26},{4,29},{5,28},{6,31},{7,30},{8,17},{9,... | collective-permute-start | bytes 294920 | tf_op jit(solution)/shard_map/ppermute | solution.py:381
  41.1 6.2 %collective-permute-start.14 = (bf16[96,512]{1,0:T(8,128)(2,1)S(1)}, bf16[96,512]{1,0:T(8,128)(2,1)S(1)}, u32[]{:S(2)}, u32[]{:S(2)}) collective-permute-start(bf16[96,512]{1,0:T(8,128)(2,1)S(1)} %shard_map.213.refs_0_.mine), channel_id=1, source_target_pairs={{0,17},{1,16},{2,19},{3,18},{4,21},{5,20},{6,23},{7,22},{8,25},{9,... | collective-permute-start | bytes 294920 | tf_op jit(solution)/shard_map/ppermute | solution.py:381
  41.5 6.0 %collective-permute-start.13 = (bf16[96,512]{1,0:T(8,128)(2,1)S(1)}, bf16[96,512]{1,0:T(8,128)(2,1)S(1)}, u32[]{:S(2)}, u32[]{:S(2)}) collective-permute-start(bf16[96,512]{1,0:T(8,128)(2,1)S(1)} %shard_map.213.refs_0_.mine), channel_id=1, source_target_pairs={{0,8},{1,9},{2,10},{3,11},{4,12},{5,13},{6,14},{7,15},{8,0},{9,1},... | collective-permute-start | bytes 294920 | tf_op jit(solution)/shard_map/ppermute | solution.py:381
  42.5 5.4 %collective-permute-start.16 = (bf16[96,512]{1,0:T(8,128)(2,1)S(1)}, bf16[96,512]{1,0:T(8,128)(2,1)S(1)}, u32[]{:S(2)}, u32[]{:S(2)}) collective-permute-start(bf16[96,512]{1,0:T(8,128)(2,1)S(1)} %shard_map.213.refs_0_.mine), channel_id=1, source_target_pairs={{0,1},{1,0},{2,3},{3,2},{4,5},{5,4},{6,7},{7,6},{8,9},{9,8},{10,11... | collective-permute-start | bytes 294920 | tf_op jit(solution)/shard_map/ppermute | solution.py:33
  45.0 6.0 %collective-permute-start.19 = (bf16[96,512]{1,0:T(8,128)(2,1)S(1)}, bf16[96,512]{1,0:T(8,128)(2,1)S(1)}, u32[]{:S(2)}, u32[]{:S(2)}) collective-permute-start(bf16[96,512]{1,0:T(8,128)(2,1)S(1)} %collective-permute-done.15.refs_3_), channel_id=1, source_target_pairs={{0,1},{1,0},{2,3},{3,2},{4,5},{5,4},{6,7},{7,6},{8,9},{9,8},{10,11... | collective-permute-start | bytes 294920 | tf_op jit(solution)/shard_map/ppermute | solution.py:33
  47.3 4.7 %collective-permute-start.18 = (bf16[96,512]{1,0:T(8,128)(2,1)S(1)}, bf16[96,512]{1,0:T(8,128)(2,1)S(1)}, u32[]{:S(2)}, u32[]{:S(2)}) collective-permute-start(bf16[96,512]{1,0:T(8,128)(2,1)S(1)} %collective-permute-done.14.refs_2_), channel_id=1, source_target_pairs={{0,1},{1,0},{2,3},{3,2},{4,5},{5,4},{6,7},{7,6},{8,9},{9,8},{10,11... | collective-permute-start | bytes 294920 | tf_op jit(solution)/shard_map/ppermute | solution.py:33
  47.5 4.5 %collective-permute-start.17 = (bf16[96,512]{1,0:T(8,128)(2,1)S(1)}, bf16[96,512]{1,0:T(8,128)(2,1)S(1)}, u32[]{:S(2)}, u32[]{:S(2)}) collective-permute-start(bf16[96,512]{1,0:T(8,128)(2,1)S(1)} %collective-permute-done.13.refs_1_), channel_id=1, source_target_pairs={{0,1},{1,0},{2,3},{3,2},{4,5},{5,4},{6,7},{7,6},{8,9},{9,8},{10,11... | collective-permute-start | bytes 294920 | tf_op jit(solution)/shard_map/ppermute | solution.py:33
  48.4 7.7 %collective-permute-start.22 = (bf16[96,768]{1,0:T(8,128)(2,1)S(1)}, bf16[96,768]{1,0:T(8,128)(2,1)S(1)}, u32[]{:S(2)}, u32[]{:S(2)}) collective-permute-start(bf16[96,768]{1,0:T(8,128)(2,1)S(1)} %get-tuple-element.79), channel_id=1, source_target_pairs={{0,24},{8,16},{16,8},{24,0},{1,25},{9,17},{17,9},{25,1},{2,26},{10... | collective-permute-start | bytes 442376 | tf_op jit(solution)/shard_map/ppermute | solution.py:33
  49.9 8.5 %collective-permute-start.21 = (bf16[96,768]{1,0:T(8,128)(2,1)S(1)}, bf16[96,768]{1,0:T(8,128)(2,1)S(1)}, u32[]{:S(2)}, u32[]{:S(2)}) collective-permute-start(bf16[96,768]{1,0:T(8,128)(2,1)S(1)} %get-tuple-element.79), channel_id=1, source_target_pairs={{0,16},{8,24},{16,0},{24,8},{1,17},{9,25},{17,1},{25,9},{2,18},{10... | collective-permute-start | bytes 442376 | tf_op jit(solution)/shard_map/ppermute | solution.py:33
  51.0 7.5 %collective-permute-start.20 = (bf16[96,768]{1,0:T(8,128)(2,1)S(1)}, bf16[96,768]{1,0:T(8,128)(2,1)S(1)}, u32[]{:S(2)}, u32[]{:S(2)}) collective-permute-start(bf16[96,768]{1,0:T(8,128)(2,1)S(1)} %get-tuple-element.79), channel_id=1, source_target_pairs={{0,8},{8,0},{16,24},{24,16},{1,9},{9,1},{17,25},{25,17},{2,10},{10... | collective-permute-start | bytes 442376 | tf_op jit(solution)/shard_map/ppermute | solution.py:33
  52.0 6.5 %copy-start = (bf16[352,1024]{1,0:T(8,128)(2,1)S(1)}, bf16[352,1024]{1,0:T(8,128)(2,1)}, u32[]{:S(2)}) copy-start(bf16[352,1024]{1,0:T(8,128)(2,1)} %refs_2_.3) | copy-start | bytes 2162692
  59.4 1.8 %collective-permute-start.23 = (bf16[96,2048]{1,0:T(8,128)(2,1)S(1)}, bf16[96,2048]{1,0:T(8,128)(2,1)S(1)}, u32[]{:S(2)}, u32[]{:S(2)}) collective-permute-start(bf16[96,2048]{1,0:T(8,128)(2,1)S(1)} %get-tuple-element.83), channel_id=1, source_target_pairs={{0,1},{1,0},{2,3},{3,2},{4,5},{5,4},{6,7},{7,6},{8,9},{9,8},{10,11... | collective-permute-start | bytes 1179656 | tf_op jit(solution)/shard_map/ppermute | solution.py:33
  61.2 5.1 %collective-permute-start.24 = (bf16[24,2048]{1,0:T(8,128)(2,1)S(1)}, bf16[24,2048]{1,0:T(8,128)(2,1)S(1)}, u32[]{:S(2)}, u32[]{:S(2)}) collective-permute-start(bf16[24,2048]{1,0:T(8,128)(2,1)S(1)} %get-tuple-element.85), channel_id=1, source_target_pairs={{0,8},{8,0},{16,24},{24,16},{1,9},{9,1},{17,25},{25,17},{2,10},{10... | collective-permute-start | bytes 294920 | tf_op jit(solution)/shard_map/ppermute | solution.py:33
  62.3 6.7 %collective-permute-start.25 = (bf16[24,2048]{1,0:T(8,128)(2,1)S(1)}, bf16[24,2048]{1,0:T(8,128)(2,1)S(1)}, u32[]{:S(2)}, u32[]{:S(2)}) collective-permute-start(bf16[24,2048]{1,0:T(8,128)(2,1)S(1)} %get-tuple-element.86), channel_id=1, source_target_pairs={{0,16},{8,24},{16,0},{24,8},{1,17},{9,25},{17,1},{25,9},{2,18},{10... | collective-permute-start | bytes 294920 | tf_op jit(solution)/shard_map/ppermute | solution.py:33
  63.3 5.8 %collective-permute-start.26 = (bf16[24,2048]{1,0:T(8,128)(2,1)S(1)}, bf16[24,2048]{1,0:T(8,128)(2,1)S(1)}, u32[]{:S(2)}, u32[]{:S(2)}) collective-permute-start(bf16[24,2048]{1,0:T(8,128)(2,1)S(1)} %get-tuple-element.87), channel_id=1, source_target_pairs={{0,24},{8,16},{16,8},{24,0},{1,25},{9,17},{17,9},{25,1},{2,26},{10... | collective-permute-start | bytes 294920 | tf_op jit(solution)/shard_map/ppermute | solution.py:33
  69.1 4.5 %collective-permute-start.27 = (bf16[24,512]{1,0:T(8,128)(2,1)S(1)}, bf16[24,512]{1,0:T(8,128)(2,1)S(1)}, u32[]{:S(2)}, u32[]{:S(2)}) collective-permute-start(bf16[24,512]{1,0:T(8,128)(2,1)S(1)} %get-tuple-element.90), channel_id=1, source_target_pairs={{0,2},{1,3},{2,0},{3,1},{4,6},{5,7},{6,4},{7,5},{8,10},{9,11},{10,... | collective-permute-start | bytes 73736 | tf_op jit(solution)/shard_map/ppermute | solution.py:33
  70.0 5.0 %collective-permute-start.28 = (bf16[24,512]{1,0:T(8,128)(2,1)S(1)}, bf16[24,512]{1,0:T(8,128)(2,1)S(1)}, u32[]{:S(2)}, u32[]{:S(2)}) collective-permute-start(bf16[24,512]{1,0:T(8,128)(2,1)S(1)} %get-tuple-element.91), channel_id=1, source_target_pairs={{0,4},{1,5},{2,6},{3,7},{4,0},{5,1},{6,2},{7,3},{8,12},{9,13},{10,... | collective-permute-start | bytes 73736 | tf_op jit(solution)/shard_map/ppermute | solution.py:33
  72.2 5.6 %collective-permute-start.29 = (bf16[24,512]{1,0:T(8,128)(2,1)S(1)}, bf16[24,512]{1,0:T(8,128)(2,1)S(1)}, u32[]{:S(2)}, u32[]{:S(2)}) collective-permute-start(bf16[24,512]{1,0:T(8,128)(2,1)S(1)} %get-tuple-element.92), channel_id=1, source_target_pairs={{0,6},{1,7},{2,4},{3,5},{4,2},{5,3},{6,0},{7,1},{8,14},{9,15},{10,... | collective-permute-start | bytes 73736 | tf_op jit(solution)/shard_map/ppermute | solution.py:33

commit v3 on v2

--- a/solution.py
+++ b/solution.py
@@ -183,7 +183,7 @@
         mixed[:, lanes] = (read * inverse_rms(read) * scale[:, lanes]).astype(BF16)
 
 
-def update_kernel(group, gates, state, out, token, buffer, sems):
+def update_kernel(group, gates, state, _, out, token, buffer, sems):
     batch, heads, size = state.shape[:3]
     channels = heads * size
     forget = columns_of(gates[:, :channels])
@@ -349,7 +349,7 @@
 
 def gather_kernel(n_ep, n_z, *refs):
     own, got = refs[0], refs[1:n_ep]
-    hidden, base, sent, scratch = refs[n_ep], refs[n_ep + 1], refs[n_ep + 2 : -1], refs[-1]
+    hidden, base, sent, scratch = refs[n_ep], refs[n_ep + 2], refs[n_ep + 3 : -1], refs[-1]
     z = lax.div(lax.axis_index("tp"), 2)
     size = base.shape[1]
     total = own[...]
@@ -448,28 +448,11 @@
         )
         mixed_all = [mixed] + [ep_swap(mixed, k) for k in others]
 
-        group = 4
-        new_state, token = pl.pallas_call(
-            functools.partial(update_kernel, group),
-            out_shape=[
-                jax.ShapeDtypeStruct(recurrent_state.shape, F32),
-                jax.ShapeDtypeStruct((8, LANES), F32),
-            ],
-            in_specs=[VMEM] * 2,
-            out_specs=[HBM, VMEM],
-            scratch_shapes=[
-                pltpu.VMEM(recurrent_state.shape, F32),
-                pltpu.SemaphoreType.DMA((batch // group,)),
-            ],
-            cost_estimate=pl.CostEstimate(flops=1 << 26, bytes_accessed=0, transcendentals=0),
-            compiler_params=pltpu.CompilerParams(vmem_limit_bytes=16 << 20),
-        )(gates, state)
-
         give, keep = call(
             functools.partial(output_kernel, n_ep),
             [((rows, half), BF16), ((rows, half), F32)],
-            [VMEM] * (n_ep + 2),
-            (*mixed_all, w_output, token),
+            [VMEM] * (n_ep + 1),
+            (*mixed_all, w_output),
             flops=2 * rows * channels * block,
         )
         core = core_swap(give)
@@ -544,11 +527,27 @@
             (keep, core),
         )
         got = [ep_swap(sent[k - 1], k) for k in others]
+        group = 4
+        new_state, token = pl.pallas_call(
+            functools.partial(update_kernel, group),
+            out_shape=[
+                jax.ShapeDtypeStruct(recurrent_state.shape, F32),
+                jax.ShapeDtypeStruct((8, LANES), F32),
+            ],
+            in_specs=[VMEM] * 3,
+            out_specs=[HBM, VMEM],
+            scratch_shapes=[
+                pltpu.VMEM(recurrent_state.shape, F32),
+                pltpu.SemaphoreType.DMA((batch // group,)),
+            ],
+            cost_estimate=pl.CostEstimate(flops=1 << 26, bytes_accessed=0, transcendentals=0),
+            compiler_params=pltpu.CompilerParams(vmem_limit_bytes=16 << 20),
+        )(gates, state, own)
         base, *sent = call(
             functools.partial(gather_kernel, n_ep, n_z),
             [((batch, slice_width), F32)] + [((batch, slice_width), BF16)] * (n_z - 1),
-            [VMEM] * (n_ep + 1),
-            (own, *got, own_hidden),
+            [VMEM] * (n_ep + 2),
+            (own, *got, own_hidden, token),
             [pltpu.VMEM((batch, side), F32)],
         )
         got = [z_swap(sent[m - 1], m) for m in range(1, n_z)]

time: 78.7 us -> 78.6 us (level)
  transfers between devices with their start and end apart: 30 -> 30, of which waited for: 13 -> 15; matrix products, arithmetic and copies ran while one was open for 1% -> 1% of each run, Pallas kernels for 23% -> 23%
where the time goes in v3:
time: 78.6 us; the launch traced here: 78.4 us
  starting transfers between devices  31.4 us (40%)
  Pallas kernels  22.8 us (29%)
  waiting for transfers between devices  22.6 us (29%)
  between operations  0.87 us (1%)
    ppermute x24, starting transfers between devices, swap(): return lax.ppermute(value, axis, [(s, s ^ step) for s in range(size)])  23.9 us
    pallas_call x17, Pallas kernels, call(): pl.pallas_call(body, out_shape=[jax.ShapeDtypeStruct(s, d) for s, d in ou...  20.1 us
    ppermute x24, waiting for transfers between devices, swap(): return lax.ppermute(value, axis, [(s, s ^ step) for s in range(size)])  16.7 us
    ppermute x6, starting transfers between devices, cross_swap(): return lax.ppermute(value, ('ep', 'tp'), pairs)  7.57 us
    ppermute x6, waiting for transfers between devices, cross_swap(): return lax.ppermute(value, ('ep', 'tp'), pairs)  5.92 us
    pallas_call x1, Pallas kernels, body(): pl.pallas_call(functools.partial(update_kernel, group), out_shape=[jax.Sh...  2.69 us
  transfers between devices with their start and end apart: 30, of which 15 were waited for; matrix products, arithmetic and copies ran while one was open for 1% of the time, Pallas kernels for 23%

profile of v3, /device:TPU:0, one launch (start us, length us, event | category | flops | bytes accessed | tf_op | source)
XLA Modules:
  0.0 78.4 jit_solution(10927510902177334372)
XLA Ops:
  0.7 0.9 %shard_map.203 = (bf16[24,1024]{1,0:T(8,128)(2,1)S(1)}, bf16[24,1024]{1,0:T(8,128)(2,1)S(1)}, bf16[24,1024]{1,0:T(8,128)(2,1)S(1)}, bf16[24,1024]{1,0:T(8,128)(2,1)S(1)}) custom-call(bf16[24,4096]{1,0:T(8,128)(2,1)} %refs_1_.3), custom_call_target="tpu_custom_call" | custom-call | tf_op jit(solution)/shard_map/pallas_call | solution.py:50
  1.6 2.5 %collective-permute-start = (bf16[24,1024]{1,0:T(8,128)(2,1)S(1)}, bf16[24,1024]{1,0:T(8,128)(2,1)S(1)}, u32[]{:S(2)}, u32[]{:S(2)}) collective-permute-start(bf16[24,1024]{1,0:T(8,128)(2,1)S(1)} %get-tuple-element.49), channel_id=1, source_target_pairs={{0,9},{1,8},{2,11},{3,10},{4,13},{5,12},{6,15},{7,14},{8,1},{9,0},... | collective-permute-start | bytes 147464 | tf_op jit(solution)/shard_map/ppermute | solution.py:381
  4.1 1.8 %collective-permute-start.1 = (bf16[24,1024]{1,0:T(8,128)(2,1)S(1)}, bf16[24,1024]{1,0:T(8,128)(2,1)S(1)}, u32[]{:S(2)}, u32[]{:S(2)}) collective-permute-start(bf16[24,1024]{1,0:T(8,128)(2,1)S(1)} %get-tuple-element.50), channel_id=1, source_target_pairs={{0,17},{1,16},{2,19},{3,18},{4,21},{5,20},{6,23},{7,22},{8,25},{9,... | collective-permute-start | bytes 147464 | tf_op jit(solution)/shard_map/ppermute | solution.py:381
  5.9 0.7 broadcast_in_dim.17.refs_6_.branch
  6.6 2.7 %shard_map.204 = (bf16[1024,256]{1,0:T(8,128)(2,1)S(1)}, bf16[1024,256]{1,0:T(8,128)(2,1)S(1)}, bf16[1024,256]{1,0:T(8,128)(2,1)S(1)}, bf16[1024,256]{1,0:T(8,12...) custom-call(bf16[1024,256]{1,0:T(8,128)(2,1)} %refs_0_.2, bf16[1024,256]{1,0:T(8,128)(2,1)} %refs_1_.2, ...), custom_call_target="tpu_custom_call" | custom-call | flops 67108864 | tf_op jit(solution)/shard_map/pallas_call | solution.py:50
  9.4 1.4 %collective-permute-done.2.refs_3_ = bf16[24,1024]{1,0:T(8,128)(2,1)S(1)} collective-permute-done((bf16[24,1024]{1,0:T(8,128)(2,1)S(1)}, bf16[24,1024]{1,0:T(8,128)(2,1)S(1)}, u32[]{:S(2)}, u32[]{:S(2)}) %collective-permute-start.2) | collective-permute-done | bytes 49184 | tf_op jit(solution)/shard_map/ppermute | solution.py:381
  10.8 0.5 shard_map.205
  11.3 0.5 collective-permute-start.3
  11.8 1.1 %collective-permute-start.4 = (bf16[24,1024]{1,0:T(8,128)(2,1)S(1)}, bf16[24,1024]{1,0:T(8,128)(2,1)S(1)}, u32[]{:S(2)}, u32[]{:S(2)}) collective-permute-start(bf16[24,1024]{1,0:T(8,128)(2,1)S(1)} %get-tuple-element.60), channel_id=1, source_target_pairs={{0,16},{8,24},{16,0},{24,8},{1,17},{9,25},{17,1},{25,9},{2,18},{10... | collective-permute-start | bytes 147464 | tf_op jit(solution)/shard_map/ppermute | solution.py:33
  12.8 2.0 %collective-permute-start.5 = (bf16[24,1024]{1,0:T(8,128)(2,1)S(1)}, bf16[24,1024]{1,0:T(8,128)(2,1)S(1)}, u32[]{:S(2)}, u32[]{:S(2)}) collective-permute-start(bf16[24,1024]{1,0:T(8,128)(2,1)S(1)} %get-tuple-element.61), channel_id=1, source_target_pairs={{0,24},{8,16},{16,8},{24,0},{1,25},{9,17},{17,9},{25,1},{2,26},{10... | collective-permute-start | bytes 147464 | tf_op jit(solution)/shard_map/ppermute | solution.py:33
  14.8 2.5 %shard_map.206 = (f32[24,2,128,128]{3,2,1,0:T(8,128)S(1)}, bf16[24,4096]{1,0:T(8,128)(2,1)S(1)}, bf16[8,4096]{1,0:T(8,128)(2,1)S(1)}, f32[8,128]{1,0:T(8,128)S(1)}) custom-call(f32[24,2,128,128]{3,2,1,0:T(8,128)} %refs_0_.3, bf16[24,4096]{1,0:T(8,128)(2,1)} %refs_1_.3, bf16[8,4096]{1,0:T(8,128)(2,1)} %bitcast.19, ...), custom_call_target="tpu_custom_call" | custom-call | flops 67108864 | tf_op jit(solution)/shard_map/pallas_call | solution.py:50
  17.8 1.2 %shard_map.208 = (bf16[24,384]{1,0:T(8,128)(2,1)S(1)}, f32[24,768]{1,0:T(8,128)S(1)}) custom-call(f32[24,1024]{1,0:T(8,128)S(1)} %get-tuple-element.58.refs_3_.refs_0_, bf16[24,1024]{1,0:T(8,128)(2,1)S(1)} %collective-permute-done.3.refs_1_, bf16[24,1024]{1,0:T(8,128)(2,1)S(1)} %collective-permute-done.4.refs_2_, ...), custom_call_target="tpu_custom_call" | custom-call | flops 16777216 | tf_op jit(solution)/shard_map/pallas_call | solution.py:50
  19.0 2.1 %collective-permute-start.8 = (bf16[24,384]{1,0:T(8,128)(2,1)S(1)}, bf16[24,384]{1,0:T(8,128)(2,1)S(1)}, u32[]{:S(2)}, u32[]{:S(2)}) collective-permute-start(bf16[24,384]{1,0:T(8,128)(2,1)S(1)} %get-tuple-element.68.refs_0_.refs_8_), channel_id=1, source_target_pairs={{0,24},{8,16},{16,8},{24,0},{1,25},{9,17},{17,9},{25,1},{2,26},{10... | collective-permute-start | bytes 55304 | tf_op jit(solution)/shard_map/ppermute | solution.py:33
  21.1 0.5 collective-permute-start.7
  21.5 1.0 %collective-permute-start.6 = (bf16[24,384]{1,0:T(8,128)(2,1)S(1)}, bf16[24,384]{1,0:T(8,128)(2,1)S(1)}, u32[]{:S(2)}, u32[]{:S(2)}) collective-permute-start(bf16[24,384]{1,0:T(8,128)(2,1)S(1)} %get-tuple-element.68.refs_0_.refs_8_), channel_id=1, source_target_pairs={{0,8},{8,0},{16,24},{24,16},{1,9},{9,1},{17,25},{25,17},{2,10},{10... | collective-permute-start | bytes 55304 | tf_op jit(solution)/shard_map/ppermute | solution.py:33
  22.6 1.2 %collective-permute-done.8.refs_3_.refs_11_ = bf16[24,384]{1,0:T(8,128)(2,1)S(1)} collective-permute-done((bf16[24,384]{1,0:T(8,128)(2,1)S(1)}, bf16[24,384]{1,0:T(8,128)(2,1)S(1)}, u32[]{:S(2)}, u32[]{:S(2)}) %collective-permute-start.8) | collective-permute-done | bytes 18464 | tf_op jit(solution)/shard_map/ppermute | solution.py:33
  23.7 1.1 %collective-permute-done.7.refs_2_.refs_10_ = bf16[24,384]{1,0:T(8,128)(2,1)S(1)} collective-permute-done((bf16[24,384]{1,0:T(8,128)(2,1)S(1)}, bf16[24,384]{1,0:T(8,128)(2,1)S(1)}, u32[]{:S(2)}, u32[]{:S(2)}) %collective-permute-start.7) | collective-permute-done | bytes 18464 | tf_op jit(solution)/shard_map/ppermute | solution.py:33
  24.8 0.5 collective-permute-done.6.refs_1_.refs_9_
  25.6 1.3 %collective-permute-done.9.got.refs_5_ = bf16[96,512]{1,0:T(8,128)(2,1)S(1)} collective-permute-done((bf16[96,512]{1,0:T(8,128)(2,1)S(1)}, bf16[96,512]{1,0:T(8,128)(2,1)S(1)}, u32[]{:S(2)}, u32[]{:S(2)}) %collective-permute-start.9) | collective-permute-done | bytes 98336 | tf_op jit(solution)/shard_map/ppermute | solution.py:33
  26.9 3.4 %collective-permute-start.12 = (bf16[96,512]{1,0:T(8,128)(2,1)S(1)}, bf16[96,512]{1,0:T(8,128)(2,1)S(1)}, u32[]{:S(2)}, u32[]{:S(2)}) collective-permute-start(bf16[96,512]{1,0:T(8,128)(2,1)S(1)} %shard_map.210.refs_2_), channel_id=1, source_target_pairs={{0,7},{1,6},{2,5},{3,4},{4,3},{5,2},{6,1},{7,0},{8,15},{9,14},{10,... | collective-permute-start | bytes 294920 | tf_op jit(solution)/shard_map/ppermute | solution.py:33
  30.3 0.7 collective-permute-start.10
  31.1 4.9 %shard_map.211 = (bf16[2,352,4096]{2,1,0:T(8,128)(2,1)S(1)}, bf16[2,352,4096]{2,1,0:T(8,128)(2,1)S(1)}, f32[8,128]{1,0:T(8,128)S(1)}) custom-call(bf16[2,352,4096]{2,1,0:T(8,128)(2,1)} %bitcast.17, bf16[2,352,4096]{2,1,0:T(8,128)(2,1)} %bitcast.18, bf16[96,512]{1,0:T(8,128)(2,1)S(1)} %shard_map.210.refs_2_), custom_call_target="tpu_custom_call" | custom-call | flops 67108864 | tf_op jit(solution)/shard_map/pallas_call | solution.py:50
  36.0 3.1 %collective-permute-done.11.refs_7_ = bf16[96,512]{1,0:T(8,128)(2,1)S(1)} collective-permute-done((bf16[96,512]{1,0:T(8,128)(2,1)S(1)}, bf16[96,512]{1,0:T(8,128)(2,1)S(1)}, u32[]{:S(2)}, u32[]{:S(2)}) %collective-permute-start.11) | collective-permute-done | bytes 98336 | tf_op jit(solution)/shard_map/ppermute | solution.py:33
  39.2 1.3 %collective-permute-start.15 = (bf16[96,512]{1,0:T(8,128)(2,1)S(1)}, bf16[96,512]{1,0:T(8,128)(2,1)S(1)}, u32[]{:S(2)}, u32[]{:S(2)}) collective-permute-start(bf16[96,512]{1,0:T(8,128)(2,1)S(1)} %shard_map.212.refs_0_.mine), channel_id=1, source_target_pairs={{0,25},{1,24},{2,27},{3,26},{4,29},{5,28},{6,31},{7,30},{8,17},{9,... | collective-permute-start | bytes 294920 | tf_op jit(solution)/shard_map/ppermute | solution.py:381
  40.4 1.0 %collective-permute-start.14 = (bf16[96,512]{1,0:T(8,128)(2,1)S(1)}, bf16[96,512]{1,0:T(8,128)(2,1)S(1)}, u32[]{:S(2)}, u32[]{:S(2)}) collective-permute-start(bf16[96,512]{1,0:T(8,128)(2,1)S(1)} %shard_map.212.refs_0_.mine), channel_id=1, source_target_pairs={{0,17},{1,16},{2,19},{3,18},{4,21},{5,20},{6,23},{7,22},{8,25},{9,... | collective-permute-start | bytes 294920 | tf_op jit(solution)/shard_map/ppermute | solution.py:381
  41.4 1.0 %collective-permute-start.13 = (bf16[96,512]{1,0:T(8,128)(2,1)S(1)}, bf16[96,512]{1,0:T(8,128)(2,1)S(1)}, u32[]{:S(2)}, u32[]{:S(2)}) collective-permute-start(bf16[96,512]{1,0:T(8,128)(2,1)S(1)} %shard_map.212.refs_0_.mine), channel_id=1, source_target_pairs={{0,8},{1,9},{2,10},{3,11},{4,12},{5,13},{6,14},{7,15},{8,0},{9,1},... | collective-permute-start | bytes 294920 | tf_op jit(solution)/shard_map/ppermute | solution.py:381
  42.4 2.5 %collective-permute-done.15.refs_3_ = bf16[96,512]{1,0:T(8,128)(2,1)S(1)} collective-permute-done((bf16[96,512]{1,0:T(8,128)(2,1)S(1)}, bf16[96,512]{1,0:T(8,128)(2,1)S(1)}, u32[]{:S(2)}, u32[]{:S(2)}) %collective-permute-start.15) | collective-permute-done | bytes 98336 | tf_op jit(solution)/shard_map/ppermute | solution.py:381
  45.4 1.9 %collective-permute-done.14.refs_2_ = bf16[96,512]{1,0:T(8,128)(2,1)S(1)} collective-permute-done((bf16[96,512]{1,0:T(8,128)(2,1)S(1)}, bf16[96,512]{1,0:T(8,128)(2,1)S(1)}, u32[]{:S(2)}, u32[]{:S(2)}) %collective-permute-start.14) | collective-permute-done | bytes 98336 | tf_op jit(solution)/shard_map/ppermute | solution.py:381
  47.8 0.6 shard_map.214
  48.4 1.5 %collective-permute-start.22 = (bf16[96,768]{1,0:T(8,128)(2,1)S(1)}, bf16[96,768]{1,0:T(8,128)(2,1)S(1)}, u32[]{:S(2)}, u32[]{:S(2)}) collective-permute-start(bf16[96,768]{1,0:T(8,128)(2,1)S(1)} %get-tuple-element.77), channel_id=1, source_target_pairs={{0,24},{8,16},{16,8},{24,0},{1,25},{9,17},{17,9},{25,1},{2,26},{10... | collective-permute-start | bytes 442376 | tf_op jit(solution)/shard_map/ppermute | solution.py:33
  49.9 1.1 %collective-permute-start.21 = (bf16[96,768]{1,0:T(8,128)(2,1)S(1)}, bf16[96,768]{1,0:T(8,128)(2,1)S(1)}, u32[]{:S(2)}, u32[]{:S(2)}) collective-permute-start(bf16[96,768]{1,0:T(8,128)(2,1)S(1)} %get-tuple-element.77), channel_id=1, source_target_pairs={{0,16},{8,24},{16,0},{24,8},{1,17},{9,25},{17,1},{25,9},{2,18},{10... | collective-permute-start | bytes 442376 | tf_op jit(solution)/shard_map/ppermute | solution.py:33
  51.0 1.0 %collective-permute-start.20 = (bf16[96,768]{1,0:T(8,128)(2,1)S(1)}, bf16[96,768]{1,0:T(8,128)(2,1)S(1)}, u32[]{:S(2)}, u32[]{:S(2)}) collective-permute-start(bf16[96,768]{1,0:T(8,128)(2,1)S(1)} %get-tuple-element.77), channel_id=1, source_target_pairs={{0,8},{8,0},{16,24},{24,16},{1,9},{9,1},{17,25},{25,17},{2,10},{10... | collective-permute-start | bytes 442376 | tf_op jit(solution)/shard_map/ppermute | solution.py:33
  52.0 3.8 %shard_map.213 = (bf16[96,704]{1,0:T(8,128)(2,1)S(1)}, f32[96,128]{1,0:T(8,128)S(1)}, f32[24,512]{1,0:T(8,128)S(1)}, bf16[704,4096]{1,0:T(8,128)(2,1)S(1)}) custom-call(bf16[96,512]{1,0:T(8,128)(2,1)S(1)} %shard_map.212.refs_0_.mine, bf16[96,512]{1,0:T(8,128)(2,1)S(1)} %collective-permute-done.13.refs_1_, ...), custom_call_target="tpu_custom_call" | custom-call | flops 1107296256 | tf_op jit(solution)/shard_map/pallas_call | solution.py:50
  56.1 2.4 %collective-permute-done.21.refs_2_ = bf16[96,768]{1,0:T(8,128)(2,1)S(1)} collective-permute-done((bf16[96,768]{1,0:T(8,128)(2,1)S(1)}, bf16[96,768]{1,0:T(8,128)(2,1)S(1)}, u32[]{:S(2)}, u32[]{:S(2)}) %collective-permute-start.21) | collective-permute-done | bytes 147488 | tf_op jit(solution)/shard_map/ppermute | solution.py:33
  58.5 0.9 %shard_map.215 = (bf16[96,2048]{1,0:T(8,128)(2,1)S(1)}, bf16[96,352]{1,0:T(8,128)(2,1)S(1)}) custom-call(bf16[96,704]{1,0:T(8,128)(2,1)S(1)} %get-tuple-element.75.inner, f32[96,768]{1,0:T(8,128)S(1)} %get-tuple-element.76.refs_0_, bf16[96,768]{1,0:T(8,128)(2,1)S(1)} %collective-permute-done.20.refs_1_, bf16[96,768]{1,0:T(8,128)(2,1)S(1)} %collective-permute-done.21.refs_2_, ...), custom_call_target="tpu_custom_call" | custom-call | flops 276824064 | tf_op jit(solution)/shard_map/pallas_call | solution.py:50
  59.4 0.8 %shard_map.216.keep = f32[96,2048]{1,0:T(8,128)S(1)} custom-call(bf16[96,704]{1,0:T(8,128)(2,1)S(1)} %get-tuple-element.75.inner, bf16[96,352]{1,0:T(8,128)(2,1)S(1)} %get-tuple-element.80.refs_0_, bf16[704,4096]{1,0:T(8,128)(2,1)S(1)} %get-tuple-element.79.refs_5_.refs_1_, bf16[352,1024]{1,0:T(8,128)(2,1)S(1)} %copy-done), custom_call_target="tpu_custom_call" | custom-call | flops 276824064 | tf_op jit(solution)/shard_map/pallas_call | solution.py:50
  60.3 0.9 %collective-permute-done.23.got = bf16[96,2048]{1,0:T(8,128)(2,1)S(1)} collective-permute-done((bf16[96,2048]{1,0:T(8,128)(2,1)S(1)}, bf16[96,2048]{1,0:T(8,128)(2,1)S(1)}, u32[]{:S(2)}, u32[]{:S(2)}) %collective-permute-start.23) | collective-permute-done | bytes 393248 | tf_op jit(solution)/shard_map/ppermute | solution.py:33
  61.2 1.0 %collective-permute-start.24 = (bf16[24,2048]{1,0:T(8,128)(2,1)S(1)}, bf16[24,2048]{1,0:T(8,128)(2,1)S(1)}, u32[]{:S(2)}, u32[]{:S(2)}) collective-permute-start(bf16[24,2048]{1,0:T(8,128)(2,1)S(1)} %get-tuple-element.83), channel_id=1, source_target_pairs={{0,8},{8,0},{16,24},{24,16},{1,9},{9,1},{17,25},{25,17},{2,10},{10... | collective-permute-start | bytes 294920 | tf_op jit(solution)/shard_map/ppermute | solution.py:33
  62.2 0.9 %collective-permute-start.25 = (bf16[24,2048]{1,0:T(8,128)(2,1)S(1)}, bf16[24,2048]{1,0:T(8,128)(2,1)S(1)}, u32[]{:S(2)}, u32[]{:S(2)}) collective-permute-start(bf16[24,2048]{1,0:T(8,128)(2,1)S(1)} %get-tuple-element.84), channel_id=1, source_target_pairs={{0,16},{8,24},{16,0},{24,8},{1,17},{9,25},{17,1},{25,9},{2,18},{10... | collective-permute-start | bytes 294920 | tf_op jit(solution)/shard_map/ppermute | solution.py:33
  63.2 1.6 %collective-permute-start.26 = (bf16[24,2048]{1,0:T(8,128)(2,1)S(1)}, bf16[24,2048]{1,0:T(8,128)(2,1)S(1)}, u32[]{:S(2)}, u32[]{:S(2)}) collective-permute-start(bf16[24,2048]{1,0:T(8,128)(2,1)S(1)} %get-tuple-element.85), channel_id=1, source_target_pairs={{0,24},{8,16},{16,8},{24,0},{1,25},{9,17},{17,9},{25,1},{2,26},{10... | collective-permute-start | bytes 294920 | tf_op jit(solution)/shard_map/ppermute | solution.py:33
  64.8 2.7 %shard_map.218 = (f32[24,2,128,128]{3,2,1,0:T(8,128)}, f32[8,128]{1,0:T(8,128)S(1)}) custom-call(f32[24,768]{1,0:T(8,128)S(1)} %get-tuple-element.87.gates, f32[24,2,128,128]{3,2,1,0:T(8,128)S(1)} %get-tuple-element.65.refs_7_.state, f32[24,2048]{1,0:T(8,128)S(1)} %get-tuple-element.82._.refs_0_), custom_call_target="tpu_custom_call" | custom-call | flops 67108864 | tf_op jit(solution)/shard_map/pallas_call | solution.py:531
  67.5 1.5 %collective-permute-done.25.refs_2_ = bf16[24,2048]{1,0:T(8,128)(2,1)S(1)} collective-permute-done((bf16[24,2048]{1,0:T(8,128)(2,1)S(1)}, bf16[24,2048]{1,0:T(8,128)(2,1)S(1)}, u32[]{:S(2)}, u32[]{:S(2)}) %collective-permute-start.25) | collective-permute-done | bytes 98336 | tf_op jit(solution)/shard_map/ppermute | solution.py:33
  69.0 0.9 %collective-permute-start.27 = (bf16[24,512]{1,0:T(8,128)(2,1)S(1)}, bf16[24,512]{1,0:T(8,128)(2,1)S(1)}, u32[]{:S(2)}, u32[]{:S(2)}) collective-permute-start(bf16[24,512]{1,0:T(8,128)(2,1)S(1)} %get-tuple-element.90), channel_id=1, source_target_pairs={{0,2},{1,3},{2,0},{3,1},{4,6},{5,7},{6,4},{7,5},{8,10},{9,11},{10,... | collective-permute-start | bytes 73736 | tf_op jit(solution)/shard_map/ppermute | solution.py:33
  69.9 2.3 %collective-permute-start.28 = (bf16[24,512]{1,0:T(8,128)(2,1)S(1)}, bf16[24,512]{1,0:T(8,128)(2,1)S(1)}, u32[]{:S(2)}, u32[]{:S(2)}) collective-permute-start(bf16[24,512]{1,0:T(8,128)(2,1)S(1)} %get-tuple-element.91), channel_id=1, source_target_pairs={{0,4},{1,5},{2,6},{3,7},{4,0},{5,1},{6,2},{7,3},{8,12},{9,13},{10,... | collective-permute-start | bytes 73736 | tf_op jit(solution)/shard_map/ppermute | solution.py:33
  72.1 1.3 %collective-permute-start.29 = (bf16[24,512]{1,0:T(8,128)(2,1)S(1)}, bf16[24,512]{1,0:T(8,128)(2,1)S(1)}, u32[]{:S(2)}, u32[]{:S(2)}) collective-permute-start(bf16[24,512]{1,0:T(8,128)(2,1)S(1)} %get-tuple-element.92), channel_id=1, source_target_pairs={{0,6},{1,7},{2,4},{3,5},{4,2},{5,3},{6,0},{7,1},{8,14},{9,15},{10,... | collective-permute-start | bytes 73736 | tf_op jit(solution)/shard_map/ppermute | solution.py:33
  73.5 1.1 %collective-permute-done.28.refs_2_ = bf16[24,512]{1,0:T(8,128)(2,1)S(1)} collective-permute-done((bf16[24,512]{1,0:T(8,128)(2,1)S(1)}, bf16[24,512]{1,0:T(8,128)(2,1)S(1)}, u32[]{:S(2)}, u32[]{:S(2)}) %collective-permute-start.28) | collective-permute-done | bytes 24608 | tf_op jit(solution)/shard_map/ppermute | solution.py:33
  74.6 3.1 %collective-permute-done.29.refs_3_ = bf16[24,512]{1,0:T(8,128)(2,1)S(1)} collective-permute-done((bf16[24,512]{1,0:T(8,128)(2,1)S(1)}, bf16[24,512]{1,0:T(8,128)(2,1)S(1)}, u32[]{:S(2)}, u32[]{:S(2)}) %collective-permute-start.29) | collective-permute-done | bytes 24608 | tf_op jit(solution)/shard_map/ppermute | solution.py:33
  77.8 0.6 shard_map.220
  (47 shorter events, 2.3 us)
Async XLA Ops:
  0.6 16.7 %copy-start.5 = (s32[24,2]{0,1:T(2,128)S(1)}, s32[24,2]{0,1:T(2,128)}, u32[]{:S(2)}) copy-start(s32[24,2]{0,1:T(2,128)} %param.32) | copy-start | bytes 580
  0.6 17.2 %copy-start.7 = (f32[256]{0:T(256)S(1)}, f32[256]{0:T(256)}, u32[]{:S(2)}) copy-start(f32[256]{0:T(256)} %param.27) | copy-start | bytes 3076
  0.7 17.2 %copy-start.6 = (f32[256]{0:T(256)S(1)}, f32[256]{0:T(256)}, u32[]{:S(2)}) copy-start(f32[256]{0:T(256)} %param.26) | copy-start | bytes 3076
  1.6 7.7 %collective-permute-start = (bf16[24,1024]{1,0:T(8,128)(2,1)S(1)}, bf16[24,1024]{1,0:T(8,128)(2,1)S(1)}, u32[]{:S(2)}, u32[]{:S(2)}) collective-permute-start(bf16[24,1024]{1,0:T(8,128)(2,1)S(1)} %get-tuple-element.49), channel_id=1, source_target_pairs={{0,9},{1,8},{2,11},{3,10},{4,13},{5,12},{6,15},{7,14},{8,1},{9,0},... | collective-permute-start | bytes 147464 | tf_op jit(solution)/shard_map/ppermute | solution.py:381
  4.1 5.3 %collective-permute-start.1 = (bf16[24,1024]{1,0:T(8,128)(2,1)S(1)}, bf16[24,1024]{1,0:T(8,128)(2,1)S(1)}, u32[]{:S(2)}, u32[]{:S(2)}) collective-permute-start(bf16[24,1024]{1,0:T(8,128)(2,1)S(1)} %get-tuple-element.50), channel_id=1, source_target_pairs={{0,17},{1,16},{2,19},{3,18},{4,21},{5,20},{6,23},{7,22},{8,25},{9,... | collective-permute-start | bytes 147464 | tf_op jit(solution)/shard_map/ppermute | solution.py:381
  5.9 4.9 %collective-permute-start.2 = (bf16[24,1024]{1,0:T(8,128)(2,1)S(1)}, bf16[24,1024]{1,0:T(8,128)(2,1)S(1)}, u32[]{:S(2)}, u32[]{:S(2)}) collective-permute-start(bf16[24,1024]{1,0:T(8,128)(2,1)S(1)} %get-tuple-element.51), channel_id=1, source_target_pairs={{0,25},{1,24},{2,27},{3,26},{4,29},{5,28},{6,31},{7,30},{8,17},{9,... | collective-permute-start | bytes 147464 | tf_op jit(solution)/shard_map/ppermute | solution.py:381
  6.6 18.7 %copy-start.3 = (bf16[256,1024]{1,0:T(8,128)(2,1)S(1)}, bf16[256,1024]{1,0:T(8,128)(2,1)}, u32[]{:S(2)}) copy-start(bf16[256,1024]{1,0:T(8,128)(2,1)} %refs_4_.1) | copy-start | bytes 1572868
  11.3 6.2 %collective-permute-start.3 = (bf16[24,1024]{1,0:T(8,128)(2,1)S(1)}, bf16[24,1024]{1,0:T(8,128)(2,1)S(1)}, u32[]{:S(2)}, u32[]{:S(2)}) collective-permute-start(bf16[24,1024]{1,0:T(8,128)(2,1)S(1)} %get-tuple-element.59), channel_id=1, source_target_pairs={{0,8},{8,0},{16,24},{24,16},{1,9},{9,1},{17,25},{25,17},{2,10},{10... | collective-permute-start | bytes 147464 | tf_op jit(solution)/shard_map/ppermute | solution.py:33
  11.8 5.8 %collective-permute-start.4 = (bf16[24,1024]{1,0:T(8,128)(2,1)S(1)}, bf16[24,1024]{1,0:T(8,128)(2,1)S(1)}, u32[]{:S(2)}, u32[]{:S(2)}) collective-permute-start(bf16[24,1024]{1,0:T(8,128)(2,1)S(1)} %get-tuple-element.60), channel_id=1, source_target_pairs={{0,16},{8,24},{16,0},{24,8},{1,17},{9,25},{17,1},{25,9},{2,18},{10... | collective-permute-start | bytes 147464 | tf_op jit(solution)/shard_map/ppermute | solution.py:33
  12.8 5.0 %collective-permute-start.5 = (bf16[24,1024]{1,0:T(8,128)(2,1)S(1)}, bf16[24,1024]{1,0:T(8,128)(2,1)S(1)}, u32[]{:S(2)}, u32[]{:S(2)}) collective-permute-start(bf16[24,1024]{1,0:T(8,128)(2,1)S(1)} %get-tuple-element.61), channel_id=1, source_target_pairs={{0,24},{8,16},{16,8},{24,0},{1,25},{9,17},{17,9},{25,1},{2,26},{10... | collective-permute-start | bytes 147464 | tf_op jit(solution)/shard_map/ppermute | solution.py:33
  19.0 4.7 %collective-permute-start.8 = (bf16[24,384]{1,0:T(8,128)(2,1)S(1)}, bf16[24,384]{1,0:T(8,128)(2,1)S(1)}, u32[]{:S(2)}, u32[]{:S(2)}) collective-permute-start(bf16[24,384]{1,0:T(8,128)(2,1)S(1)} %get-tuple-element.68.refs_0_.refs_8_), channel_id=1, source_target_pairs={{0,24},{8,16},{16,8},{24,0},{1,25},{9,17},{17,9},{25,1},{2,26},{10... | collective-permute-start | bytes 55304 | tf_op jit(solution)/shard_map/ppermute | solution.py:33
  21.1 3.8 %collective-permute-start.7 = (bf16[24,384]{1,0:T(8,128)(2,1)S(1)}, bf16[24,384]{1,0:T(8,128)(2,1)S(1)}, u32[]{:S(2)}, u32[]{:S(2)}) collective-permute-start(bf16[24,384]{1,0:T(8,128)(2,1)S(1)} %get-tuple-element.68.refs_0_.refs_8_), channel_id=1, source_target_pairs={{0,16},{8,24},{16,0},{24,8},{1,17},{9,25},{17,1},{25,9},{2,18},{10... | collective-permute-start | bytes 55304 | tf_op jit(solution)/shard_map/ppermute | solution.py:33
  21.5 3.8 %collective-permute-start.6 = (bf16[24,384]{1,0:T(8,128)(2,1)S(1)}, bf16[24,384]{1,0:T(8,128)(2,1)S(1)}, u32[]{:S(2)}, u32[]{:S(2)}) collective-permute-start(bf16[24,384]{1,0:T(8,128)(2,1)S(1)} %get-tuple-element.68.refs_0_.refs_8_), channel_id=1, source_target_pairs={{0,8},{8,0},{16,24},{24,16},{1,9},{9,1},{17,25},{25,17},{2,10},{10... | collective-permute-start | bytes 55304 | tf_op jit(solution)/shard_map/ppermute | solution.py:33
  25.5 1.4 %collective-permute-start.9 = (bf16[96,512]{1,0:T(8,128)(2,1)S(1)}, bf16[96,512]{1,0:T(8,128)(2,1)S(1)}, u32[]{:S(2)}, u32[]{:S(2)}) collective-permute-start(bf16[96,512]{1,0:T(8,128)(2,1)S(1)} %get-tuple-element.70), channel_id=1, source_target_pairs={{0,1},{1,0},{2,3},{3,2},{4,5},{5,4},{6,7},{7,6},{8,9},{9,8},{10,11... | collective-permute-start | bytes 294920 | tf_op jit(solution)/shard_map/ppermute | solution.py:33
  26.9 9.1 %collective-permute-start.12 = (bf16[96,512]{1,0:T(8,128)(2,1)S(1)}, bf16[96,512]{1,0:T(8,128)(2,1)S(1)}, u32[]{:S(2)}, u32[]{:S(2)}) collective-permute-start(bf16[96,512]{1,0:T(8,128)(2,1)S(1)} %shard_map.210.refs_2_), channel_id=1, source_target_pairs={{0,7},{1,6},{2,5},{3,4},{4,3},{5,2},{6,1},{7,0},{8,15},{9,14},{10,... | collective-permute-start | bytes 294920 | tf_op jit(solution)/shard_map/ppermute | solution.py:33
  30.3 8.7 %collective-permute-start.11 = (bf16[96,512]{1,0:T(8,128)(2,1)S(1)}, bf16[96,512]{1,0:T(8,128)(2,1)S(1)}, u32[]{:S(2)}, u32[]{:S(2)}) collective-permute-start(bf16[96,512]{1,0:T(8,128)(2,1)S(1)} %shard_map.210.refs_2_), channel_id=1, source_target_pairs={{0,5},{1,4},{2,7},{3,6},{4,1},{5,0},{6,3},{7,2},{8,13},{9,12},{10,... | collective-permute-start | bytes 294920 | tf_op jit(solution)/shard_map/ppermute | solution.py:33
  30.3 8.7 %collective-permute-start.10 = (bf16[96,512]{1,0:T(8,128)(2,1)S(1)}, bf16[96,512]{1,0:T(8,128)(2,1)S(1)}, u32[]{:S(2)}, u32[]{:S(2)}) collective-permute-start(bf16[96,512]{1,0:T(8,128)(2,1)S(1)} %shard_map.210.refs_2_), channel_id=1, source_target_pairs={{0,2},{1,3},{2,0},{3,1},{4,6},{5,7},{6,4},{7,5},{8,10},{9,11},{10,... | collective-permute-start | bytes 294920 | tf_op jit(solution)/shard_map/ppermute | solution.py:33
  31.1 16.7 %copy-start.1 = (bf16[1024,352]{0,1:T(8,128)(2,1)S(1)}, bf16[1024,352]{0,1:T(8,128)(2,1)}, u32[]{:S(2)}) copy-start(bf16[1024,352]{0,1:T(8,128)(2,1)} %param.36) | copy-start | bytes 2162692
  31.1 16.7 %copy-start.2 = (bf16[1024,352]{0,1:T(8,128)(2,1)S(1)}, bf16[1024,352]{0,1:T(8,128)(2,1)}, u32[]{:S(2)}) copy-start(bf16[1024,352]{0,1:T(8,128)(2,1)} %param.37) | copy-start | bytes 2162692
  31.1 16.7 %copy-start.4 = (f32[4096]{0:T(1024)S(1)}, f32[4096]{0:T(1024)}, u32[]{:S(2)}) copy-start(f32[4096]{0:T(1024)} %param.30) | copy-start | bytes 49156
  39.2 5.8 %collective-permute-start.15 = (bf16[96,512]{1,0:T(8,128)(2,1)S(1)}, bf16[96,512]{1,0:T(8,128)(2,1)S(1)}, u32[]{:S(2)}, u32[]{:S(2)}) collective-permute-start(bf16[96,512]{1,0:T(8,128)(2,1)S(1)} %shard_map.212.refs_0_.mine), channel_id=1, source_target_pairs={{0,25},{1,24},{2,27},{3,26},{4,29},{5,28},{6,31},{7,30},{8,17},{9,... | collective-permute-start | bytes 294920 | tf_op jit(solution)/shard_map/ppermute | solution.py:381
  40.4 6.9 %collective-permute-start.14 = (bf16[96,512]{1,0:T(8,128)(2,1)S(1)}, bf16[96,512]{1,0:T(8,128)(2,1)S(1)}, u32[]{:S(2)}, u32[]{:S(2)}) collective-permute-start(bf16[96,512]{1,0:T(8,128)(2,1)S(1)} %shard_map.212.refs_0_.mine), channel_id=1, source_target_pairs={{0,17},{1,16},{2,19},{3,18},{4,21},{5,20},{6,23},{7,22},{8,25},{9,... | collective-permute-start | bytes 294920 | tf_op jit(solution)/shard_map/ppermute | solution.py:381
  41.4 6.0 %collective-permute-start.13 = (bf16[96,512]{1,0:T(8,128)(2,1)S(1)}, bf16[96,512]{1,0:T(8,128)(2,1)S(1)}, u32[]{:S(2)}, u32[]{:S(2)}) collective-permute-start(bf16[96,512]{1,0:T(8,128)(2,1)S(1)} %shard_map.212.refs_0_.mine), channel_id=1, source_target_pairs={{0,8},{1,9},{2,10},{3,11},{4,12},{5,13},{6,14},{7,15},{8,0},{9,1},... | collective-permute-start | bytes 294920 | tf_op jit(solution)/shard_map/ppermute | solution.py:381
  42.4 5.4 %collective-permute-start.16 = (bf16[96,512]{1,0:T(8,128)(2,1)S(1)}, bf16[96,512]{1,0:T(8,128)(2,1)S(1)}, u32[]{:S(2)}, u32[]{:S(2)}) collective-permute-start(bf16[96,512]{1,0:T(8,128)(2,1)S(1)} %shard_map.212.refs_0_.mine), channel_id=1, source_target_pairs={{0,1},{1,0},{2,3},{3,2},{4,5},{5,4},{6,7},{7,6},{8,9},{9,8},{10,11... | collective-permute-start | bytes 294920 | tf_op jit(solution)/shard_map/ppermute | solution.py:33
  45.0 6.0 %collective-permute-start.19 = (bf16[96,512]{1,0:T(8,128)(2,1)S(1)}, bf16[96,512]{1,0:T(8,128)(2,1)S(1)}, u32[]{:S(2)}, u32[]{:S(2)}) collective-permute-start(bf16[96,512]{1,0:T(8,128)(2,1)S(1)} %collective-permute-done.15.refs_3_), channel_id=1, source_target_pairs={{0,1},{1,0},{2,3},{3,2},{4,5},{5,4},{6,7},{7,6},{8,9},{9,8},{10,11... | collective-permute-start | bytes 294920 | tf_op jit(solution)/shard_map/ppermute | solution.py:33
  47.3 4.7 %collective-permute-start.18 = (bf16[96,512]{1,0:T(8,128)(2,1)S(1)}, bf16[96,512]{1,0:T(8,128)(2,1)S(1)}, u32[]{:S(2)}, u32[]{:S(2)}) collective-permute-start(bf16[96,512]{1,0:T(8,128)(2,1)S(1)} %collective-permute-done.14.refs_2_), channel_id=1, source_target_pairs={{0,1},{1,0},{2,3},{3,2},{4,5},{5,4},{6,7},{7,6},{8,9},{9,8},{10,11... | collective-permute-start | bytes 294920 | tf_op jit(solution)/shard_map/ppermute | solution.py:33
  47.5 4.5 %collective-permute-start.17 = (bf16[96,512]{1,0:T(8,128)(2,1)S(1)}, bf16[96,512]{1,0:T(8,128)(2,1)S(1)}, u32[]{:S(2)}, u32[]{:S(2)}) collective-permute-start(bf16[96,512]{1,0:T(8,128)(2,1)S(1)} %collective-permute-done.13.refs_1_), channel_id=1, source_target_pairs={{0,1},{1,0},{2,3},{3,2},{4,5},{5,4},{6,7},{7,6},{8,9},{9,8},{10,11... | collective-permute-start | bytes 294920 | tf_op jit(solution)/shard_map/ppermute | solution.py:33
  48.4 7.7 %collective-permute-start.22 = (bf16[96,768]{1,0:T(8,128)(2,1)S(1)}, bf16[96,768]{1,0:T(8,128)(2,1)S(1)}, u32[]{:S(2)}, u32[]{:S(2)}) collective-permute-start(bf16[96,768]{1,0:T(8,128)(2,1)S(1)} %get-tuple-element.77), channel_id=1, source_target_pairs={{0,24},{8,16},{16,8},{24,0},{1,25},{9,17},{17,9},{25,1},{2,26},{10... | collective-permute-start | bytes 442376 | tf_op jit(solution)/shard_map/ppermute | solution.py:33
  49.9 8.6 %collective-permute-start.21 = (bf16[96,768]{1,0:T(8,128)(2,1)S(1)}, bf16[96,768]{1,0:T(8,128)(2,1)S(1)}, u32[]{:S(2)}, u32[]{:S(2)}) collective-permute-start(bf16[96,768]{1,0:T(8,128)(2,1)S(1)} %get-tuple-element.77), channel_id=1, source_target_pairs={{0,16},{8,24},{16,0},{24,8},{1,17},{9,25},{17,1},{25,9},{2,18},{10... | collective-permute-start | bytes 442376 | tf_op jit(solution)/shard_map/ppermute | solution.py:33
  51.0 7.5 %collective-permute-start.20 = (bf16[96,768]{1,0:T(8,128)(2,1)S(1)}, bf16[96,768]{1,0:T(8,128)(2,1)S(1)}, u32[]{:S(2)}, u32[]{:S(2)}) collective-permute-start(bf16[96,768]{1,0:T(8,128)(2,1)S(1)} %get-tuple-element.77), channel_id=1, source_target_pairs={{0,8},{8,0},{16,24},{24,16},{1,9},{9,1},{17,25},{25,17},{2,10},{10... | collective-permute-start | bytes 442376 | tf_op jit(solution)/shard_map/ppermute | solution.py:33
  51.9 6.5 %copy-start = (bf16[352,1024]{1,0:T(8,128)(2,1)S(1)}, bf16[352,1024]{1,0:T(8,128)(2,1)}, u32[]{:S(2)}) copy-start(bf16[352,1024]{1,0:T(8,128)(2,1)} %refs_2_.3) | copy-start | bytes 2162692
  59.3 1.8 %collective-permute-start.23 = (bf16[96,2048]{1,0:T(8,128)(2,1)S(1)}, bf16[96,2048]{1,0:T(8,128)(2,1)S(1)}, u32[]{:S(2)}, u32[]{:S(2)}) collective-permute-start(bf16[96,2048]{1,0:T(8,128)(2,1)S(1)} %get-tuple-element.81), channel_id=1, source_target_pairs={{0,1},{1,0},{2,3},{3,2},{4,5},{5,4},{6,7},{7,6},{8,9},{9,8},{10,11... | collective-permute-start | bytes 1179656 | tf_op jit(solution)/shard_map/ppermute | solution.py:33
  61.2 6.3 %collective-permute-start.24 = (bf16[24,2048]{1,0:T(8,128)(2,1)S(1)}, bf16[24,2048]{1,0:T(8,128)(2,1)S(1)}, u32[]{:S(2)}, u32[]{:S(2)}) collective-permute-start(bf16[24,2048]{1,0:T(8,128)(2,1)S(1)} %get-tuple-element.83), channel_id=1, source_target_pairs={{0,8},{8,0},{16,24},{24,16},{1,9},{9,1},{17,25},{25,17},{2,10},{10... | collective-permute-start | bytes 294920 | tf_op jit(solution)/shard_map/ppermute | solution.py:33
  62.2 6.7 %collective-permute-start.25 = (bf16[24,2048]{1,0:T(8,128)(2,1)S(1)}, bf16[24,2048]{1,0:T(8,128)(2,1)S(1)}, u32[]{:S(2)}, u32[]{:S(2)}) collective-permute-start(bf16[24,2048]{1,0:T(8,128)(2,1)S(1)} %get-tuple-element.84), channel_id=1, source_target_pairs={{0,16},{8,24},{16,0},{24,8},{1,17},{9,25},{17,1},{25,9},{2,18},{10... | collective-permute-start | bytes 294920 | tf_op jit(solution)/shard_map/ppermute | solution.py:33
  63.2 5.8 %collective-permute-start.26 = (bf16[24,2048]{1,0:T(8,128)(2,1)S(1)}, bf16[24,2048]{1,0:T(8,128)(2,1)S(1)}, u32[]{:S(2)}, u32[]{:S(2)}) collective-permute-start(bf16[24,2048]{1,0:T(8,128)(2,1)S(1)} %get-tuple-element.85), channel_id=1, source_target_pairs={{0,24},{8,16},{16,8},{24,0},{1,25},{9,17},{17,9},{25,1},{2,26},{10... | collective-permute-start | bytes 294920 | tf_op jit(solution)/shard_map/ppermute | solution.py:33
  69.0 4.5 %collective-permute-start.27 = (bf16[24,512]{1,0:T(8,128)(2,1)S(1)}, bf16[24,512]{1,0:T(8,128)(2,1)S(1)}, u32[]{:S(2)}, u32[]{:S(2)}) collective-permute-start(bf16[24,512]{1,0:T(8,128)(2,1)S(1)} %get-tuple-element.90), channel_id=1, source_target_pairs={{0,2},{1,3},{2,0},{3,1},{4,6},{5,7},{6,4},{7,5},{8,10},{9,11},{10,... | collective-permute-start | bytes 73736 | tf_op jit(solution)/shard_map/ppermute | solution.py:33
  69.9 4.7 %collective-permute-start.28 = (bf16[24,512]{1,0:T(8,128)(2,1)S(1)}, bf16[24,512]{1,0:T(8,128)(2,1)S(1)}, u32[]{:S(2)}, u32[]{:S(2)}) collective-permute-start(bf16[24,512]{1,0:T(8,128)(2,1)S(1)} %get-tuple-element.91), channel_id=1, source_target_pairs={{0,4},{1,5},{2,6},{3,7},{4,0},{5,1},{6,2},{7,3},{8,12},{9,13},{10,... | collective-permute-start | bytes 73736 | tf_op jit(solution)/shard_map/ppermute | solution.py:33
  72.1 5.6 %collective-permute-start.29 = (bf16[24,512]{1,0:T(8,128)(2,1)S(1)}, bf16[24,512]{1,0:T(8,128)(2,1)S(1)}, u32[]{:S(2)}, u32[]{:S(2)}) collective-permute-start(bf16[24,512]{1,0:T(8,128)(2,1)S(1)} %get-tuple-element.92), channel_id=1, source_target_pairs={{0,6},{1,7},{2,4},{3,5},{4,2},{5,3},{6,0},{7,1},{8,14},{9,15},{10,... | collective-permute-start | bytes 73736 | tf_op jit(solution)/shard_map/ppermute | solution.py:33
